TPU v7x, 256 devices: a whole 4x4x8 slice. The times are simulated.
256 devices in a mesh: sp: 32 (over z, x), tp: 8 (over y, core).
Axes of the slice: x: 4, y: 4, z: 8, core: 2. Of those that a mesh axis runs over, the one named last changes fastest.
Arguments:
- latents: bfloat16 [16384, 2048], P(('sp', 'tp')), may hold values from -6 to 6
- context: bfloat16 [512, 2048], P('sp'), may hold values from -6 to 6
- cond: float32 [2048], P('sp'), may hold values from -6 to 6
- ctx_cond: float32 [2048], P('sp'), may hold values from -6 to 6
- mod_weight: float32 [2048, 6144], P('sp', 'tp'), may hold values from -0.125 to 0.125
- query_weight: bfloat16 [2048, 2048], P(None, 'tp'), may hold values from -1 to 1, as said below
- key_matrix: bfloat16 [2048, 1024], P(None, 'tp'), may hold values from -1 to 1, as said below
- value_matrix: bfloat16 [2048, 1024], P(None, 'tp'), may hold values from -0.125 to 0.125
- out_weight: bfloat16 [2048, 2048], P('tp'), may hold values from -0.125 to 0.125
- query_gain: float32 [128], replicated, may hold values from 0.7 to 7
- key_gain: float32 [128], replicated, may hold values from 0.7 to 7
Outputs:
- updated: bfloat16 [16384, 2048], P(('sp', 'tp'))
Inputs may be any that keep to these rules, and one draw needn't show every extreme that they name: `query_weight`: entries of order 2048 to the power -1/2. `key_matrix`: entries of order 2048 to the power -1/2.
All inputs are finite; a program needn't handle non-finite values.
Results may differ from a plain program's by a relative error of at most 0.0085.
The roundings to bfloat16 on the way count: a program that leaves them out, or rounds other values in their place, can miss the bound.
Values may be sent and summed in bfloat16 or wider, within the bound.
No kernel may reach another device: no remote copies, remote signals or barrier semaphores. Data moves between devices by JAX's collectives and lax.ppermute only.
A program may use at most 128 MiB of HBM per device.

v0:
```python
import functools
import math

import jax
import jax.numpy as jnp
import numpy as np
from jax import lax
from jax.experimental import pallas as pl
from jax.experimental.pallas import tpu as pltpu
from jax.sharding import Mesh
from jax.sharding import PartitionSpec as P

GRID_W = 64
SP = ("z", "x")
TP = ("y", "c")
ALL = ("z", "x", "y", "c")
NORM_EPS = 1e-06
ROPE_BASE = 10000.0
HD = 128
OFFS = (0, -1, 1, 2)
BQ = 512

BF = jnp.bfloat16
F32 = jnp.float32


def shift(n, k):
    return [(i, (i + k) % n) for i in range(n)]


def rope_tables(count):
    quarter = HD // 4
    freq = ROPE_BASE ** (-np.arange(quarter, dtype=np.float64) / quarter)

    def pair(n):
        angle = np.arange(n, dtype=np.float64)[:, None] * freq[None, :]
        cos, sin = np.cos(angle), np.sin(angle)
        return np.concatenate([cos, cos], 1), np.concatenate([-sin, sin], 1)

    (rc, rs), (cc, cs) = pair(count // GRID_W), pair(GRID_W)
    left = lambda a: np.concatenate([a, np.zeros_like(a)], 1).astype(np.float32)
    right = lambda a: np.concatenate([np.zeros_like(a), a], 1).astype(np.float32)
    return left(rc), left(rs), right(cc), right(cs)


def rms(v):
    return v * lax.rsqrt(jnp.mean(v * v, axis=-1, keepdims=True) + NORM_EPS)


def columns_of(mod, row, first, last):
    wide = mod.shape[2]
    found = []
    for piece in range(mod.shape[0]):
        lo, hi = max(first - piece * wide, 0), min(last - piece * wide, wide)
        if lo < hi:
            found.append(mod[piece, row : row + 1, lo:hi])
    return jnp.concatenate(found, axis=1)


def tp_of(offset, core):
    return lax.rem(lax.axis_index("y") + offset + 4, 4) * 2 + core


def project_kernel(*refs):
    blocks, mod, far = list(refs[:7]), refs[7], refs[8:19]
    q_out, kv_out, buf = refs[19:22]
    held, arrived = refs[22:33], refs[33]
    copies = [pltpu.make_async_copy(f, h, arrived.at[i]) for i, (f, h) in enumerate(zip(far, held))]
    for copy in copies:
        copy.start()
    lat, wq, wk, wv, ctx, qg, kg, row_c, row_s, col_c, col_s = held
    blocks.insert(0, lat)
    width = ctx.shape[1]
    rows = GRID_W
    sp = lax.axis_index("z") * 4 + lax.axis_index("x")
    core = lax.axis_index("c")

    def modulate(v, r):
        scale = columns_of(mod, r, width, 2 * width)
        return (rms(v.astype(F32)) * (1.0 + scale) + columns_of(mod, r, 0, width)).astype(BF)

    def turn(v, cos, sin):
        lane = lax.broadcasted_iota(jnp.int32, v.shape, 1)
        other = jnp.where(lane % 64 < 32, pltpu.roll(v, HD - 32, 1), pltpu.roll(v, 32, 1))
        return v * cos + other * sin

    def dot(a, b):
        return jnp.dot(a, b, preferred_element_type=F32)

    for side in range(2):
        for j in (1, 2, 3, 0) if side == 0 else range(4):
            if side == 0 and j == 0:
                for copy in copies:
                    copy.wait()
            buf[j * rows : (j + 1) * rows] = modulate(blocks[side * 4 + j][...], 0)
        normed = buf[...]
        q = dot(normed, wq[...])
        k = dot(normed, wk[...])
        v = dot(normed, wv[...]).astype(BF)
        k = rms(k) * kg[...]
        q0 = rms(q[:, :HD]) * qg[...]
        q1 = rms(q[:, HD:]) * qg[...]
        for j in range(4):
            at = slice(j * rows, (j + 1) * rows)
            tp = tp_of(OFFS[j], core if side == 0 else 1 - core)
            cos = row_c[pl.ds(sp * 8 + tp, 1), :] + col_c[...]
            sin = row_s[pl.ds(sp * 8 + tp, 1), :] + col_s[...]
            to = pl.ds(pl.multiple_of(tp * rows, rows), rows)
            q_out[0, to, :] = turn(q0[at], cos, sin).astype(BF)
            q_out[1, to, :] = turn(q1[at], cos, sin).astype(BF)
            kv_out[to, :HD] = turn(k[at], cos, sin).astype(BF)
            kv_out[to, HD:] = v[at]
    normed = modulate(ctx[...], 1)
    total = 8 * rows
    kv_out[total:, :HD] = (rms(dot(normed, wk[...])) * kg[...]).astype(BF)
    kv_out[total:, HD:] = dot(normed, wv[...]).astype(BF)


def scores_of(q, keys):
    return lax.dot_general(q, keys, (((1,), (1,)), ((), ())), preferred_element_type=F32)


def attend_kernel(*refs, first, last, pieces, lift):
    refs = list(refs)
    take = lambda n: [refs.pop(0) for _ in range(n)]
    scale = HD**-0.5
    c2 = scale * math.log2(math.e)
    if first:
        q_parts = take(4)
    else:
        q_all, m_in, l_in, acc_in = take(4)
    kv = take(2 * pieces) if last else take(pieces)
    tails = take(7) if last else []
    if last:
        (out,) = take(1)
    elif first:
        q_all, m_out, l_out, acc_out = take(4)
    else:
        m_out, l_out, acc_out = take(3)
    (k_buf, v_buf) = take(2)
    chunk = 512
    if last:
        kr, vr = kv
        k_buf[:chunk] = kr[:chunk]
        v_buf[:chunk] = vr[:chunk]
        k_buf[chunk : chunk + 16] = kr[chunk:]
        v_buf[chunk : chunk + 16] = vr[chunk:]
        for i, t in enumerate(tails):
            at = slice(chunk + 16 * (i + 1), chunk + 16 * (i + 2))
            k_buf[at] = t[chunk:, :HD]
            v_buf[at] = t[chunk:, HD:]
    else:
        for i, r in enumerate(kv):
            at = slice(i * chunk, (i + 1) * chunk)
            k_buf[at] = r[:chunk, :HD]
            v_buf[at] = r[:chunk, HD:]
    if first:
        for j, r in enumerate(q_parts):
            for h in range(2):
                q_all[(2 * j + h) * chunk : (2 * j + h + 1) * chunk] = r[h]

    def tree(values, op):
        while len(values) > 1:
            odd = values[len(values) // 2 * 2 :]
            values = [op(values[2 * i], values[2 * i + 1]) for i in range(len(values) // 2)] + odd
        return values[0]

    def softmax_block(at):
        s = scores_of(q_all[at], k_buf[...])
        tiles = [s[:, i * HD : (i + 1) * HD] for i in range(s.shape[1] // HD)]
        if last:
            tiles[-1] = tiles[-1] + lift / scale
        top = jnp.max(tree(tiles, jnp.maximum), axis=1, keepdims=True)
        if first:
            m_new = jnp.broadcast_to(top, (s.shape[0], HD))
        else:
            m_old = m_in[at]
            m_new = jnp.maximum(m_old, top)
        base = m_new * c2
        probs = [jnp.exp2(t * c2 - base) for t in tiles]
        p = jnp.concatenate([t.astype(BF) for t in probs], axis=1)
        pv = jnp.dot(p, v_buf[...], preferred_element_type=F32)
        sums = tree(probs, jnp.add)
        if first:
            return m_new, sums, pv
        alpha = jnp.exp2((m_old - m_new) * c2)
        return m_new, l_in[at] * alpha + sums, acc_in[at] * alpha + pv

    if not last:

        def step(b, carry):
            at = pl.ds(pl.multiple_of(b * BQ, BQ), BQ)
            m_out[at], l_out[at], acc_out[at] = softmax_block(at)
            return carry

        lax.fori_loop(0, 4096 // BQ, step, 0, unroll=2)
        return

    per = BQ // GRID_W
    out[:, GRID_W:, HD:] = jnp.zeros((32, 16, HD), BF)

    def step(b, carry):
        part, sub = b // (chunk // BQ), b % (chunk // BQ)
        x_at = lax.rem(lax.axis_index("x") + jnp.where(part == 1, 3, jnp.where(part == 0, 0, part - 1)), 4)
        found = []
        for h in range(2):
            at = pl.ds(pl.multiple_of((part * 2 + h) * chunk + sub * BQ, BQ), BQ)
            m, l, acc = softmax_block(at)
            l = jnp.broadcast_to(jnp.sum(l, axis=1, keepdims=True), l.shape)
            found.append(((acc / l).astype(BF), m * c2 + jnp.log2(l)))
        for i in range(per):
            rows = slice(i * GRID_W, (i + 1) * GRID_W)
            block = x_at * 8 + sub * per + i
            for h in range(2):
                out[block, :GRID_W, h * HD : (h + 1) * HD] = found[h][0][rows]
            lse = jnp.concatenate([found[0][1][rows], found[1][1][rows]], axis=0).T[:16]
            high = lse.astype(BF).astype(F32)
            mid = (lse - high).astype(BF).astype(F32)
            low = lse - high - mid
            line = lax.broadcasted_iota(jnp.int32, lse.shape, 0)
            packed = jnp.where(line == 0, high, jnp.where(line == 1, mid, jnp.where(line == 2, low, 0.0)))
            out[block, GRID_W:, :HD] = packed.astype(BF)
        return carry

    lax.fori_loop(0, 4 * (chunk // BQ), step, 0)


def near(v):
    return pltpu.with_memory_space_constraint(v, pltpu.VMEM)


VMEM = pl.BlockSpec(memory_space=pltpu.VMEM)


def attend(first, last, pieces, lift, operands):
    rows = 4096
    state = [pltpu.VMEM((rows, HD), F32)] * 3
    keys = 640 if last else 512 * pieces
    alias = {}
    if last:
        shape = [pltpu.VMEM((32, GRID_W + 16, 2 * HD), BF)]
    elif first:
        shape = [pltpu.VMEM((rows, HD), BF)] + state
    else:
        shape = state
        alias = {1: 0, 2: 1, 3: 2}
    return pl.pallas_call(
        functools.partial(attend_kernel, first=first, last=last, pieces=1 if last else pieces, lift=lift),
        out_shape=shape,
        in_specs=[VMEM] * len(operands),
        out_specs=[VMEM] * len(shape),
        input_output_aliases=alias,
        scratch_shapes=[pltpu.VMEM((keys, HD), BF), pltpu.VMEM((keys, HD), BF)],
        compiler_params=pltpu.CompilerParams(vmem_limit_bytes=32 * 2**20),
        cost_estimate=pl.CostEstimate(
            flops=rows * keys * 4 * HD, transcendentals=rows * keys, bytes_accessed=2 * 2**20
        ),
        name="attend_last" if last else ("attend_first" if first else "attend_more"),
    )(*[near(v) for v in operands])


def finish_kernel(got, w0, w1, w2, w3, w4, w5, w6, w7, lat, mod, out, att, held, arrived):
    copies = [
        pltpu.make_async_copy(ref, held.at[j], arrived.at[j])
        for j, ref in enumerate((w0, w1, w2, w3, w4, w5, w6, w7))
    ]
    for copy in copies:
        copy.start()
    core = lax.axis_index("c")
    width = lat.shape[1]
    for j in range(8):
        side, piece = j // 4, j % 4
        owner = core if side == 0 else 1 - core
        ahead = 1 - 2 * owner
        tp = tp_of((0, -ahead, ahead, 2)[piece], owner)
        lse = []
        for x in range(4):
            tail = got[x * 8 + tp, GRID_W:, :HD].astype(F32)
            lse.append(tail[0:1] + tail[1:2] + tail[2:3])
        top = jnp.maximum(jnp.maximum(lse[0], lse[1]), jnp.maximum(lse[2], lse[3]))
        share = [jnp.exp2(v - top) for v in lse]
        inv = 1.0 / (share[0] + share[1] + share[2] + share[3])
        total = None
        for x in range(4):
            w = jnp.broadcast_to(share[x] * inv, (HD, HD)).T
            w = jnp.concatenate([w[:GRID_W], w[GRID_W:]], axis=1)
            term = got[x * 8 + tp, :GRID_W, :].astype(F32) * w
            total = term if total is None else total + term
        att[:, j * 256 : (j + 1) * 256] = total.astype(BF)
    mixed = None
    for j, copy in enumerate(copies):
        copy.wait()
        part = jnp.dot(att[:, j * 256 : (j + 1) * 256], held[j], preferred_element_type=F32)
        mixed = part if mixed is None else mixed + part
    gate = columns_of(mod, 0, 2 * width, 3 * width)
    out[...] = (lat[...].astype(F32) + gate * rms(mixed)).astype(BF)


def body(
    latents, context, cond, ctx_cond, mod_weight, query_weight, key_matrix, value_matrix, out_weight,
    query_gain, key_gain,
):
    def over_four(v, axis):
        return [
            v,
            lax.ppermute(v, axis, shift(4, 1)),
            lax.ppermute(v, axis, shift(4, -1)),
            lax.ppermute(v, axis, shift(4, 2)),
        ]

    def swap(v):
        return lax.ppermute(v, "c", [(0, 1), (1, 0)])

    ahead = [(2 * i + c, 2 * ((i + 1 - 2 * c) % 4) + c) for i in range(4) for c in range(2)]
    behind = [(b, a) for a, b in ahead]

    mine = over_four(latents, "y")
    partial = jnp.dot(
        jax.nn.silu(jnp.stack([cond, ctx_cond])), mod_weight, precision=lax.Precision.HIGHEST
    )
    shares = lax.all_to_all(jnp.broadcast_to(partial[None], (32,) + partial.shape), SP, 0, 0)
    theirs = [swap(v) for v in mine]
    summed = jnp.sum(shares, axis=0)
    modulation = lax.all_to_all(jnp.broadcast_to(summed[None], (8,) + summed.shape), TP, 0, 0)
    count = 16384
    tables = [jnp.asarray(t) for t in rope_tables(count)]
    loaded = [
        latents, query_weight, key_matrix, value_matrix, context, query_gain[None], key_gain[None], *tables,
    ]
    q, kv = pl.pallas_call(
        project_kernel,
        out_shape=[pltpu.VMEM((2, 512, HD), BF), pltpu.VMEM((528, 2 * HD), BF)],
        in_specs=[VMEM] * 8 + [pl.BlockSpec(memory_space=pltpu.HBM)] * len(loaded),
        out_specs=[VMEM] * 2,
        scratch_shapes=[pltpu.VMEM((256, 2048), BF)]
        + [pltpu.VMEM(v.shape, v.dtype) for v in loaded]
        + [pltpu.SemaphoreType.DMA((len(loaded),))],
        compiler_params=pltpu.CompilerParams(vmem_limit_bytes=32 * 2**20),
        cost_estimate=pl.CostEstimate(flops=2 * 528 * 2048 * 512, transcendentals=0, bytes_accessed=4 * 2**20),
        name="project",
    )(
        *[near(v) for v in mine[1:] + theirs],
        near(modulation),
        *[pltpu.with_memory_space_constraint(v, pltpu.HBM) for v in loaded],
    )
    lift = math.log(count / (2.0 * 512))
    kv, late_weight = lax.optimization_barrier((kv, out_weight))
    up, down = [kv], [kv]
    up.append(lax.ppermute(kv, "z", shift(8, 1)))
    down.append(lax.ppermute(kv, "z", shift(8, -1)))
    q_parts = over_four(q, "x")
    for _ in range(2):
        up.append(lax.ppermute(up[-1], "z", shift(8, 1)))
        down.append(lax.ppermute(down[-1], "z", shift(8, -1)))
    k_last = lax.ppermute(up[3][:, :HD], "z", shift(8, 1))
    v_last = lax.ppermute(down[3][:, HD:], "z", shift(8, -1))
    first = lax.ppermute(late_weight, TP, ahead)
    second = lax.ppermute(late_weight, TP, behind)
    weights = [out_weight, first, second, lax.ppermute(first, TP, ahead)]
    weights += [swap(late_weight), swap(first), swap(second)]
    weights.append(swap(weights[3]))

    q_all, *state = attend(True, False, 1, lift, [*q_parts, kv])
    for t in range(1, 4):
        state = attend(False, False, 2, lift, [q_all, *state, up[t], down[t]])
    tails = [kv] + up[1:] + down[1:]
    (sent,) = attend(False, True, 1, lift, [q_all, *state, k_last, v_last, *tails])
    got = lax.all_to_all(sent, ("x", "y", "c"), 0, 0)
    return pl.pallas_call(
        finish_kernel,
        out_shape=jax.ShapeDtypeStruct(latents.shape, BF),
        in_specs=[VMEM] + [pl.BlockSpec(memory_space=pltpu.HBM)] * 8 + [VMEM] * 2,
        out_specs=VMEM,
        scratch_shapes=[
            pltpu.VMEM(latents.shape, BF),
            pltpu.VMEM((8,) + out_weight.shape, BF),
            pltpu.SemaphoreType.DMA((8,)),
        ],
        compiler_params=pltpu.CompilerParams(vmem_limit_bytes=32 * 2**20),
        cost_estimate=pl.CostEstimate(flops=2 * 64 * 2048 * 2048, transcendentals=0, bytes_accessed=10 * 2**20),
        name="finish",
    )(
        near(got),
        *[pltpu.with_memory_space_constraint(v, pltpu.HBM) for v in weights],
        near(latents),
        near(modulation),
    )


def solution(mesh):
    torus = Mesh(mesh.devices.reshape(8, 4, 4, 2), ALL)
    placed = (
        P(ALL, None), P(SP, None), P(SP), P(SP), P(SP, TP), P(None, TP), P(None, TP), P(None, TP),
        P(TP, None), P(), P(),
    )

    return jax.shard_map(body, mesh=torus, in_specs=placed, out_specs=P(ALL, None), check_vma=False)
```

profile of v0, /device:TPU:1, one launch (start us, length us, event | category | flops | bytes accessed | tf_op | source)
XLA Modules:
  0.0 137.5 jit_solution(2275939608088523033)
XLA Ops:
  0.0 2.1 %collective-permute-start = (bf16[64,2048]{1,0:T(8,128)(2,1)}, bf16[64,2048]{1,0:T(8,128)(2,1)S(1)}, u32[]{:S(2)}, u32[]{:S(2)}) collective-permute-start(bf16[64,2048]{1,0:T(8,128)(2,1)} %lat.1), channel_id=1, source_target_pairs={{0,2},{2,4},{4,6},{6,0},{1,3},{3,5},{5,7},{7,1},{8,10},{10,12},{12... | collective-permute-start | bytes 786440 | tf_op jit(solution)/shard_map/ppermute | solution.py:306
  2.1 1.5 %collective-permute-start.1 = (bf16[64,2048]{1,0:T(8,128)(2,1)}, bf16[64,2048]{1,0:T(8,128)(2,1)S(1)}, u32[]{:S(2)}, u32[]{:S(2)}) collective-permute-start(bf16[64,2048]{1,0:T(8,128)(2,1)} %lat.1), channel_id=1, source_target_pairs={{0,6},{2,0},{4,2},{6,4},{1,7},{3,1},{5,3},{7,5},{8,14},{10,8},{12,... | collective-permute-start | bytes 786440 | tf_op jit(solution)/shard_map/ppermute | solution.py:307
  3.6 1.6 %collective-permute-start.2 = (bf16[64,2048]{1,0:T(8,128)(2,1)}, bf16[64,2048]{1,0:T(8,128)(2,1)S(1)}, u32[]{:S(2)}, u32[]{:S(2)}) collective-permute-start(bf16[64,2048]{1,0:T(8,128)(2,1)} %lat.1), channel_id=1, source_target_pairs={{0,4},{2,6},{4,0},{6,2},{1,5},{3,7},{5,1},{7,3},{8,12},{10,14},{12... | collective-permute-start | bytes 786440 | tf_op jit(solution)/shard_map/ppermute | solution.py:308
  5.2 0.9 fusion
  6.1 0.7 broadcast_in_dim.8
  6.8 11.0 %all-to-all-start = ((f32[32,2,768]{2,1,0:T(2,128)}), f32[32,2,768]{2,1,0:T(2,128)S(1)}, u32[]{:S(2)}, u32[]{:S(2)}) async-start(f32[32,2,768]{2,1,0:T(2,128)} %broadcast_in_dim.8), calls=%async_computation | async-start | bytes 393216 | tf_op jit(solution)/shard_map/all_to_all | solution.py:321
  17.9 1.9 %collective-permute-start.3 = (bf16[64,2048]{1,0:T(8,128)(2,1)}, bf16[64,2048]{1,0:T(8,128)(2,1)S(1)}, u32[]{:S(2)}, u32[]{:S(2)}) collective-permute-start(bf16[64,2048]{1,0:T(8,128)(2,1)} %lat.1), channel_id=1, source_target_pairs={{0,1},{1,0},{2,3},{3,2},{4,5},{5,4},{6,7},{7,6},{8,9},{9,8},{10,11... | collective-permute-start | bytes 786440 | tf_op jit(solution)/shard_map/ppermute | solution.py:312
  20.4 7.4 %all-to-all-done = f32[32,2,768]{2,1,0:T(2,128)S(1)} async-done(((f32[32,2,768]{2,1,0:T(2,128)}), f32[32,2,768]{2,1,0:T(2,128)S(1)}, u32[]{:S(2)}, u32[]{:S(2)}) %all-to-all-start) | async-done | bytes 196640 | tf_op jit(solution)/shard_map/all_to_all | solution.py:321
  28.5 6.4 %all-to-all-start.1 = ((f32[8,2,768]{2,1,0:T(2,128)}), f32[8,2,768]{2,1,0:T(2,128)S(1)}, u32[]{:S(2)}, u32[]{:S(2)}) async-start(f32[8,2,768]{2,1,0:T(2,128)} %broadcast_in_dim.9), calls=%async_computation.1 | async-start | bytes 98304 | tf_op jit(solution)/shard_map/all_to_all | solution.py:324
  34.9 4.8 %all-to-all-done.1.refs_7_.mod = f32[8,2,768]{2,1,0:T(2,128)S(1)} async-done(((f32[8,2,768]{2,1,0:T(2,128)}), f32[8,2,768]{2,1,0:T(2,128)S(1)}, u32[]{:S(2)}, u32[]{:S(2)}) %all-to-all-start.1) | async-done | bytes 49184 | tf_op jit(solution)/shard_map/all_to_all | solution.py:324
  39.7 4.2 %project.1 = (bf16[2,512,128]{2,1,0:T(8,128)(2,1)S(1)}, bf16[528,256]{1,0:T(8,128)(2,1)S(1)}) custom-call(bf16[64,2048]{1,0:T(8,128)(2,1)S(1)} %collective-permute-done.refs_0_, bf16[64,2048]{1,0:T(8,128)(2,1)S(1)} %collective-permute-done.1.refs_1_, bf16[64,2048]{1,0:T(8,128)(2,1)S(1)} %collective-permute-done.2.refs_2_, ...), custom_call_target="tpu_custom_call" | custom-call | flops 1107296256 | bytes 4194304 | tf_op jit(solution)/shard_map/project/pallas_call | solution.py:330
  43.9 1.0 collective-permute-start.18
  45.6 2.0 %collective-permute-start.11 = (bf16[528,256]{1,0:T(8,128)(2,1)S(1)}, bf16[528,256]{1,0:T(8,128)(2,1)S(1)}, u32[]{:S(2)}, u32[]{:S(2)}) collective-permute-start(bf16[528,256]{1,0:T(8,128)(2,1)S(1)} %get-tuple-element.24.refs_4_.refs_6_), channel_id=1, source_target_pairs={{0,224},{32,0},{64,32},{96,64},{128,96},{160,128},{192,160},{224,1... | collective-permute-start | bytes 811016 | tf_op jit(solution)/shard_map/ppermute | solution.py:350
  47.6 2.7 %collective-permute-start.8 = (bf16[2,512,128]{2,1,0:T(8,128)(2,1)S(1)}, bf16[2,512,128]{2,1,0:T(8,128)(2,1)S(1)}, u32[]{:S(2)}, u32[]{:S(2)}) collective-permute-start(bf16[2,512,128]{2,1,0:T(8,128)(2,1)S(1)} %get-tuple-element.22.refs_0_), channel_id=1, source_target_pairs={{0,24},{8,0},{16,8},{24,16},{1,25},{9,1},{17,9},{25,17},{2,26},{10... | collective-permute-start | bytes 786440 | tf_op jit(solution)/shard_map/ppermute | solution.py:307
  50.2 3.4 %collective-permute-done.7.refs_1_ = bf16[2,512,128]{2,1,0:T(8,128)(2,1)S(1)} collective-permute-done((bf16[2,512,128]{2,1,0:T(8,128)(2,1)S(1)}, bf16[2,512,128]{2,1,0:T(8,128)(2,1)S(1)}, u32[]{:S(2)}, u32[]{:S(2)}) %collective-permute-start.7) | collective-permute-done | bytes 262176 | tf_op jit(solution)/shard_map/ppermute | solution.py:306
  54.0 2.4 %collective-permute-start.13 = (bf16[528,256]{1,0:T(8,128)(2,1)S(1)}, bf16[528,256]{1,0:T(8,128)(2,1)S(1)}, u32[]{:S(2)}, u32[]{:S(2)}) collective-permute-start(bf16[528,256]{1,0:T(8,128)(2,1)S(1)} %collective-permute-done.11.refs_5_.refs_10_), channel_id=1, source_target_pairs={{0,224},{32,0},{64,32},{96,64},{128,96},{160,128},{192,160},{224,1... | collective-permute-start | bytes 811016 | tf_op jit(solution)/shard_map/ppermute | solution.py:354
  56.5 0.9 collective-permute-start.19
  58.1 2.0 %collective-permute-start.20 = (bf16[256,2048]{1,0:T(8,128)(2,1)}, bf16[256,2048]{1,0:T(8,128)(2,1)}, u32[]{:S(2)}, u32[]{:S(2)}) collective-permute-start(bf16[256,2048]{1,0:T(8,128)(2,1)} %collective-permute-done.18.w1), channel_id=1, source_target_pairs={{0,2},{1,7},{2,4},{3,1},{4,6},{5,3},{6,0},{7,5},{8,10},{9,15},{10,... | collective-permute-start | bytes 3145736 | tf_op jit(solution)/shard_map/ppermute | solution.py:359
  60.0 1.7 %collective-permute-done.9.refs_3_ = bf16[2,512,128]{2,1,0:T(8,128)(2,1)S(1)} collective-permute-done((bf16[2,512,128]{2,1,0:T(8,128)(2,1)S(1)}, bf16[2,512,128]{2,1,0:T(8,128)(2,1)S(1)}, u32[]{:S(2)}, u32[]{:S(2)}) %collective-permute-start.9) | collective-permute-done | bytes 262176 | tf_op jit(solution)/shard_map/ppermute | solution.py:308
  61.8 4.4 %attend_first.1 = (bf16[4096,128]{1,0:T(8,128)(2,1)S(1)}, f32[4096,128]{1,0:T(8,128)S(1)}, f32[4096,128]{1,0:T(8,128)S(1)}, f32[4096,128]{1,0:T(8,128)S(1)}) custom-call(bf16[2,512,128]{2,1,0:T(8,128)(2,1)S(1)} %get-tuple-element.22.refs_0_, bf16[2,512,128]{2,1,0:T(8,128)(2,1)S(1)} %collective-permute-done.7.refs_1_, ...), custom_call_target="tpu_custom_call" | custom-call | flops 1073741824 | bytes 2097152 | tf_op jit(solution)/shard_map/attend_first/pallas_call | solution.py:247
  66.7 2.3 %collective-permute-start.15 = (bf16[528,256]{1,0:T(8,128)(2,1)S(1)}, bf16[528,256]{1,0:T(8,128)(2,1)S(1)}, u32[]{:S(2)}, u32[]{:S(2)}) collective-permute-start(bf16[528,256]{1,0:T(8,128)(2,1)S(1)} %collective-permute-done.13.refs_5_.refs_11_), channel_id=1, source_target_pairs={{0,224},{32,0},{64,32},{96,64},{128,96},{160,128},{192,160},{224,1... | collective-permute-start | bytes 811016 | tf_op jit(solution)/shard_map/ppermute | solution.py:354
  69.0 7.4 %attend_more.3 = (f32[4096,128]{1,0:T(8,128)S(1)}, f32[4096,128]{1,0:T(8,128)S(1)}, f32[4096,128]{1,0:T(8,128)S(1)}) custom-call(bf16[4096,128]{1,0:T(8,128)(2,1)S(1)} %get-tuple-element.25.refs_0_, f32[4096,128]{1,0:T(8,128)S(1)} %get-tuple-element.26.refs_1_, ...), custom_call_target="tpu_custom_call", output_to_operand_aliasing={{0}: (1, {}), {1}: (2, {}), {2}: (3, {})} | custom-call | flops 2147483648 | bytes 2097152 | tf_op jit(solution)/shard_map/attend_more/pallas_call | solution.py:247
  76.4 7.4 %attend_more.4 = (f32[4096,128]{1,0:T(8,128)S(1)}, f32[4096,128]{1,0:T(8,128)S(1)}, f32[4096,128]{1,0:T(8,128)S(1)}) custom-call(bf16[4096,128]{1,0:T(8,128)(2,1)S(1)} %get-tuple-element.25.refs_0_, f32[4096,128]{1,0:T(8,128)S(1)} %get-tuple-element.29.refs_1_, ...), custom_call_target="tpu_custom_call", output_to_operand_aliasing={{0}: (1, {}), {1}: (2, {}), {2}: (3, {})} | custom-call | flops 2147483648 | bytes 2097152 | tf_op jit(solution)/shard_map/attend_more/pallas_call | solution.py:247
  83.9 2.9 %collective-permute-start.17 = (bf16[528,128]{1,0:T(8,128)(2,1)S(1)}, bf16[528,128]{1,0:T(8,128)(2,1)S(1)}, u32[]{:S(2)}, u32[]{:S(2)}) collective-permute-start(bf16[528,128]{1,0:T(8,128)(2,1)S(1)} %slice.9), channel_id=1, source_target_pairs={{0,224},{32,0},{64,32},{96,64},{128,96},{160,128},{192,160},{224,1... | collective-permute-start | bytes 405512 | tf_op jit(solution)/shard_map/ppermute | solution.py:356
  86.9 7.4 %attend_more.5 = (f32[4096,128]{1,0:T(8,128)S(1)}, f32[4096,128]{1,0:T(8,128)S(1)}, f32[4096,128]{1,0:T(8,128)S(1)}) custom-call(bf16[4096,128]{1,0:T(8,128)(2,1)S(1)} %get-tuple-element.25.refs_0_, f32[4096,128]{1,0:T(8,128)S(1)} %get-tuple-element.32.refs_1_, ...), custom_call_target="tpu_custom_call", output_to_operand_aliasing={{0}: (1, {}), {1}: (2, {}), {2}: (3, {})} | custom-call | flops 2147483648 | bytes 2097152 | tf_op jit(solution)/shard_map/attend_more/pallas_call | solution.py:247
  94.3 7.9 %attend_last.1 = bf16[32,80,256]{2,1,0:T(8,128)(2,1)} custom-call(bf16[4096,128]{1,0:T(8,128)(2,1)S(1)} %get-tuple-element.25.refs_0_, f32[4096,128]{1,0:T(8,128)S(1)} %get-tuple-element.35.refs_1_, f32[4096,128]{1,0:T(8,128)S(1)} %get-tuple-element.36.refs_2_, f32[4096,128]{1,0:T(8,128)S(1)} %get-tuple-element.37.refs_3_, ...), custom_call_target="tpu_custom_call" | custom-call | flops 1342177280 | bytes 2097152 | tf_op jit(solution)/shard_map/attend_last/pallas_call | solution.py:247
  102.3 10.1 %all-to-all-start.2 = ((bf16[32,80,256]{2,1,0:T(8,128)(2,1)}), bf16[32,80,256]{2,1,0:T(8,128)(2,1)S(1)}, u32[]{:S(2)}, u32[]{:S(2)}) async-start(bf16[32,80,256]{2,1,0:T(8,128)(2,1)} %attend_last.1), calls=%async_computation.2 | async-start | bytes 2621440 | tf_op jit(solution)/shard_map/all_to_all | solution.py:368
  113.5 1.6 %collective-permute-done.21.w4 = bf16[256,2048]{1,0:T(8,128)(2,1)S(1)} collective-permute-done((bf16[256,2048]{1,0:T(8,128)(2,1)S(1)}, bf16[256,2048]{1,0:T(8,128)(2,1)S(1)}, u32[]{:S(2)}, u32[]{:S(2)}) %collective-permute-start.21) | collective-permute-done | bytes 1048608 | tf_op jit(solution)/shard_map/ppermute | solution.py:312
  115.2 1.5 %collective-permute-done.22.w5 = bf16[256,2048]{1,0:T(8,128)(2,1)S(1)} collective-permute-done((bf16[256,2048]{1,0:T(8,128)(2,1)}, bf16[256,2048]{1,0:T(8,128)(2,1)S(1)}, u32[]{:S(2)}, u32[]{:S(2)}) %collective-permute-start.22) | collective-permute-done | bytes 1048608 | tf_op jit(solution)/shard_map/ppermute | solution.py:312
  116.7 1.0 copy-done.4
  118.3 13.9 %all-to-all-done.2.got = bf16[32,80,256]{2,1,0:T(8,128)(2,1)S(1)} async-done(((bf16[32,80,256]{2,1,0:T(8,128)(2,1)}), bf16[32,80,256]{2,1,0:T(8,128)(2,1)S(1)}, u32[]{:S(2)}, u32[]{:S(2)}) %all-to-all-start.2) | async-done | bytes 1310752 | tf_op jit(solution)/shard_map/all_to_all | solution.py:368
  132.2 5.1 %finish.1 = bf16[64,2048]{1,0:T(8,128)(2,1)} custom-call(bf16[32,80,256]{2,1,0:T(8,128)(2,1)S(1)} %all-to-all-done.2.got, bf16[256,2048]{1,0:T(8,128)(2,1)} %w0.1, bf16[256,2048]{1,0:T(8,128)(2,1)} %collective-permute-done.18.w1, bf16[256,2048]{1,0:T(8,128)(2,1)} %collective-permute-done.19.w2, bf16[256,2048]{1,0:T(8,128)(2,1)} %collective-permute-done.20.w3, ...), custom_call_target="tpu_custom_call" | custom-call | flops 536870912 | bytes 10485760 | tf_op jit(solution)/shard_map/finish/pallas_call | solution.py:369
  (47 shorter events, 5.5 us)
Async XLA Ops:
  0.0 5.2 %copy-start = (f32[64,768]{1,0:T(8,128)S(1)}, f32[64,768]{1,0:T(8,128)}, u32[]{:S(2)}) copy-start(f32[64,768]{1,0:T(8,128)} %param.19) | copy-start | bytes 589828
  0.0 19.8 %collective-permute-start = (bf16[64,2048]{1,0:T(8,128)(2,1)}, bf16[64,2048]{1,0:T(8,128)(2,1)S(1)}, u32[]{:S(2)}, u32[]{:S(2)}) collective-permute-start(bf16[64,2048]{1,0:T(8,128)(2,1)} %lat.1), channel_id=1, source_target_pairs={{0,2},{2,4},{4,6},{6,0},{1,3},{3,5},{5,7},{7,1},{8,10},{10,12},{12... | collective-permute-start | bytes 786440 | tf_op jit(solution)/shard_map/ppermute | solution.py:306
  2.1 17.8 %collective-permute-start.1 = (bf16[64,2048]{1,0:T(8,128)(2,1)}, bf16[64,2048]{1,0:T(8,128)(2,1)S(1)}, u32[]{:S(2)}, u32[]{:S(2)}) collective-permute-start(bf16[64,2048]{1,0:T(8,128)(2,1)} %lat.1), channel_id=1, source_target_pairs={{0,6},{2,0},{4,2},{6,4},{1,7},{3,1},{5,3},{7,5},{8,14},{10,8},{12,... | collective-permute-start | bytes 786440 | tf_op jit(solution)/shard_map/ppermute | solution.py:307
  3.6 16.6 %collective-permute-start.2 = (bf16[64,2048]{1,0:T(8,128)(2,1)}, bf16[64,2048]{1,0:T(8,128)(2,1)S(1)}, u32[]{:S(2)}, u32[]{:S(2)}) collective-permute-start(bf16[64,2048]{1,0:T(8,128)(2,1)} %lat.1), channel_id=1, source_target_pairs={{0,4},{2,6},{4,0},{6,2},{1,5},{3,7},{5,1},{7,3},{8,12},{10,14},{12... | collective-permute-start | bytes 786440 | tf_op jit(solution)/shard_map/ppermute | solution.py:308
  6.8 20.9 %all-to-all-start = ((f32[32,2,768]{2,1,0:T(2,128)}), f32[32,2,768]{2,1,0:T(2,128)S(1)}, u32[]{:S(2)}, u32[]{:S(2)}) async-start(f32[32,2,768]{2,1,0:T(2,128)} %broadcast_in_dim.8), calls=%async_computation | async-start | bytes 393216 | tf_op jit(solution)/shard_map/all_to_all | solution.py:321
  17.9 17.0 %collective-permute-start.3 = (bf16[64,2048]{1,0:T(8,128)(2,1)}, bf16[64,2048]{1,0:T(8,128)(2,1)S(1)}, u32[]{:S(2)}, u32[]{:S(2)}) collective-permute-start(bf16[64,2048]{1,0:T(8,128)(2,1)} %lat.1), channel_id=1, source_target_pairs={{0,1},{1,0},{2,3},{3,2},{4,5},{5,4},{6,7},{7,6},{8,9},{9,8},{10,11... | collective-permute-start | bytes 786440 | tf_op jit(solution)/shard_map/ppermute | solution.py:312
  19.8 19.9 %collective-permute-start.4 = (bf16[64,2048]{1,0:T(8,128)(2,1)S(1)}, bf16[64,2048]{1,0:T(8,128)(2,1)S(1)}, u32[]{:S(2)}, u32[]{:S(2)}) collective-permute-start(bf16[64,2048]{1,0:T(8,128)(2,1)S(1)} %collective-permute-done.refs_0_), channel_id=1, source_target_pairs={{0,1},{1,0},{2,3},{3,2},{4,5},{5,4},{6,7},{7,6},{8,9},{9,8},{10,11... | collective-permute-start | bytes 786440 | tf_op jit(solution)/shard_map/ppermute | solution.py:312
  19.9 19.8 %collective-permute-start.5 = (bf16[64,2048]{1,0:T(8,128)(2,1)S(1)}, bf16[64,2048]{1,0:T(8,128)(2,1)S(1)}, u32[]{:S(2)}, u32[]{:S(2)}) collective-permute-start(bf16[64,2048]{1,0:T(8,128)(2,1)S(1)} %collective-permute-done.1.refs_1_), channel_id=1, source_target_pairs={{0,1},{1,0},{2,3},{3,2},{4,5},{5,4},{6,7},{7,6},{8,9},{9,8},{10,11... | collective-permute-start | bytes 786440 | tf_op jit(solution)/shard_map/ppermute | solution.py:312
  20.3 19.4 %collective-permute-start.6 = (bf16[64,2048]{1,0:T(8,128)(2,1)S(1)}, bf16[64,2048]{1,0:T(8,128)(2,1)S(1)}, u32[]{:S(2)}, u32[]{:S(2)}) collective-permute-start(bf16[64,2048]{1,0:T(8,128)(2,1)S(1)} %collective-permute-done.2.refs_2_), channel_id=1, source_target_pairs={{0,1},{1,0},{2,3},{3,2},{4,5},{5,4},{6,7},{7,6},{8,9},{9,8},{10,11... | collective-permute-start | bytes 786440 | tf_op jit(solution)/shard_map/ppermute | solution.py:312
  28.5 11.2 %all-to-all-start.1 = ((f32[8,2,768]{2,1,0:T(2,128)}), f32[8,2,768]{2,1,0:T(2,128)S(1)}, u32[]{:S(2)}, u32[]{:S(2)}) async-start(f32[8,2,768]{2,1,0:T(2,128)} %broadcast_in_dim.9), calls=%async_computation.1 | async-start | bytes 98304 | tf_op jit(solution)/shard_map/all_to_all | solution.py:324
  39.7 4.2 %copy-start.2 = (bf16[256,2048]{1,0:T(8,128)(2,1)S(1)}, bf16[256,2048]{1,0:T(8,128)(2,1)}, u32[]{:S(2)}) copy-start(bf16[256,2048]{1,0:T(8,128)(2,1)} %w0.1) | copy-start | bytes 3145732
  43.9 14.1 %collective-permute-start.18 = (bf16[256,2048]{1,0:T(8,128)(2,1)S(1)}, bf16[256,2048]{1,0:T(8,128)(2,1)}, u32[]{:S(2)}, u32[]{:S(2)}) collective-permute-start(bf16[256,2048]{1,0:T(8,128)(2,1)S(1)} %copy-done.2), channel_id=1, source_target_pairs={{0,2},{1,7},{2,4},{3,1},{4,6},{5,3},{6,0},{7,5},{8,10},{9,15},{10,... | collective-permute-start | bytes 3145736 | tf_op jit(solution)/shard_map/ppermute | solution.py:357
  44.9 8.7 %collective-permute-start.7 = (bf16[2,512,128]{2,1,0:T(8,128)(2,1)S(1)}, bf16[2,512,128]{2,1,0:T(8,128)(2,1)S(1)}, u32[]{:S(2)}, u32[]{:S(2)}) collective-permute-start(bf16[2,512,128]{2,1,0:T(8,128)(2,1)S(1)} %get-tuple-element.22.refs_0_), channel_id=1, source_target_pairs={{0,8},{8,16},{16,24},{24,0},{1,9},{9,17},{17,25},{25,1},{2,10},{10... | collective-permute-start | bytes 786440 | tf_op jit(solution)/shard_map/ppermute | solution.py:306
  44.9 8.9 %collective-permute-start.10 = (bf16[528,256]{1,0:T(8,128)(2,1)S(1)}, bf16[528,256]{1,0:T(8,128)(2,1)S(1)}, u32[]{:S(2)}, u32[]{:S(2)}) collective-permute-start(bf16[528,256]{1,0:T(8,128)(2,1)S(1)} %get-tuple-element.24.refs_4_.refs_6_), channel_id=1, source_target_pairs={{0,32},{32,64},{64,96},{96,128},{128,160},{160,192},{192,224},{224... | collective-permute-start | bytes 811016 | tf_op jit(solution)/shard_map/ppermute | solution.py:349
  45.6 8.4 %collective-permute-start.11 = (bf16[528,256]{1,0:T(8,128)(2,1)S(1)}, bf16[528,256]{1,0:T(8,128)(2,1)S(1)}, u32[]{:S(2)}, u32[]{:S(2)}) collective-permute-start(bf16[528,256]{1,0:T(8,128)(2,1)S(1)} %get-tuple-element.24.refs_4_.refs_6_), channel_id=1, source_target_pairs={{0,224},{32,0},{64,32},{96,64},{128,96},{160,128},{192,160},{224,1... | collective-permute-start | bytes 811016 | tf_op jit(solution)/shard_map/ppermute | solution.py:350
  47.6 8.9 %collective-permute-start.8 = (bf16[2,512,128]{2,1,0:T(8,128)(2,1)S(1)}, bf16[2,512,128]{2,1,0:T(8,128)(2,1)S(1)}, u32[]{:S(2)}, u32[]{:S(2)}) collective-permute-start(bf16[2,512,128]{2,1,0:T(8,128)(2,1)S(1)} %get-tuple-element.22.refs_0_), channel_id=1, source_target_pairs={{0,24},{8,0},{16,8},{24,16},{1,25},{9,1},{17,9},{25,17},{2,26},{10... | collective-permute-start | bytes 786440 | tf_op jit(solution)/shard_map/ppermute | solution.py:307
  53.6 8.2 %collective-permute-start.9 = (bf16[2,512,128]{2,1,0:T(8,128)(2,1)S(1)}, bf16[2,512,128]{2,1,0:T(8,128)(2,1)S(1)}, u32[]{:S(2)}, u32[]{:S(2)}) collective-permute-start(bf16[2,512,128]{2,1,0:T(8,128)(2,1)S(1)} %get-tuple-element.22.refs_0_), channel_id=1, source_target_pairs={{0,16},{8,24},{16,0},{24,8},{1,17},{9,25},{17,1},{25,9},{2,18},{10... | collective-permute-start | bytes 786440 | tf_op jit(solution)/shard_map/ppermute | solution.py:308
  53.8 12.4 %collective-permute-start.12 = (bf16[528,256]{1,0:T(8,128)(2,1)S(1)}, bf16[528,256]{1,0:T(8,128)(2,1)S(1)}, u32[]{:S(2)}, u32[]{:S(2)}) collective-permute-start(bf16[528,256]{1,0:T(8,128)(2,1)S(1)} %collective-permute-done.10.refs_4_.refs_7_), channel_id=1, source_target_pairs={{0,32},{32,64},{64,96},{96,128},{128,160},{160,192},{192,224},{224... | collective-permute-start | bytes 811016 | tf_op jit(solution)/shard_map/ppermute | solution.py:353
  54.0 12.7 %collective-permute-start.13 = (bf16[528,256]{1,0:T(8,128)(2,1)S(1)}, bf16[528,256]{1,0:T(8,128)(2,1)S(1)}, u32[]{:S(2)}, u32[]{:S(2)}) collective-permute-start(bf16[528,256]{1,0:T(8,128)(2,1)S(1)} %collective-permute-done.11.refs_5_.refs_10_), channel_id=1, source_target_pairs={{0,224},{32,0},{64,32},{96,64},{128,96},{160,128},{192,160},{224,1... | collective-permute-start | bytes 811016 | tf_op jit(solution)/shard_map/ppermute | solution.py:354
  56.5 56.5 %collective-permute-start.19 = (bf16[256,2048]{1,0:T(8,128)(2,1)S(1)}, bf16[256,2048]{1,0:T(8,128)(2,1)}, u32[]{:S(2)}, u32[]{:S(2)}) collective-permute-start(bf16[256,2048]{1,0:T(8,128)(2,1)S(1)} %copy-done.2), channel_id=1, source_target_pairs={{2,0},{7,1},{4,2},{1,3},{6,4},{3,5},{0,6},{5,7},{10,8},{15,9},{12,... | collective-permute-start | bytes 3145736 | tf_op jit(solution)/shard_map/ppermute | solution.py:358
  58.1 55.2 %collective-permute-start.20 = (bf16[256,2048]{1,0:T(8,128)(2,1)}, bf16[256,2048]{1,0:T(8,128)(2,1)}, u32[]{:S(2)}, u32[]{:S(2)}) collective-permute-start(bf16[256,2048]{1,0:T(8,128)(2,1)} %collective-permute-done.18.w1), channel_id=1, source_target_pairs={{0,2},{1,7},{2,4},{3,1},{4,6},{5,3},{6,0},{7,5},{8,10},{9,15},{10,... | collective-permute-start | bytes 3145736 | tf_op jit(solution)/shard_map/ppermute | solution.py:359
  66.2 17.6 %collective-permute-start.14 = (bf16[528,256]{1,0:T(8,128)(2,1)S(1)}, bf16[528,256]{1,0:T(8,128)(2,1)S(1)}, u32[]{:S(2)}, u32[]{:S(2)}) collective-permute-start(bf16[528,256]{1,0:T(8,128)(2,1)S(1)} %collective-permute-done.12.refs_4_.refs_8_), channel_id=1, source_target_pairs={{0,32},{32,64},{64,96},{96,128},{128,160},{160,192},{192,224},{224... | collective-permute-start | bytes 811016 | tf_op jit(solution)/shard_map/ppermute | solution.py:353
  66.7 17.2 %collective-permute-start.15 = (bf16[528,256]{1,0:T(8,128)(2,1)S(1)}, bf16[528,256]{1,0:T(8,128)(2,1)S(1)}, u32[]{:S(2)}, u32[]{:S(2)}) collective-permute-start(bf16[528,256]{1,0:T(8,128)(2,1)S(1)} %collective-permute-done.13.refs_5_.refs_11_), channel_id=1, source_target_pairs={{0,224},{32,0},{64,32},{96,64},{128,96},{160,128},{192,160},{224,1... | collective-permute-start | bytes 811016 | tf_op jit(solution)/shard_map/ppermute | solution.py:354
  83.8 10.5 %collective-permute-start.16 = (bf16[528,128]{1,0:T(8,128)(2,1)S(1)}, bf16[528,128]{1,0:T(8,128)(2,1)S(1)}, u32[]{:S(2)}, u32[]{:S(2)}) collective-permute-start(bf16[528,128]{1,0:T(8,128)(2,1)S(1)} %slice.8), channel_id=1, source_target_pairs={{0,32},{32,64},{64,96},{96,128},{128,160},{160,192},{192,224},{224... | collective-permute-start | bytes 405512 | tf_op jit(solution)/shard_map/ppermute | solution.py:355
  83.9 10.4 %collective-permute-start.17 = (bf16[528,128]{1,0:T(8,128)(2,1)S(1)}, bf16[528,128]{1,0:T(8,128)(2,1)S(1)}, u32[]{:S(2)}, u32[]{:S(2)}) collective-permute-start(bf16[528,128]{1,0:T(8,128)(2,1)S(1)} %slice.9), channel_id=1, source_target_pairs={{0,224},{32,0},{64,32},{96,64},{128,96},{160,128},{192,160},{224,1... | collective-permute-start | bytes 405512 | tf_op jit(solution)/shard_map/ppermute | solution.py:356
  102.3 29.9 %copy-start.1 = (bf16[64,2048]{1,0:T(8,128)(2,1)S(1)}, bf16[64,2048]{1,0:T(8,128)(2,1)}, u32[]{:S(2)}) copy-start(bf16[64,2048]{1,0:T(8,128)(2,1)} %lat.1) | copy-start | bytes 786436
  102.3 29.9 %all-to-all-start.2 = ((bf16[32,80,256]{2,1,0:T(8,128)(2,1)}), bf16[32,80,256]{2,1,0:T(8,128)(2,1)S(1)}, u32[]{:S(2)}, u32[]{:S(2)}) async-start(bf16[32,80,256]{2,1,0:T(8,128)(2,1)} %attend_last.1), calls=%async_computation.2 | async-start | bytes 2621440 | tf_op jit(solution)/shard_map/all_to_all | solution.py:368
  112.4 2.7 %collective-permute-start.21 = (bf16[256,2048]{1,0:T(8,128)(2,1)S(1)}, bf16[256,2048]{1,0:T(8,128)(2,1)S(1)}, u32[]{:S(2)}, u32[]{:S(2)}) collective-permute-start(bf16[256,2048]{1,0:T(8,128)(2,1)S(1)} %copy-done.2), channel_id=1, source_target_pairs={{0,1},{1,0},{2,3},{3,2},{4,5},{5,4},{6,7},{7,6},{8,9},{9,8},{10,11... | collective-permute-start | bytes 3145736 | tf_op jit(solution)/shard_map/ppermute | solution.py:312
  112.7 3.9 %collective-permute-start.22 = (bf16[256,2048]{1,0:T(8,128)(2,1)}, bf16[256,2048]{1,0:T(8,128)(2,1)S(1)}, u32[]{:S(2)}, u32[]{:S(2)}) collective-permute-start(bf16[256,2048]{1,0:T(8,128)(2,1)} %collective-permute-done.18.w1), channel_id=1, source_target_pairs={{0,1},{1,0},{2,3},{3,2},{4,5},{5,4},{6,7},{7,6},{8,9},{9,8},{10,11... | collective-permute-start | bytes 3145736 | tf_op jit(solution)/shard_map/ppermute | solution.py:312
  113.0 5.3 %collective-permute-start.23 = (bf16[256,2048]{1,0:T(8,128)(2,1)}, bf16[256,2048]{1,0:T(8,128)(2,1)}, u32[]{:S(2)}, u32[]{:S(2)}) collective-permute-start(bf16[256,2048]{1,0:T(8,128)(2,1)} %collective-permute-done.19.w2), channel_id=1, source_target_pairs={{0,1},{1,0},{2,3},{3,2},{4,5},{5,4},{6,7},{7,6},{8,9},{9,8},{10,11... | collective-permute-start | bytes 3145736 | tf_op jit(solution)/shard_map/ppermute | solution.py:312
  113.2 19.0 %collective-permute-start.24 = (bf16[256,2048]{1,0:T(8,128)(2,1)}, bf16[256,2048]{1,0:T(8,128)(2,1)}, u32[]{:S(2)}, u32[]{:S(2)}) collective-permute-start(bf16[256,2048]{1,0:T(8,128)(2,1)} %collective-permute-done.20.w3), channel_id=1, source_target_pairs={{0,1},{1,0},{2,3},{3,2},{4,5},{5,4},{6,7},{7,6},{8,9},{9,8},{10,11... | collective-permute-start | bytes 3145736 | tf_op jit(solution)/shard_map/ppermute | solution.py:312
  115.2 1.5 %copy-start.3 = (bf16[256,2048]{1,0:T(8,128)(2,1)}, bf16[256,2048]{1,0:T(8,128)(2,1)S(1)}, u32[]{:S(2)}) copy-start(bf16[256,2048]{1,0:T(8,128)(2,1)S(1)} %collective-permute-done.21.w4) | copy-start | bytes 3145732
  (1 other events, 1.0 us)
where the time goes:
time: 138 us
  starting transfers between devices  54 us (39%)
  Pallas kernels  43.9 us (32%)
  waiting for transfers between devices  35.8 us (26%)
  local copies, waits for them, and re-layouts  2.41 us (2%)
    pallas_call x5, Pallas kernels, attend(): pl.pallas_call(functools.partial(attend_kernel, first=first, last=last, p...  34.6 us
    all_to_all x1, waiting for transfers between devices, body(): got = lax.all_to_all(sent, ('x', 'y', 'c'), 0, 0)  13.9 us
    all_to_all x1, starting transfers between devices, body(): lax.all_to_all(jnp.broadcast_to(partial[None], (32,) + partial.shape), SP...  11 us
    all_to_all x1, starting transfers between devices, body(): got = lax.all_to_all(sent, ('x', 'y', 'c'), 0, 0)  10.1 us
    all_to_all x1, waiting for transfers between devices, body(): lax.all_to_all(jnp.broadcast_to(partial[None], (32,) + partial.shape), SP...  7.36 us
    all_to_all x1, starting transfers between devices, body(): lax.all_to_all(jnp.broadcast_to(summed[None], (8,) + summed.shape), TP, 0...  6.4 us
    pallas_call x1, Pallas kernels, body(): pl.pallas_call(finish_kernel, out_shape=jax.ShapeDtypeStruct(latents.shap...  5.12 us
    all_to_all x1, waiting for transfers between devices, body(): lax.all_to_all(jnp.broadcast_to(summed[None], (8,) + summed.shape), TP, 0...  4.8 us
  transfers between devices with their start and end apart: 28, of which 10 were waited for; matrix products, arithmetic and copies ran while one was open for 2% of the time, Pallas kernels for 25%

commit v1 on v0

v1 whole, which is shorter than its diff:
```python
import functools
import math

import jax
import jax.numpy as jnp
import numpy as np
from jax import lax
from jax.experimental import pallas as pl
from jax.experimental.pallas import tpu as pltpu
from jax.sharding import Mesh
from jax.sharding import PartitionSpec as P

GRID_W = 64
SP = ("z", "x")
TP = ("y", "c")
ALL = ("z", "x", "y", "c")
NORM_EPS = 1e-06
ROPE_BASE = 10000.0
HD = 128
OFFS = (0, -1, 1, 2)

BF = jnp.bfloat16
F32 = jnp.float32


def shift(n, k):
    return [(i, (i + k) % n) for i in range(n)]


def rope_tables(count):
    quarter = HD // 4
    freq = ROPE_BASE ** (-np.arange(quarter, dtype=np.float64) / quarter)

    def table(positions, right):
        angle = np.asarray(positions, np.float64)[:, None] * freq[None, :]
        cos, sin = np.cos(angle), np.sin(angle)
        both = np.stack([np.concatenate([cos, cos], 1), np.concatenate([-sin, sin], 1)])
        blank = np.zeros_like(both)
        return np.concatenate([blank, both] if right else [both, blank], 2).astype(np.float32)

    rows = count // GRID_W
    return table(range(0, rows, 8), False), table(range(8), False), table(range(GRID_W), True)


def rms(v):
    return v * lax.rsqrt(jnp.mean(v * v, axis=-1, keepdims=True) + NORM_EPS)


def columns_of(mod, row, first, last):
    wide = mod.shape[2]
    found = []
    for piece in range(mod.shape[0]):
        lo, hi = max(first - piece * wide, 0), min(last - piece * wide, wide)
        if lo < hi:
            found.append(mod[piece, row : row + 1, lo:hi])
    return jnp.concatenate(found, axis=1)


def tp_of(offset, core):
    return lax.rem(lax.axis_index("y") + offset + 4, 4) * 2 + core


def project_kernel(*refs):
    blocks, mod, far = list(refs[:7]), refs[7], refs[8:18]
    q_out, kv_out, buf = refs[18:21]
    held, arrived = refs[21:31], refs[31]
    copies = [pltpu.make_async_copy(f, h, arrived.at[i]) for i, (f, h) in enumerate(zip(far, held))]
    for copy in copies:
        copy.start()
    lat, wq, wk, wv, ctx, qg, kg, eights, ones, cols = held
    blocks.insert(0, lat)
    width = ctx.shape[1]
    rows = GRID_W
    sp = lax.axis_index("z") * 4 + lax.axis_index("x")
    core = lax.axis_index("c")

    def modulate(v, r):
        scale = columns_of(mod, r, width, 2 * width)
        return (rms(v.astype(F32)) * (1.0 + scale) + columns_of(mod, r, 0, width)).astype(BF)

    def turn(v, cos, sin):
        lane = lax.broadcasted_iota(jnp.int32, v.shape, 1)
        other = jnp.where(lane % 64 < 32, pltpu.roll(v, HD - 32, 1), pltpu.roll(v, 32, 1))
        return v * cos + other * sin

    def dot(a, b):
        return jnp.dot(a, b, preferred_element_type=F32)

    for side in range(2):
        for j in (1, 2, 3, 0) if side == 0 else range(4):
            if side == 0 and j == 0:
                for copy in copies:
                    copy.wait()
            buf[j * rows : (j + 1) * rows] = modulate(blocks[side * 4 + j][...], 0)
        normed = buf[...]
        q = dot(normed, wq[...])
        k = dot(normed, wk[...])
        v = dot(normed, wv[...]).astype(BF)
        k = rms(k) * kg[...]
        q0 = rms(q[:, :HD]) * qg[...]
        q1 = rms(q[:, HD:]) * qg[...]
        for j in range(4):
            at = slice(j * rows, (j + 1) * rows)
            tp = tp_of(OFFS[j], core if side == 0 else 1 - core)
            c8, s8, c1, s1 = (t[i, pl.ds(p, 1), :] for t, p in ((eights, sp), (ones, tp)) for i in (0, 1))
            cos = c8 * c1 - s8 * s1 + cols[0]
            sin = s8 * c1 + c8 * s1 + cols[1]
            to = pl.ds(pl.multiple_of(tp * rows, rows), rows)
            q_out[0, to, :] = turn(q0[at], cos, sin).astype(BF)
            q_out[1, to, :] = turn(q1[at], cos, sin).astype(BF)
            kv_out[to, :HD] = turn(k[at], cos, sin).astype(BF)
            kv_out[to, HD:] = v[at]
    normed = modulate(ctx[...], 1)
    total = 8 * rows
    kv_out[total:, :HD] = (rms(dot(normed, wk[...])) * kg[...]).astype(BF)
    kv_out[total:, HD:] = dot(normed, wv[...]).astype(BF)


def scores_of(q, keys):
    return lax.dot_general(q, keys, (((1,), (1,)), ((), ())), preferred_element_type=F32)


def tree(values, op):
    while len(values) > 1:
        odd = values[len(values) // 2 * 2 :]
        values = [op(values[2 * i], values[2 * i + 1]) for i in range(len(values) // 2)] + odd
    return values[0]


SCALE = HD**-0.5
C2 = SCALE * math.log2(math.e)
CHUNK = 512


def fill(k_buf, v_buf, pieces):
    for i, r in enumerate(pieces):
        at = slice(i * CHUNK, (i + 1) * CHUNK)
        k_buf[at] = r[:CHUNK, :HD]
        v_buf[at] = r[:CHUNK, HD:]


def softmax_block(q, k_buf, v_buf, before, lift=None):
    s = scores_of(q, k_buf[...])
    tiles = [s[:, i * HD : (i + 1) * HD] for i in range(s.shape[1] // HD)]
    if lift is not None:
        tiles[-1] = tiles[-1] + lift / SCALE
    top = jnp.max(tree(tiles, jnp.maximum), axis=1, keepdims=True)
    if before is None:
        m_new = jnp.broadcast_to(top, (s.shape[0], HD))
    else:
        m_old, l_old, acc_old = before
        m_new = jnp.maximum(m_old, top)
    base = m_new * C2
    probs = [jnp.exp2(t * C2 - base) for t in tiles]
    p = jnp.concatenate([t.astype(BF) for t in probs], axis=1)
    pv = jnp.dot(p, v_buf[...], preferred_element_type=F32)
    sums = tree(probs, jnp.add)
    if before is None:
        return m_new, sums, pv
    alpha = jnp.exp2((m_old - m_new) * C2)
    return m_new, l_old * alpha + sums, acc_old * alpha + pv


def rows_at(b, size=CHUNK):
    return pl.ds(pl.multiple_of(b * size, size), size)


def own_kernel(q, kv, up, down, m, l, acc, k_buf, v_buf):
    fill(k_buf, v_buf, (kv, up, down))

    def step(b, carry):
        at, size = rows_at(b, CHUNK // 2), CHUNK // 2
        m[at], l[at], acc[at] = softmax_block(q[b // 2, rows_at(lax.rem(b, 2), size)], k_buf, v_buf, None)
        return carry

    lax.fori_loop(0, 4, step, 0)


def rest_kernel(q0, q1, q2, q3, m_own, l_own, acc_own, kv, up, down, q_all, m, l, acc, k_buf, v_buf):
    fill(k_buf, v_buf, (kv, up, down))
    for j, r in enumerate((q0, q1, q2, q3)):
        for h in range(2):
            q_all[(2 * j + h) * CHUNK : (2 * j + h + 1) * CHUNK] = r[h]
    for whole, own in ((m, m_own), (l, l_own), (acc, acc_own)):
        whole[: 2 * CHUNK] = own[...]

    def step(b, carry):
        at = rows_at(b)
        m[at], l[at], acc[at] = softmax_block(q_all[at], k_buf, v_buf, None)
        return carry

    lax.fori_loop(2, 8, step, 0)


def more_kernel(q_all, m_in, l_in, acc_in, up, down, m, l, acc, k_buf, v_buf):
    fill(k_buf, v_buf, (up, down))

    def step(b, carry):
        at = rows_at(b)
        m[at], l[at], acc[at] = softmax_block(q_all[at], k_buf, v_buf, (m_in[at], l_in[at], acc_in[at]))
        return carry

    lax.fori_loop(0, 8, step, 0)


def final_kernel(*refs, parts, lift, size):
    q_all, m_in, l_in, acc_in, up, down, k_far, v_far = refs[:8]
    tails = refs[8:15]
    outs, (k_buf, v_buf) = refs[15:-2], refs[-2:]
    fill(k_buf, v_buf, (up, down))
    at = 2 * CHUNK
    k_buf[at : at + CHUNK] = k_far[:CHUNK]
    v_buf[at : at + CHUNK] = v_far[:CHUNK]
    at += CHUNK
    k_buf[at : at + 16] = k_far[CHUNK:]
    v_buf[at : at + 16] = v_far[CHUNK:]
    for t in tails:
        at += 16
        k_buf[at : at + 16] = t[CHUNK:, :HD]
        v_buf[at : at + 16] = t[CHUNK:, HD:]

    subs = CHUNK // size

    def step(b, carry):
        at = rows_at(parts[0] * 2 * subs + b, size)
        sub, h = lax.rem(b, subs), lax.rem(b // subs, 2)
        m, l, acc = softmax_block(q_all[at], k_buf, v_buf, (m_in[at], l_in[at], acc_in[at]), lift)
        l = jnp.broadcast_to(jnp.sum(l, axis=1, keepdims=True), l.shape)
        values = (acc / l).astype(BF)
        lse = m * C2 + jnp.log2(l)
        packed = jnp.zeros((16, HD), F32)
        line = lax.broadcasted_iota(jnp.int32, (16, HD), 0)
        for t in range(size // HD):
            whole = lse[t * HD : (t + 1) * HD].T[:16]
            high = whole.astype(BF).astype(F32)
            mid = (whole - high).astype(BF).astype(F32)
            for i, v in enumerate((high, mid, whole - high - mid)):
                packed = jnp.where(line == 3 * (t + sub * (size // HD)) + i, v, packed)
        for i, out in enumerate(outs):

            @pl.when(b // (2 * subs) == i)
            def _(out=out):
                out[h, rows_at(sub, size)] = values
                rest = out[h, CHUNK:].astype(F32)
                out[h, CHUNK:] = jnp.where(
                    line < 3 * sub * (size // HD), rest, packed
                ).astype(BF)

        return carry

    lax.fori_loop(0, 2 * subs * len(parts), step, 0)


def merge_kernel(p0, p1, p2, p3, out):
    per = HD // GRID_W
    for h in range(2):
        tails = [p[h, CHUNK:].astype(F32) for p in (p0, p1, p2, p3)]
        for t in range(CHUNK // HD):
            lse = [v[3 * t : 3 * t + 1] + v[3 * t + 1 : 3 * t + 2] + v[3 * t + 2 : 3 * t + 3] for v in tails]
            top = tree(lse, jnp.maximum)
            share = [jnp.exp2(v - top) for v in lse]
            inv = 1.0 / tree(share, jnp.add)
            total = None
            for p, v in zip((p0, p1, p2, p3), share):
                w = jnp.broadcast_to(v * inv, (HD, HD)).T
                term = p[h, t * HD : (t + 1) * HD].astype(F32) * w
                total = term if total is None else total + term
            total = total.astype(BF)
            for i in range(per):
                out[t * per + i, :, h * HD : (h + 1) * HD] = total[i * GRID_W : (i + 1) * GRID_W]


def near(v):
    return pltpu.with_memory_space_constraint(v, pltpu.VMEM)


VMEM = pl.BlockSpec(memory_space=pltpu.VMEM)


def call(kernel, operands, shape, keys, rows, alias=None):
    scratch = [pltpu.VMEM((keys, HD), BF)] * 2 if keys else []
    return pl.pallas_call(
        kernel,
        out_shape=shape,
        in_specs=[VMEM] * len(operands),
        out_specs=[VMEM] * len(shape),
        input_output_aliases=alias or {},
        scratch_shapes=scratch,
        compiler_params=pltpu.CompilerParams(vmem_limit_bytes=20 * 2**20),
        cost_estimate=pl.CostEstimate(
            flops=rows * max(keys, 128) * 4 * HD, transcendentals=rows * keys, bytes_accessed=2**20
        ),
    )(*[near(v) for v in operands])


def finish_kernel(got, w0, w1, w2, w3, w4, w5, w6, w7, lat, mod, out):
    core = lax.axis_index("c")
    width = lat.shape[1]
    mixed = None
    for j, weight in enumerate((w0, w1, w2, w3, w4, w5, w6, w7)):
        side, piece = j // 4, j % 4
        owner = core if side == 0 else 1 - core
        ahead = 1 - 2 * owner
        tp = tp_of((0, -ahead, ahead, 2)[piece], owner)
        part = jnp.dot(got[tp], weight[...], preferred_element_type=F32)
        mixed = part if mixed is None else mixed + part
    gate = columns_of(mod, 0, 2 * width, 3 * width)
    out[...] = (lat[...].astype(F32) + gate * rms(mixed)).astype(BF)


def body(
    latents, context, cond, ctx_cond, mod_weight, query_weight, key_matrix, value_matrix, out_weight,
    query_gain, key_gain,
):
    def over_four(v, axis):
        return [
            v,
            lax.ppermute(v, axis, shift(4, 1)),
            lax.ppermute(v, axis, shift(4, -1)),
            lax.ppermute(v, axis, shift(4, 2)),
        ]

    def swap(v):
        return lax.ppermute(v, "c", [(0, 1), (1, 0)])

    ahead = [(2 * i + c, 2 * ((i + 1 - 2 * c) % 4) + c) for i in range(4) for c in range(2)]
    behind = [(b, a) for a, b in ahead]

    mine = over_four(latents, "y")
    partial = jnp.dot(
        jax.nn.silu(jnp.stack([cond, ctx_cond])), mod_weight, precision=lax.Precision.HIGHEST
    )
    shares = lax.all_to_all(jnp.broadcast_to(partial[None], (32,) + partial.shape), SP, 0, 0)
    theirs = [swap(v) for v in mine]
    summed = jnp.sum(shares, axis=0)
    modulation = lax.all_to_all(jnp.broadcast_to(summed[None], (8,) + summed.shape), TP, 0, 0)
    count = 16384
    tables = [jnp.asarray(t) for t in rope_tables(count)]
    loaded = [
        latents, query_weight, key_matrix, value_matrix, context, query_gain[None], key_gain[None], *tables,
    ]
    q, kv = pl.pallas_call(
        project_kernel,
        out_shape=[pltpu.VMEM((2, 512, HD), BF), pltpu.VMEM((528, 2 * HD), BF)],
        in_specs=[VMEM] * 8 + [pl.BlockSpec(memory_space=pltpu.HBM)] * len(loaded),
        out_specs=[VMEM] * 2,
        scratch_shapes=[pltpu.VMEM((256, 2048), BF)]
        + [pltpu.VMEM(v.shape, v.dtype) for v in loaded]
        + [pltpu.SemaphoreType.DMA((len(loaded),))],
        compiler_params=pltpu.CompilerParams(vmem_limit_bytes=20 * 2**20),
        cost_estimate=pl.CostEstimate(flops=2 * 528 * 2048 * 512, transcendentals=0, bytes_accessed=4 * 2**20),
        name="project",
    )(
        *[near(v) for v in mine[1:] + theirs],
        near(modulation),
        *[pltpu.with_memory_space_constraint(v, pltpu.HBM) for v in loaded],
    )
    lift = math.log(count / (2.0 * 512))
    kv, late_weight = lax.optimization_barrier((kv, out_weight))
    up, down = [kv], [kv]
    up.append(lax.ppermute(kv, "z", shift(8, 1)))
    down.append(lax.ppermute(kv, "z", shift(8, -1)))
    q_parts = over_four(q, "x")
    for _ in range(2):
        up.append(lax.ppermute(up[-1], "z", shift(8, 1)))
        down.append(lax.ppermute(down[-1], "z", shift(8, -1)))
    k_far = lax.ppermute(up[3][:, :HD], "z", shift(8, 1))
    v_far = lax.ppermute(down[3][:, HD:], "z", shift(8, -1))
    first = lax.ppermute(late_weight, TP, ahead)
    second = lax.ppermute(late_weight, TP, behind)
    weights = [out_weight, first, second, lax.ppermute(first, TP, ahead)]
    weights += [swap(late_weight), swap(first), swap(second)]
    weights.append(swap(weights[3]))

    rows = 8 * CHUNK
    state_of = lambda n: [pltpu.VMEM((n, HD), F32)] * 3
    firsts = [kv, up[1], down[1]]
    own = call(own_kernel, [q, *firsts], state_of(2 * CHUNK), 3 * CHUNK, 2 * CHUNK)
    q_all, *state = call(
        rest_kernel, [*q_parts, *own, *firsts], [pltpu.VMEM((rows, HD), BF)] + state_of(rows),
        3 * CHUNK, 6 * CHUNK,
    )
    state = call(
        more_kernel, [q_all, *state, up[2], down[2]], state_of(rows), 2 * CHUNK, rows,
        {1: 0, 2: 1, 3: 2},
    )

    def final(*parts):
        return call(
            functools.partial(final_kernel, parts=parts, lift=lift, size=CHUNK * len(parts) // 2),
            [q_all, *state, up[3], down[3], k_far, v_far, kv, *up[1:], *down[1:]],
            [pltpu.VMEM((2, CHUNK + 16, HD), BF)] * len(parts), 3 * CHUNK + HD, 2 * CHUNK * len(parts),
        )

    (to_far,) = final(3)
    partials = [lax.ppermute(to_far, "x", shift(4, 2))]
    to_down, to_up = final(1, 2)
    partials.append(lax.ppermute(to_down, "x", shift(4, -1)))
    partials.append(lax.ppermute(to_up, "x", shift(4, 1)))
    partials += final(0)
    (sent,) = call(merge_kernel, partials, [jax.ShapeDtypeStruct((8, GRID_W, 2 * HD), BF)], 0, CHUNK)
    got = lax.all_to_all(sent, TP, 0, 0)
    operands = [got, *weights, latents, modulation]
    return pl.pallas_call(
        finish_kernel,
        out_shape=jax.ShapeDtypeStruct(latents.shape, BF),
        in_specs=[VMEM] * len(operands),
        out_specs=VMEM,
        compiler_params=pltpu.CompilerParams(vmem_limit_bytes=20 * 2**20),
        cost_estimate=pl.CostEstimate(flops=2 * 64 * 2048 * 2048, transcendentals=0, bytes_accessed=10 * 2**20),
        name="finish",
    )(*[near(v) for v in operands])


def solution(mesh):
    torus = Mesh(mesh.devices.reshape(8, 4, 4, 2), ALL)
    placed = (
        P(ALL, None), P(SP, None), P(SP), P(SP), P(SP, TP), P(None, TP), P(None, TP), P(None, TP),
        P(TP, None), P(), P(),
    )

    return jax.shard_map(body, mesh=torus, in_specs=placed, out_specs=P(ALL, None), check_vma=False)
```

time: 138 us -> 177 us (1.28)
  waiting for transfers between devices: 35.8 us -> 60.6 us
  Pallas kernels: 43.9 us -> 52.3 us
  starting transfers between devices: 54 us -> 59 us
    ppermute x1, waiting for transfers between devices: 0.66 us -> 21.9 us  [body(): first = lax.ppermute(late_weight, TP, ahead)]
    ppermute x2 -> x5, waiting for transfers between devices: 0.01 us -> 11.7 us  [the longest x1 5.77 us: body(): partials.append(lax.ppermute(to_down, 'x', shift(4, -1)))]
    pallas_call x5 -> x7, Pallas kernels: 34.6 us -> 43.3 us  [call(): pl.pallas_call(kernel, out_shape=shape, in_specs=[VMEM] * len(operands),...]
    all_to_all x1, waiting for transfers between devices: 13.9 us -> 6.57 us  [body(): got = lax.all_to_all(sent, TP, 0, 0)]
    ppermute x8, starting transfers between devices: 3.61 us -> 10.9 us  [swap(): return lax.ppermute(v, 'c', [(0, 1), (1, 0)])]
    ppermute x2, waiting for transfers between devices: 0.01 us -> 4.38 us  [body(): up.append(lax.ppermute(up[-1], 'z', shift(8, 1)))]
    ppermute x8, waiting for transfers between devices: 3.77 us -> 0.02 us  [swap(): return lax.ppermute(v, 'c', [(0, 1), (1, 0)])]
    ppermute x1, waiting for transfers between devices: 0.17 us -> 3.84 us  [body(): up.append(lax.ppermute(kv, 'z', shift(8, 1)))]
  transfers between devices with their start and end apart: 28 -> 31, of which waited for: 10 -> 9; matrix products, arithmetic and copies ran while one was open for 2% -> 1% of each run, Pallas kernels for 25% -> 25%
where the time goes in v1:
time: 177 us; the launch traced here: 176 us
  waiting for transfers between devices  60.6 us (34%)
  starting transfers between devices  59 us (33%)
  Pallas kernels  52.3 us (30%)
  local copies, waits for them, and re-layouts  3.04 us (2%)
    pallas_call x7, Pallas kernels, call(): pl.pallas_call(kernel, out_shape=shape, in_specs=[VMEM] * len(operands),...  43.3 us
    ppermute x1, waiting for transfers between devices, body(): first = lax.ppermute(late_weight, TP, ahead)  21.9 us
    all_to_all x1, starting transfers between devices, body(): lax.all_to_all(jnp.broadcast_to(partial[None], (32,) + partial.shape), SP...  11 us
    ppermute x8, starting transfers between devices, swap(): return lax.ppermute(v, 'c', [(0, 1), (1, 0)])  10.9 us
    all_to_all x1, starting transfers between devices, body(): got = lax.all_to_all(sent, TP, 0, 0)  7.95 us
    all_to_all x1, waiting for transfers between devices, body(): lax.all_to_all(jnp.broadcast_to(partial[None], (32,) + partial.shape), SP...  7.36 us
    all_to_all x1, waiting for transfers between devices, body(): got = lax.all_to_all(sent, TP, 0, 0)  6.57 us
    all_to_all x1, starting transfers between devices, body(): lax.all_to_all(jnp.broadcast_to(summed[None], (8,) + summed.shape), TP, 0...  6.4 us
  transfers between devices with their start and end apart: 31, of which 9 were waited for; matrix products, arithmetic and copies ran while one was open for 1% of the time, Pallas kernels for 25%

profile of v1, /device:TPU:1, one launch (start us, length us, event | category | flops | bytes accessed | tf_op | source)
XLA Modules:
  0.0 176.2 jit_solution(5665260796219997192)
XLA Ops:
  0.0 2.1 %collective-permute-start = (bf16[64,2048]{1,0:T(8,128)(2,1)}, bf16[64,2048]{1,0:T(8,128)(2,1)S(1)}, u32[]{:S(2)}, u32[]{:S(2)}) collective-permute-start(bf16[64,2048]{1,0:T(8,128)(2,1)} %lat.1), channel_id=1, source_target_pairs={{0,2},{2,4},{4,6},{6,0},{1,3},{3,5},{5,7},{7,1},{8,10},{10,12},{12... | collective-permute-start | bytes 786440 | tf_op jit(solution)/shard_map/ppermute | solution.py:318
  2.1 1.5 collective-permute-start.1
  3.6 1.6 collective-permute-start.2
  6.8 11.0 %all-to-all-start = ((f32[32,2,768]{2,1,0:T(2,128)}), f32[32,2,768]{2,1,0:T(2,128)S(1)}, u32[]{:S(2)}, u32[]{:S(2)}) async-start(f32[32,2,768]{2,1,0:T(2,128)} %broadcast_in_dim.8), calls=%async_computation | async-start | bytes 393216 | tf_op jit(solution)/shard_map/all_to_all | solution.py:333
  17.9 1.9 %collective-permute-start.3 = (bf16[64,2048]{1,0:T(8,128)(2,1)}, bf16[64,2048]{1,0:T(8,128)(2,1)S(1)}, u32[]{:S(2)}, u32[]{:S(2)}) collective-permute-start(bf16[64,2048]{1,0:T(8,128)(2,1)} %lat.1), channel_id=1, source_target_pairs={{0,1},{1,0},{2,3},{3,2},{4,5},{5,4},{6,7},{7,6},{8,9},{9,8},{10,11... | collective-permute-start | bytes 786440 | tf_op jit(solution)/shard_map/ppermute | solution.py:324
  20.4 7.4 %all-to-all-done = f32[32,2,768]{2,1,0:T(2,128)S(1)} async-done(((f32[32,2,768]{2,1,0:T(2,128)}), f32[32,2,768]{2,1,0:T(2,128)S(1)}, u32[]{:S(2)}, u32[]{:S(2)}) %all-to-all-start) | async-done | bytes 196640 | tf_op jit(solution)/shard_map/all_to_all | solution.py:333
  28.5 6.4 %all-to-all-start.1 = ((f32[8,2,768]{2,1,0:T(2,128)}), f32[8,2,768]{2,1,0:T(2,128)S(1)}, u32[]{:S(2)}, u32[]{:S(2)}) async-start(f32[8,2,768]{2,1,0:T(2,128)} %broadcast_in_dim.9), calls=%async_computation.1 | async-start | bytes 98304 | tf_op jit(solution)/shard_map/all_to_all | solution.py:336
  34.9 4.8 %all-to-all-done.1.refs_7_.mod = f32[8,2,768]{2,1,0:T(2,128)S(1)} async-done(((f32[8,2,768]{2,1,0:T(2,128)}), f32[8,2,768]{2,1,0:T(2,128)S(1)}, u32[]{:S(2)}, u32[]{:S(2)}) %all-to-all-start.1) | async-done | bytes 49184 | tf_op jit(solution)/shard_map/all_to_all | solution.py:336
  39.7 4.0 %project.1 = (bf16[2,512,128]{2,1,0:T(8,128)(2,1)S(1)}, bf16[528,256]{1,0:T(8,128)(2,1)S(1)}) custom-call(bf16[64,2048]{1,0:T(8,128)(2,1)S(1)} %collective-permute-done.refs_0_, bf16[64,2048]{1,0:T(8,128)(2,1)S(1)} %collective-permute-done.1.refs_1_, bf16[64,2048]{1,0:T(8,128)(2,1)S(1)} %collective-permute-done.2.refs_2_, ...), custom_call_target="tpu_custom_call" | custom-call | flops 1107296256 | bytes 4194304 | tf_op jit(solution)/shard_map/project/pallas_call | solution.py:342
  43.8 1.0 collective-permute-start.21
  45.3 21.9 %collective-permute-done.21.w1 = bf16[256,2048]{1,0:T(8,128)(2,1)S(1)} collective-permute-done((bf16[256,2048]{1,0:T(8,128)(2,1)S(1)}, bf16[256,2048]{1,0:T(8,128)(2,1)S(1)}, u32[]{:S(2)}, u32[]{:S(2)}) %collective-permute-start.21) | collective-permute-done | bytes 1048608 | tf_op jit(solution)/shard_map/ppermute | solution.py:369
  67.8 2.7 %collective-permute-start.11 = (bf16[528,256]{1,0:T(8,128)(2,1)S(1)}, bf16[528,256]{1,0:T(8,128)(2,1)S(1)}, u32[]{:S(2)}, u32[]{:S(2)}) collective-permute-start(bf16[528,256]{1,0:T(8,128)(2,1)S(1)} %get-tuple-element.23.kv.refs_8_), channel_id=1, source_target_pairs={{0,224},{32,0},{64,32},{96,64},{128,96},{160,128},{192,160},{224,1... | collective-permute-start | bytes 811016 | tf_op jit(solution)/shard_map/ppermute | solution.py:362
  70.5 3.8 %collective-permute-done.10.up.refs_9_ = bf16[528,256]{1,0:T(8,128)(2,1)S(1)} collective-permute-done((bf16[528,256]{1,0:T(8,128)(2,1)S(1)}, bf16[528,256]{1,0:T(8,128)(2,1)S(1)}, u32[]{:S(2)}, u32[]{:S(2)}) %collective-permute-start.10) | collective-permute-done | bytes 270368 | tf_op jit(solution)/shard_map/ppermute | solution.py:361
  74.3 3.1 %collective-permute-start.13 = (bf16[528,256]{1,0:T(8,128)(2,1)S(1)}, bf16[528,256]{1,0:T(8,128)(2,1)S(1)}, u32[]{:S(2)}, u32[]{:S(2)}) collective-permute-start(bf16[528,256]{1,0:T(8,128)(2,1)S(1)} %collective-permute-done.11.down.refs_12_), channel_id=1, source_target_pairs={{0,224},{32,0},{64,32},{96,64},{128,96},{160,128},{192,160},{224,1... | collective-permute-start | bytes 811016 | tf_op jit(solution)/shard_map/ppermute | solution.py:366
  77.4 4.4 %collective-permute-done.12.up.refs_10_ = bf16[528,256]{1,0:T(8,128)(2,1)S(1)} collective-permute-done((bf16[528,256]{1,0:T(8,128)(2,1)S(1)}, bf16[528,256]{1,0:T(8,128)(2,1)S(1)}, u32[]{:S(2)}, u32[]{:S(2)}) %collective-permute-start.12) | collective-permute-done | bytes 270368 | tf_op jit(solution)/shard_map/ppermute | solution.py:365
  81.8 3.0 %collective-permute-start.15 = (bf16[528,256]{1,0:T(8,128)(2,1)S(1)}, bf16[528,256]{1,0:T(8,128)(2,1)S(1)}, u32[]{:S(2)}, u32[]{:S(2)}) collective-permute-start(bf16[528,256]{1,0:T(8,128)(2,1)S(1)} %collective-permute-done.13.down.refs_13_), channel_id=1, source_target_pairs={{0,224},{32,0},{64,32},{96,64},{128,96},{160,128},{192,160},{224,1... | collective-permute-start | bytes 811016 | tf_op jit(solution)/shard_map/ppermute | solution.py:366
  84.7 3.4 %shard_map.136 = (f32[1024,128]{1,0:T(8,128)S(1)}, f32[1024,128]{1,0:T(8,128)S(1)}, f32[1024,128]{1,0:T(8,128)S(1)}) custom-call(bf16[2,512,128]{2,1,0:T(8,128)(2,1)S(1)} %get-tuple-element.21.q.q0, bf16[528,256]{1,0:T(8,128)(2,1)S(1)} %get-tuple-element.23.kv.refs_8_, bf16[528,256]{1,0:T(8,128)(2,1)S(1)} %collective-permute-done.10.up.refs_9_, ...), custom_call_target="tpu_custom_call" | custom-call | flops 805306368 | bytes 1048576 | tf_op jit(solution)/shard_map/pallas_call | solution.py:282
  88.1 7.3 %collective-permute-start.24 = (bf16[256,2048]{1,0:T(8,128)(2,1)S(1)}, bf16[256,2048]{1,0:T(8,128)(2,1)}, u32[]{:S(2)}, u32[]{:S(2)}) collective-permute-start(bf16[256,2048]{1,0:T(8,128)(2,1)S(1)} %copy-done.1), channel_id=1, source_target_pairs={{0,1},{1,0},{2,3},{3,2},{4,5},{5,4},{6,7},{7,6},{8,9},{9,8},{10,11... | collective-permute-start | bytes 3145736 | tf_op jit(solution)/shard_map/ppermute | solution.py:324
  95.4 12.3 %shard_map.137 = (bf16[4096,128]{1,0:T(8,128)(2,1)S(1)}, f32[4096,128]{1,0:T(8,128)S(1)}, f32[4096,128]{1,0:T(8,128)S(1)}, f32[4096,128]{1,0:T(8,128)S(1)}) custom-call(bf16[2,512,128]{2,1,0:T(8,128)(2,1)S(1)} %get-tuple-element.21.q.q0, bf16[2,512,128]{2,1,0:T(8,128)(2,1)S(1)} %collective-permute-done.7.q1, ...), custom_call_target="tpu_custom_call" | custom-call | flops 2415919104 | bytes 1048576 | tf_op jit(solution)/shard_map/pallas_call | solution.py:282
  107.9 2.7 %collective-permute-start.17 = (bf16[528,128]{1,0:T(8,128)(2,1)S(1)}, bf16[528,128]{1,0:T(8,128)(2,1)S(1)}, u32[]{:S(2)}, u32[]{:S(2)}) collective-permute-start(bf16[528,128]{1,0:T(8,128)(2,1)S(1)} %slice.9), channel_id=1, source_target_pairs={{0,224},{32,0},{64,32},{96,64},{128,96},{160,128},{192,160},{224,1... | collective-permute-start | bytes 405512 | tf_op jit(solution)/shard_map/ppermute | solution.py:368
  110.6 7.9 %shard_map.138 = (f32[4096,128]{1,0:T(8,128)S(1)}, f32[4096,128]{1,0:T(8,128)S(1)}, f32[4096,128]{1,0:T(8,128)S(1)}) custom-call(bf16[4096,128]{1,0:T(8,128)(2,1)S(1)} %get-tuple-element.27.q_all.refs_0_, f32[4096,128]{1,0:T(8,128)S(1)} %get-tuple-element.28.m_in, ...), custom_call_target="tpu_custom_call", output_to_operand_aliasing={{0}: (1, {}), {1}: (2, {}), {2}: (3, {})} | custom-call | flops 2147483648 | bytes 1048576 | tf_op jit(solution)/shard_map/pallas_call | solution.py:282
  119.7 9.8 %shard_map.140 = (bf16[2,528,128]{2,1,0:T(8,128)(2,1)S(1)}, bf16[2,528,128]{2,1,0:T(8,128)(2,1)S(1)}) custom-call(bf16[4096,128]{1,0:T(8,128)(2,1)S(1)} %get-tuple-element.27.q_all.refs_0_, f32[4096,128]{1,0:T(8,128)S(1)} %get-tuple-element.31.refs_1_, f32[4096,128]{1,0:T(8,128)S(1)} %get-tuple-element.32.refs_2_, ...), custom_call_target="tpu_custom_call" | custom-call | flops 1744830464 | bytes 1048576 | tf_op jit(solution)/shard_map/pallas_call | solution.py:282
  129.6 2.3 %collective-permute-start.19 = (bf16[2,528,128]{2,1,0:T(8,128)(2,1)S(1)}, bf16[2,528,128]{2,1,0:T(8,128)(2,1)S(1)}, u32[]{:S(2)}, u32[]{:S(2)}) collective-permute-start(bf16[2,528,128]{2,1,0:T(8,128)(2,1)S(1)} %get-tuple-element.34), channel_id=1, source_target_pairs={{0,24},{8,0},{16,8},{24,16},{1,25},{9,1},{17,9},{25,17},{2,26},{10... | collective-permute-start | bytes 811016 | tf_op jit(solution)/shard_map/ppermute | solution.py:398
  131.9 5.8 %collective-permute-done.19.p1 = bf16[2,528,128]{2,1,0:T(8,128)(2,1)S(1)} collective-permute-done((bf16[2,528,128]{2,1,0:T(8,128)(2,1)S(1)}, bf16[2,528,128]{2,1,0:T(8,128)(2,1)S(1)}, u32[]{:S(2)}, u32[]{:S(2)}) %collective-permute-start.19) | collective-permute-done | bytes 270368 | tf_op jit(solution)/shard_map/ppermute | solution.py:398
  137.7 1.3 collective-permute-start.20
  139.0 4.6 %shard_map.139 = bf16[2,528,128]{2,1,0:T(8,128)(2,1)S(1)} custom-call(bf16[4096,128]{1,0:T(8,128)(2,1)S(1)} %get-tuple-element.27.q_all.refs_0_, f32[4096,128]{1,0:T(8,128)S(1)} %get-tuple-element.31.refs_1_, f32[4096,128]{1,0:T(8,128)S(1)} %get-tuple-element.32.refs_2_, f32[4096,128]{1,0:T(8,128)S(1)} %get-tuple-element.33.refs_3_, ...), custom_call_target="tpu_custom_call" | custom-call | flops 872415232 | bytes 1048576 | tf_op jit(solution)/shard_map/pallas_call | solution.py:282
  143.6 2.9 %collective-permute-done.20.p2 = bf16[2,528,128]{2,1,0:T(8,128)(2,1)S(1)} collective-permute-done((bf16[2,528,128]{2,1,0:T(8,128)(2,1)S(1)}, bf16[2,528,128]{2,1,0:T(8,128)(2,1)S(1)}, u32[]{:S(2)}, u32[]{:S(2)}) %collective-permute-start.20) | collective-permute-done | bytes 270368 | tf_op jit(solution)/shard_map/ppermute | solution.py:399
  146.7 4.6 %shard_map.141.p3 = bf16[2,528,128]{2,1,0:T(8,128)(2,1)S(1)} custom-call(bf16[4096,128]{1,0:T(8,128)(2,1)S(1)} %get-tuple-element.27.q_all.refs_0_, f32[4096,128]{1,0:T(8,128)S(1)} %get-tuple-element.31.refs_1_, f32[4096,128]{1,0:T(8,128)S(1)} %get-tuple-element.32.refs_2_, f32[4096,128]{1,0:T(8,128)S(1)} %get-tuple-element.33.refs_3_, ...), custom_call_target="tpu_custom_call" | custom-call | flops 872415232 | bytes 1048576 | tf_op jit(solution)/shard_map/pallas_call | solution.py:282
  151.3 3.0 %collective-permute-done.18.p0 = bf16[2,528,128]{2,1,0:T(8,128)(2,1)S(1)} collective-permute-done((bf16[2,528,128]{2,1,0:T(8,128)(2,1)S(1)}, bf16[2,528,128]{2,1,0:T(8,128)(2,1)S(1)}, u32[]{:S(2)}, u32[]{:S(2)}) %collective-permute-start.18) | collective-permute-done | bytes 270368 | tf_op jit(solution)/shard_map/ppermute | solution.py:396
  155.7 8.0 %all-to-all-start.2 = ((bf16[8,64,256]{2,1,0:T(8,128)(2,1)}), bf16[8,64,256]{2,1,0:T(8,128)(2,1)}, u32[]{:S(2)}, u32[]{:S(2)}) async-start(bf16[8,64,256]{2,1,0:T(8,128)(2,1)} %copy-done.3), calls=%async_computation.2 | async-start | bytes 524288 | tf_op jit(solution)/shard_map/all_to_all | solution.py:402
  163.6 6.6 %all-to-all-done.2.got = bf16[8,64,256]{2,1,0:T(8,128)(2,1)} async-done(((bf16[8,64,256]{2,1,0:T(8,128)(2,1)}), bf16[8,64,256]{2,1,0:T(8,128)(2,1)}, u32[]{:S(2)}, u32[]{:S(2)}) %all-to-all-start.2) | async-done | bytes 262176 | tf_op jit(solution)/shard_map/all_to_all | solution.py:402
  171.2 5.0 %finish.1 = bf16[64,2048]{1,0:T(8,128)(2,1)} custom-call(bf16[8,64,256]{2,1,0:T(8,128)(2,1)} %all-to-all-done.2.got, bf16[256,2048]{1,0:T(8,128)(2,1)S(1)} %copy-done.1, bf16[256,2048]{1,0:T(8,128)(2,1)S(1)} %collective-permute-done.21.w1, bf16[256,2048]{1,0:T(8,128)(2,1)S(1)} %collective-permute-done.22.w2, bf16[256,2048]{1,0:T(8,128)(2,1)} %collective-permute-done.23.w3, ...), custom_call_target="tpu_custom_call" | custom-call | flops 536870912 | bytes 10485760 | tf_op jit(solution)/shard_map/finish/pallas_call | solution.py:404
  (53 shorter events, 8.0 us)
Async XLA Ops:
  0.0 5.2 %copy-start = (f32[64,768]{1,0:T(8,128)S(1)}, f32[64,768]{1,0:T(8,128)}, u32[]{:S(2)}) copy-start(f32[64,768]{1,0:T(8,128)} %param.18) | copy-start | bytes 589828
  0.0 19.8 %collective-permute-start = (bf16[64,2048]{1,0:T(8,128)(2,1)}, bf16[64,2048]{1,0:T(8,128)(2,1)S(1)}, u32[]{:S(2)}, u32[]{:S(2)}) collective-permute-start(bf16[64,2048]{1,0:T(8,128)(2,1)} %lat.1), channel_id=1, source_target_pairs={{0,2},{2,4},{4,6},{6,0},{1,3},{3,5},{5,7},{7,1},{8,10},{10,12},{12... | collective-permute-start | bytes 786440 | tf_op jit(solution)/shard_map/ppermute | solution.py:318
  2.1 17.8 %collective-permute-start.1 = (bf16[64,2048]{1,0:T(8,128)(2,1)}, bf16[64,2048]{1,0:T(8,128)(2,1)S(1)}, u32[]{:S(2)}, u32[]{:S(2)}) collective-permute-start(bf16[64,2048]{1,0:T(8,128)(2,1)} %lat.1), channel_id=1, source_target_pairs={{0,6},{2,0},{4,2},{6,4},{1,7},{3,1},{5,3},{7,5},{8,14},{10,8},{12,... | collective-permute-start | bytes 786440 | tf_op jit(solution)/shard_map/ppermute | solution.py:319
  3.6 16.6 %collective-permute-start.2 = (bf16[64,2048]{1,0:T(8,128)(2,1)}, bf16[64,2048]{1,0:T(8,128)(2,1)S(1)}, u32[]{:S(2)}, u32[]{:S(2)}) collective-permute-start(bf16[64,2048]{1,0:T(8,128)(2,1)} %lat.1), channel_id=1, source_target_pairs={{0,4},{2,6},{4,0},{6,2},{1,5},{3,7},{5,1},{7,3},{8,12},{10,14},{12... | collective-permute-start | bytes 786440 | tf_op jit(solution)/shard_map/ppermute | solution.py:320
  6.8 20.9 %all-to-all-start = ((f32[32,2,768]{2,1,0:T(2,128)}), f32[32,2,768]{2,1,0:T(2,128)S(1)}, u32[]{:S(2)}, u32[]{:S(2)}) async-start(f32[32,2,768]{2,1,0:T(2,128)} %broadcast_in_dim.8), calls=%async_computation | async-start | bytes 393216 | tf_op jit(solution)/shard_map/all_to_all | solution.py:333
  17.9 17.0 %collective-permute-start.3 = (bf16[64,2048]{1,0:T(8,128)(2,1)}, bf16[64,2048]{1,0:T(8,128)(2,1)S(1)}, u32[]{:S(2)}, u32[]{:S(2)}) collective-permute-start(bf16[64,2048]{1,0:T(8,128)(2,1)} %lat.1), channel_id=1, source_target_pairs={{0,1},{1,0},{2,3},{3,2},{4,5},{5,4},{6,7},{7,6},{8,9},{9,8},{10,11... | collective-permute-start | bytes 786440 | tf_op jit(solution)/shard_map/ppermute | solution.py:324
  19.8 19.9 %collective-permute-start.4 = (bf16[64,2048]{1,0:T(8,128)(2,1)S(1)}, bf16[64,2048]{1,0:T(8,128)(2,1)S(1)}, u32[]{:S(2)}, u32[]{:S(2)}) collective-permute-start(bf16[64,2048]{1,0:T(8,128)(2,1)S(1)} %collective-permute-done.refs_0_), channel_id=1, source_target_pairs={{0,1},{1,0},{2,3},{3,2},{4,5},{5,4},{6,7},{7,6},{8,9},{9,8},{10,11... | collective-permute-start | bytes 786440 | tf_op jit(solution)/shard_map/ppermute | solution.py:324
  19.9 19.8 %collective-permute-start.5 = (bf16[64,2048]{1,0:T(8,128)(2,1)S(1)}, bf16[64,2048]{1,0:T(8,128)(2,1)S(1)}, u32[]{:S(2)}, u32[]{:S(2)}) collective-permute-start(bf16[64,2048]{1,0:T(8,128)(2,1)S(1)} %collective-permute-done.1.refs_1_), channel_id=1, source_target_pairs={{0,1},{1,0},{2,3},{3,2},{4,5},{5,4},{6,7},{7,6},{8,9},{9,8},{10,11... | collective-permute-start | bytes 786440 | tf_op jit(solution)/shard_map/ppermute | solution.py:324
  20.3 19.4 %collective-permute-start.6 = (bf16[64,2048]{1,0:T(8,128)(2,1)S(1)}, bf16[64,2048]{1,0:T(8,128)(2,1)S(1)}, u32[]{:S(2)}, u32[]{:S(2)}) collective-permute-start(bf16[64,2048]{1,0:T(8,128)(2,1)S(1)} %collective-permute-done.2.refs_2_), channel_id=1, source_target_pairs={{0,1},{1,0},{2,3},{3,2},{4,5},{5,4},{6,7},{7,6},{8,9},{9,8},{10,11... | collective-permute-start | bytes 786440 | tf_op jit(solution)/shard_map/ppermute | solution.py:324
  28.5 11.2 %all-to-all-start.1 = ((f32[8,2,768]{2,1,0:T(2,128)}), f32[8,2,768]{2,1,0:T(2,128)S(1)}, u32[]{:S(2)}, u32[]{:S(2)}) async-start(f32[8,2,768]{2,1,0:T(2,128)} %broadcast_in_dim.9), calls=%async_computation.1 | async-start | bytes 98304 | tf_op jit(solution)/shard_map/all_to_all | solution.py:336
  43.8 23.5 %collective-permute-start.21 = (bf16[256,2048]{1,0:T(8,128)(2,1)S(1)}, bf16[256,2048]{1,0:T(8,128)(2,1)S(1)}, u32[]{:S(2)}, u32[]{:S(2)}) collective-permute-start(bf16[256,2048]{1,0:T(8,128)(2,1)S(1)} %copy-done.1), channel_id=1, source_target_pairs={{0,2},{1,7},{2,4},{3,1},{4,6},{5,3},{6,0},{7,5},{8,10},{9,15},{10,... | collective-permute-start | bytes 3145736 | tf_op jit(solution)/shard_map/ppermute | solution.py:369
  44.7 25.8 %collective-permute-start.7 = (bf16[2,512,128]{2,1,0:T(8,128)(2,1)S(1)}, bf16[2,512,128]{2,1,0:T(8,128)(2,1)S(1)}, u32[]{:S(2)}, u32[]{:S(2)}) collective-permute-start(bf16[2,512,128]{2,1,0:T(8,128)(2,1)S(1)} %get-tuple-element.21.q.q0), channel_id=1, source_target_pairs={{0,8},{8,16},{16,24},{24,0},{1,9},{9,17},{17,25},{25,1},{2,10},{10... | collective-permute-start | bytes 786440 | tf_op jit(solution)/shard_map/ppermute | solution.py:318
  44.7 74.5 %collective-permute-start.22 = (bf16[256,2048]{1,0:T(8,128)(2,1)S(1)}, bf16[256,2048]{1,0:T(8,128)(2,1)S(1)}, u32[]{:S(2)}, u32[]{:S(2)}) collective-permute-start(bf16[256,2048]{1,0:T(8,128)(2,1)S(1)} %copy-done.1), channel_id=1, source_target_pairs={{2,0},{7,1},{4,2},{1,3},{6,4},{3,5},{0,6},{5,7},{10,8},{15,9},{12,... | collective-permute-start | bytes 3145736 | tf_op jit(solution)/shard_map/ppermute | solution.py:370
  67.2 52.1 %collective-permute-start.23 = (bf16[256,2048]{1,0:T(8,128)(2,1)S(1)}, bf16[256,2048]{1,0:T(8,128)(2,1)}, u32[]{:S(2)}, u32[]{:S(2)}) collective-permute-start(bf16[256,2048]{1,0:T(8,128)(2,1)S(1)} %collective-permute-done.21.w1), channel_id=1, source_target_pairs={{0,2},{1,7},{2,4},{3,1},{4,6},{5,3},{6,0},{7,5},{8,10},{9,15},{10,... | collective-permute-start | bytes 3145736 | tf_op jit(solution)/shard_map/ppermute | solution.py:371
  67.8 6.5 %collective-permute-start.10 = (bf16[528,256]{1,0:T(8,128)(2,1)S(1)}, bf16[528,256]{1,0:T(8,128)(2,1)S(1)}, u32[]{:S(2)}, u32[]{:S(2)}) collective-permute-start(bf16[528,256]{1,0:T(8,128)(2,1)S(1)} %get-tuple-element.23.kv.refs_8_), channel_id=1, source_target_pairs={{0,32},{32,64},{64,96},{96,128},{128,160},{160,192},{192,224},{224... | collective-permute-start | bytes 811016 | tf_op jit(solution)/shard_map/ppermute | solution.py:361
  67.8 6.5 %collective-permute-start.11 = (bf16[528,256]{1,0:T(8,128)(2,1)S(1)}, bf16[528,256]{1,0:T(8,128)(2,1)S(1)}, u32[]{:S(2)}, u32[]{:S(2)}) collective-permute-start(bf16[528,256]{1,0:T(8,128)(2,1)S(1)} %get-tuple-element.23.kv.refs_8_), channel_id=1, source_target_pairs={{0,224},{32,0},{64,32},{96,64},{128,96},{160,128},{192,160},{224,1... | collective-permute-start | bytes 811016 | tf_op jit(solution)/shard_map/ppermute | solution.py:362
  70.5 6.9 %collective-permute-start.8 = (bf16[2,512,128]{2,1,0:T(8,128)(2,1)S(1)}, bf16[2,512,128]{2,1,0:T(8,128)(2,1)S(1)}, u32[]{:S(2)}, u32[]{:S(2)}) collective-permute-start(bf16[2,512,128]{2,1,0:T(8,128)(2,1)S(1)} %get-tuple-element.21.q.q0), channel_id=1, source_target_pairs={{0,24},{8,0},{16,8},{24,16},{1,25},{9,1},{17,9},{25,17},{2,26},{10... | collective-permute-start | bytes 786440 | tf_op jit(solution)/shard_map/ppermute | solution.py:319
  74.3 7.5 %collective-permute-start.12 = (bf16[528,256]{1,0:T(8,128)(2,1)S(1)}, bf16[528,256]{1,0:T(8,128)(2,1)S(1)}, u32[]{:S(2)}, u32[]{:S(2)}) collective-permute-start(bf16[528,256]{1,0:T(8,128)(2,1)S(1)} %collective-permute-done.10.up.refs_9_), channel_id=1, source_target_pairs={{0,32},{32,64},{64,96},{96,128},{128,160},{160,192},{192,224},{224... | collective-permute-start | bytes 811016 | tf_op jit(solution)/shard_map/ppermute | solution.py:365
  74.3 7.5 %collective-permute-start.13 = (bf16[528,256]{1,0:T(8,128)(2,1)S(1)}, bf16[528,256]{1,0:T(8,128)(2,1)S(1)}, u32[]{:S(2)}, u32[]{:S(2)}) collective-permute-start(bf16[528,256]{1,0:T(8,128)(2,1)S(1)} %collective-permute-done.11.down.refs_12_), channel_id=1, source_target_pairs={{0,224},{32,0},{64,32},{96,64},{128,96},{160,128},{192,160},{224,1... | collective-permute-start | bytes 811016 | tf_op jit(solution)/shard_map/ppermute | solution.py:366
  77.4 10.7 %collective-permute-start.9 = (bf16[2,512,128]{2,1,0:T(8,128)(2,1)S(1)}, bf16[2,512,128]{2,1,0:T(8,128)(2,1)S(1)}, u32[]{:S(2)}, u32[]{:S(2)}) collective-permute-start(bf16[2,512,128]{2,1,0:T(8,128)(2,1)S(1)} %get-tuple-element.21.q.q0), channel_id=1, source_target_pairs={{0,16},{8,24},{16,0},{24,8},{1,17},{9,25},{17,1},{25,9},{2,18},{10... | collective-permute-start | bytes 786440 | tf_op jit(solution)/shard_map/ppermute | solution.py:320
  81.8 25.9 %collective-permute-start.14 = (bf16[528,256]{1,0:T(8,128)(2,1)S(1)}, bf16[528,256]{1,0:T(8,128)(2,1)S(1)}, u32[]{:S(2)}, u32[]{:S(2)}) collective-permute-start(bf16[528,256]{1,0:T(8,128)(2,1)S(1)} %collective-permute-done.12.up.refs_10_), channel_id=1, source_target_pairs={{0,32},{32,64},{64,96},{96,128},{128,160},{160,192},{192,224},{224... | collective-permute-start | bytes 811016 | tf_op jit(solution)/shard_map/ppermute | solution.py:365
  81.8 26.1 %collective-permute-start.15 = (bf16[528,256]{1,0:T(8,128)(2,1)S(1)}, bf16[528,256]{1,0:T(8,128)(2,1)S(1)}, u32[]{:S(2)}, u32[]{:S(2)}) collective-permute-start(bf16[528,256]{1,0:T(8,128)(2,1)S(1)} %collective-permute-done.13.down.refs_13_), channel_id=1, source_target_pairs={{0,224},{32,0},{64,32},{96,64},{128,96},{160,128},{192,160},{224,1... | collective-permute-start | bytes 811016 | tf_op jit(solution)/shard_map/ppermute | solution.py:366
  88.1 75.5 %collective-permute-start.24 = (bf16[256,2048]{1,0:T(8,128)(2,1)S(1)}, bf16[256,2048]{1,0:T(8,128)(2,1)}, u32[]{:S(2)}, u32[]{:S(2)}) collective-permute-start(bf16[256,2048]{1,0:T(8,128)(2,1)S(1)} %copy-done.1), channel_id=1, source_target_pairs={{0,1},{1,0},{2,3},{3,2},{4,5},{5,4},{6,7},{7,6},{8,9},{9,8},{10,11... | collective-permute-start | bytes 3145736 | tf_op jit(solution)/shard_map/ppermute | solution.py:324
  107.8 10.8 %collective-permute-start.16 = (bf16[528,128]{1,0:T(8,128)(2,1)S(1)}, bf16[528,128]{1,0:T(8,128)(2,1)S(1)}, u32[]{:S(2)}, u32[]{:S(2)}) collective-permute-start(bf16[528,128]{1,0:T(8,128)(2,1)S(1)} %slice.8), channel_id=1, source_target_pairs={{0,32},{32,64},{64,96},{96,128},{128,160},{160,192},{192,224},{224... | collective-permute-start | bytes 405512 | tf_op jit(solution)/shard_map/ppermute | solution.py:367
  107.9 11.9 %collective-permute-start.17 = (bf16[528,128]{1,0:T(8,128)(2,1)S(1)}, bf16[528,128]{1,0:T(8,128)(2,1)S(1)}, u32[]{:S(2)}, u32[]{:S(2)}) collective-permute-start(bf16[528,128]{1,0:T(8,128)(2,1)S(1)} %slice.9), channel_id=1, source_target_pairs={{0,224},{32,0},{64,32},{96,64},{128,96},{160,128},{192,160},{224,1... | collective-permute-start | bytes 405512 | tf_op jit(solution)/shard_map/ppermute | solution.py:368
  118.5 51.7 %collective-permute-start.25 = (bf16[256,2048]{1,0:T(8,128)(2,1)S(1)}, bf16[256,2048]{1,0:T(8,128)(2,1)}, u32[]{:S(2)}, u32[]{:S(2)}) collective-permute-start(bf16[256,2048]{1,0:T(8,128)(2,1)S(1)} %collective-permute-done.21.w1), channel_id=1, source_target_pairs={{0,1},{1,0},{2,3},{3,2},{4,5},{5,4},{6,7},{7,6},{8,9},{9,8},{10,11... | collective-permute-start | bytes 3145736 | tf_op jit(solution)/shard_map/ppermute | solution.py:324
  119.2 51.0 %collective-permute-start.26 = (bf16[256,2048]{1,0:T(8,128)(2,1)S(1)}, bf16[256,2048]{1,0:T(8,128)(2,1)}, u32[]{:S(2)}, u32[]{:S(2)}) collective-permute-start(bf16[256,2048]{1,0:T(8,128)(2,1)S(1)} %collective-permute-done.22.w2), channel_id=1, source_target_pairs={{0,1},{1,0},{2,3},{3,2},{4,5},{5,4},{6,7},{7,6},{8,9},{9,8},{10,11... | collective-permute-start | bytes 3145736 | tf_op jit(solution)/shard_map/ppermute | solution.py:324
  119.3 50.9 %collective-permute-start.27 = (bf16[256,2048]{1,0:T(8,128)(2,1)}, bf16[256,2048]{1,0:T(8,128)(2,1)}, u32[]{:S(2)}, u32[]{:S(2)}) collective-permute-start(bf16[256,2048]{1,0:T(8,128)(2,1)} %collective-permute-done.23.w3), channel_id=1, source_target_pairs={{0,1},{1,0},{2,3},{3,2},{4,5},{5,4},{6,7},{7,6},{8,9},{9,8},{10,11... | collective-permute-start | bytes 3145736 | tf_op jit(solution)/shard_map/ppermute | solution.py:324
  129.6 8.1 %collective-permute-start.19 = (bf16[2,528,128]{2,1,0:T(8,128)(2,1)S(1)}, bf16[2,528,128]{2,1,0:T(8,128)(2,1)S(1)}, u32[]{:S(2)}, u32[]{:S(2)}) collective-permute-start(bf16[2,528,128]{2,1,0:T(8,128)(2,1)S(1)} %get-tuple-element.34), channel_id=1, source_target_pairs={{0,24},{8,0},{16,8},{24,16},{1,25},{9,1},{17,9},{25,17},{2,26},{10... | collective-permute-start | bytes 811016 | tf_op jit(solution)/shard_map/ppermute | solution.py:398
  137.7 8.9 %collective-permute-start.20 = (bf16[2,528,128]{2,1,0:T(8,128)(2,1)S(1)}, bf16[2,528,128]{2,1,0:T(8,128)(2,1)S(1)}, u32[]{:S(2)}, u32[]{:S(2)}) collective-permute-start(bf16[2,528,128]{2,1,0:T(8,128)(2,1)S(1)} %get-tuple-element.35), channel_id=1, source_target_pairs={{0,8},{8,16},{16,24},{24,0},{1,9},{9,17},{17,25},{25,1},{2,10},{10... | collective-permute-start | bytes 811016 | tf_op jit(solution)/shard_map/ppermute | solution.py:399
  146.5 7.8 %collective-permute-start.18 = (bf16[2,528,128]{2,1,0:T(8,128)(2,1)S(1)}, bf16[2,528,128]{2,1,0:T(8,128)(2,1)S(1)}, u32[]{:S(2)}, u32[]{:S(2)}) collective-permute-start(bf16[2,528,128]{2,1,0:T(8,128)(2,1)S(1)} %shard_map.139), channel_id=1, source_target_pairs={{0,16},{8,24},{16,0},{24,8},{1,17},{9,25},{17,1},{25,9},{2,18},{10... | collective-permute-start | bytes 811016 | tf_op jit(solution)/shard_map/ppermute | solution.py:396
  155.7 14.5 %all-to-all-start.2 = ((bf16[8,64,256]{2,1,0:T(8,128)(2,1)}), bf16[8,64,256]{2,1,0:T(8,128)(2,1)}, u32[]{:S(2)}, u32[]{:S(2)}) async-start(bf16[8,64,256]{2,1,0:T(8,128)(2,1)} %copy-done.3), calls=%async_computation.2 | async-start | bytes 524288 | tf_op jit(solution)/shard_map/all_to_all | solution.py:402
  (3 other events, 5.7 us)

commit v2 on v1

--- a/solution.py
+++ b/solution.py
@@ -143,22 +143,20 @@
     s = scores_of(q, k_buf[...])
     tiles = [s[:, i * HD : (i + 1) * HD] for i in range(s.shape[1] // HD)]
     if lift is not None:
-        tiles[-1] = tiles[-1] + lift / SCALE
-    top = jnp.max(tree(tiles, jnp.maximum), axis=1, keepdims=True)
+        tiles = tiles[:-2] + [tiles[-2] + lift / SCALE]
     if before is None:
-        m_new = jnp.broadcast_to(top, (s.shape[0], HD))
-    else:
-        m_old, l_old, acc_old = before
-        m_new = jnp.maximum(m_old, top)
+        blank = jnp.zeros((s.shape[0], HD), F32)
+        before = (blank - 1e30, blank, blank)
+    m_old, l_old, acc_old = before
+    m_new = jnp.maximum(m_old, jnp.max(tree(tiles, jnp.maximum), axis=1, keepdims=True))
     base = m_new * C2
+    alpha = jnp.exp2((m_old - m_new) * C2)
     probs = [jnp.exp2(t * C2 - base) for t in tiles]
-    p = jnp.concatenate([t.astype(BF) for t in probs], axis=1)
-    pv = jnp.dot(p, v_buf[...], preferred_element_type=F32)
-    sums = tree(probs, jnp.add)
-    if before is None:
-        return m_new, sums, pv
-    alpha = jnp.exp2((m_old - m_new) * C2)
-    return m_new, l_old * alpha + sums, acc_old * alpha + pv
+    p = [t.astype(BF) for t in probs]
+    if lift is not None:
+        p.append(jnp.zeros((s.shape[0], HD), BF))
+    pv = jnp.dot(jnp.concatenate(p, axis=1), v_buf[...], preferred_element_type=F32)
+    return m_new, l_old * alpha + tree(probs, jnp.add), acc_old * alpha + pv
 
 
 def rows_at(b, size=CHUNK):
@@ -218,6 +216,9 @@
         at += 16
         k_buf[at : at + 16] = t[CHUNK:, :HD]
         v_buf[at : at + 16] = t[CHUNK:, HD:]
+    at += 16
+    k_buf[at:] = jnp.zeros((HD, HD), BF)
+    v_buf[at:] = jnp.zeros((HD, HD), BF)
 
     subs = CHUNK // size
 
@@ -277,6 +278,21 @@
 VMEM = pl.BlockSpec(memory_space=pltpu.VMEM)
 
 
+def share_kernel(*refs):
+    far, out, held, arrived = refs[:3], refs[3], refs[4:7], refs[7]
+    copies = [pltpu.make_async_copy(f, h, arrived.at[i]) for i, (f, h) in enumerate(zip(far, held))]
+    for copy in copies:
+        copy.start()
+    for copy in copies:
+        copy.wait()
+    both = jnp.concatenate([held[0][...], held[1][...]], axis=0)
+    share = jnp.dot(
+        jax.nn.silu(both), held[2][...], precision=lax.Precision.HIGHEST, preferred_element_type=F32
+    )
+    for i in range(out.shape[0]):
+        out[i] = share
+
+
 def call(kernel, operands, shape, keys, rows, alias=None):
     scratch = [pltpu.VMEM((keys, HD), BF)] * 2 if keys else []
     return pl.pallas_call(
@@ -327,10 +343,16 @@
     behind = [(b, a) for a, b in ahead]
 
     mine = over_four(latents, "y")
-    partial = jnp.dot(
-        jax.nn.silu(jnp.stack([cond, ctx_cond])), mod_weight, precision=lax.Precision.HIGHEST
-    )
-    shares = lax.all_to_all(jnp.broadcast_to(partial[None], (32,) + partial.shape), SP, 0, 0)
+    loaded = [cond[None], ctx_cond[None], mod_weight]
+    shares = pl.pallas_call(
+        share_kernel,
+        out_shape=jax.ShapeDtypeStruct((32, 2, mod_weight.shape[1]), F32),
+        in_specs=[pl.BlockSpec(memory_space=pltpu.HBM)] * 3,
+        out_specs=VMEM,
+        scratch_shapes=[pltpu.VMEM(v.shape, F32) for v in loaded] + [pltpu.SemaphoreType.DMA((3,))],
+        name="share",
+    )(*[pltpu.with_memory_space_constraint(v, pltpu.HBM) for v in loaded])
+    shares = lax.all_to_all(shares, SP, 0, 0)
     theirs = [swap(v) for v in mine]
     summed = jnp.sum(shares, axis=0)
     modulation = lax.all_to_all(jnp.broadcast_to(summed[None], (8,) + summed.shape), TP, 0, 0)
@@ -356,7 +378,6 @@
         *[pltpu.with_memory_space_constraint(v, pltpu.HBM) for v in loaded],
     )
     lift = math.log(count / (2.0 * 512))
-    kv, late_weight = lax.optimization_barrier((kv, out_weight))
     up, down = [kv], [kv]
     up.append(lax.ppermute(kv, "z", shift(8, 1)))
     down.append(lax.ppermute(kv, "z", shift(8, -1)))
@@ -366,10 +387,10 @@
         down.append(lax.ppermute(down[-1], "z", shift(8, -1)))
     k_far = lax.ppermute(up[3][:, :HD], "z", shift(8, 1))
     v_far = lax.ppermute(down[3][:, HD:], "z", shift(8, -1))
-    first = lax.ppermute(late_weight, TP, ahead)
-    second = lax.ppermute(late_weight, TP, behind)
+    first = lax.ppermute(out_weight, TP, ahead)
+    second = lax.ppermute(out_weight, TP, behind)
     weights = [out_weight, first, second, lax.ppermute(first, TP, ahead)]
-    weights += [swap(late_weight), swap(first), swap(second)]
+    weights += [swap(out_weight), swap(first), swap(second)]
     weights.append(swap(weights[3]))
 
     rows = 8 * CHUNK
@@ -387,9 +408,9 @@
 
     def final(*parts):
         return call(
-            functools.partial(final_kernel, parts=parts, lift=lift, size=CHUNK * len(parts) // 2),
+            functools.partial(final_kernel, parts=parts, lift=lift, size=CHUNK),
             [q_all, *state, up[3], down[3], k_far, v_far, kv, *up[1:], *down[1:]],
-            [pltpu.VMEM((2, CHUNK + 16, HD), BF)] * len(parts), 3 * CHUNK + HD, 2 * CHUNK * len(parts),
+            [pltpu.VMEM((2, CHUNK + 16, HD), BF)] * len(parts), 3 * CHUNK + 2 * HD, 2 * CHUNK * len(parts),
         )
 
     (to_far,) = final(3)

time: 177 us -> 151 us (0.85)
  waiting for transfers between devices: 60.6 us -> 34.3 us
  Pallas kernels: 52.3 us -> 46.5 us
  starting transfers between devices: 59 us -> 64.7 us
    ppermute x2, waiting for transfers between devices: 21.9 us -> 0.01 us  [the longest x1 0.01 us: body(): first = lax.ppermute(out_weight, TP, ahead)]
    pallas_call x7, Pallas kernels: 43.3 us -> 35.6 us  [call(): pl.pallas_call(kernel, out_shape=shape, in_specs=[VMEM] * len(operands),...]
    all_to_all x1, waiting for transfers between devices: 7.36 us -> 0.01 us  [body(): shares = lax.all_to_all(shares, SP, 0, 0)]
    ppermute x8, starting transfers between devices: 10.9 us -> 15.3 us  [swap(): return lax.ppermute(v, 'c', [(0, 1), (1, 0)])]
    ppermute x2, waiting for transfers between devices: 0.01 us -> 2.41 us  [over_four(): lax.ppermute(v, axis, shift(4, 1))]
    ppermute x2, starting transfers between devices: 1.54 us -> 3.91 us  [the longest x1 3.55 us: body(): first = lax.ppermute(out_weight, TP, ahead)]
    unnamed x8 -> x14, local copies, waits for them, and re-layouts: 1.65 us -> 4.01 us
    ppermute x2, starting transfers between devices: 2.12 us -> 0.09 us  [over_four(): lax.ppermute(v, axis, shift(4, 1))]
  transfers between devices with their start and end apart: 31 -> 31, of which waited for: 9 -> 8; matrix products, arithmetic and copies ran while one was open for 1% -> 0% of each run, Pallas kernels for 25% -> 28%
where the time goes in v2:
time: 151 us; the launch traced here: 150 us
  starting transfers between devices  64.7 us (43%)
  Pallas kernels  46.5 us (31%)
  waiting for transfers between devices  34.3 us (23%)
  local copies, waits for them, and re-layouts  4.67 us (3%)
    pallas_call x7, Pallas kernels, call(): pl.pallas_call(kernel, out_shape=shape, in_specs=[VMEM] * len(operands),...  35.6 us
    ppermute x8, starting transfers between devices, swap(): return lax.ppermute(v, 'c', [(0, 1), (1, 0)])  15.3 us
    all_to_all x1, starting transfers between devices, body(): shares = lax.all_to_all(shares, SP, 0, 0)  11 us
    all_to_all x1, waiting for transfers between devices, body(): got = lax.all_to_all(sent, TP, 0, 0)  6.6 us
    all_to_all x1, starting transfers between devices, body(): got = lax.all_to_all(sent, TP, 0, 0)  6.52 us
    ppermute x1, waiting for transfers between devices, body(): partials.append(lax.ppermute(to_down, 'x', shift(4, -1)))  5.99 us
    ppermute x2, starting transfers between devices, body(): down.append(lax.ppermute(down[-1], 'z', shift(8, -1)))  5.35 us
    all_to_all x1, starting transfers between devices, body(): lax.all_to_all(jnp.broadcast_to(summed[None], (8,) + summed.shape), TP, 0...  5.17 us
  transfers between devices with their start and end apart: 31, of which 8 were waited for; matrix products, arithmetic and copies ran while one was open for 0% of the time, Pallas kernels for 28%

profile of v2, /device:TPU:1, one launch (start us, length us, event | category | flops | bytes accessed | tf_op | source)
XLA Modules:
  0.0 150.5 jit_solution(11701432381905292697)
XLA Ops:
  0.0 3.6 %collective-permute-start.21 = (bf16[256,2048]{1,0:T(8,128)(2,1)}, bf16[256,2048]{1,0:T(8,128)(2,1)S(1)}, u32[]{:S(2)}, u32[]{:S(2)}) collective-permute-start(bf16[256,2048]{1,0:T(8,128)(2,1)} %w0.1), channel_id=1, source_target_pairs={{0,2},{1,7},{2,4},{3,1},{4,6},{5,3},{6,0},{7,5},{8,10},{9,15},{10,... | collective-permute-start | bytes 3145736 | tf_op jit(solution)/shard_map/ppermute | solution.py:390
  3.6 2.7 %collective-permute-start.1 = (bf16[64,2048]{1,0:T(8,128)(2,1)}, bf16[64,2048]{1,0:T(8,128)(2,1)S(1)}, u32[]{:S(2)}, u32[]{:S(2)}) collective-permute-start(bf16[64,2048]{1,0:T(8,128)(2,1)} %lat.1), channel_id=1, source_target_pairs={{0,6},{2,0},{4,2},{6,4},{1,7},{3,1},{5,3},{7,5},{8,14},{10,8},{12,... | collective-permute-start | bytes 786440 | tf_op jit(solution)/shard_map/ppermute | solution.py:335
  6.2 1.9 %share.1 = f32[32,2,768]{2,1,0:T(2,128)} custom-call(f32[1,64]{1,0:T(1,128)} %bitcast.4, f32[1,64]{1,0:T(1,128)} %bitcast.5, f32[64,768]{1,0:T(8,128)} %refs_2_.1), custom_call_target="tpu_custom_call" | custom-call | tf_op jit(solution)/shard_map/share/pallas_call | solution.py:347
  8.1 11.0 %all-to-all-start = ((f32[32,2,768]{2,1,0:T(2,128)}), f32[32,2,768]{2,1,0:T(2,128)S(1)}, u32[]{:S(2)}, u32[]{:S(2)}) async-start(f32[32,2,768]{2,1,0:T(2,128)} %share.1), calls=%async_computation | async-start | bytes 393216 | tf_op jit(solution)/shard_map/all_to_all | solution.py:355
  19.2 2.1 %collective-permute-start.3 = (bf16[64,2048]{1,0:T(8,128)(2,1)}, bf16[64,2048]{1,0:T(8,128)(2,1)S(1)}, u32[]{:S(2)}, u32[]{:S(2)}) collective-permute-start(bf16[64,2048]{1,0:T(8,128)(2,1)} %lat.1), channel_id=1, source_target_pairs={{0,1},{1,0},{2,3},{3,2},{4,5},{5,4},{6,7},{7,6},{8,9},{9,8},{10,11... | collective-permute-start | bytes 786440 | tf_op jit(solution)/shard_map/ppermute | solution.py:340
  21.3 9.2 %collective-permute-start.4 = (bf16[64,2048]{1,0:T(8,128)(2,1)S(1)}, bf16[64,2048]{1,0:T(8,128)(2,1)S(1)}, u32[]{:S(2)}, u32[]{:S(2)}) collective-permute-start(bf16[64,2048]{1,0:T(8,128)(2,1)S(1)} %collective-permute-done.refs_0_), channel_id=1, source_target_pairs={{0,1},{1,0},{2,3},{3,2},{4,5},{5,4},{6,7},{7,6},{8,9},{9,8},{10,11... | collective-permute-start | bytes 786440 | tf_op jit(solution)/shard_map/ppermute | solution.py:340
  31.8 5.2 %all-to-all-start.1 = ((f32[8,2,768]{2,1,0:T(2,128)}), f32[8,2,768]{2,1,0:T(2,128)S(1)}, u32[]{:S(2)}, u32[]{:S(2)}) async-start(f32[8,2,768]{2,1,0:T(2,128)} %broadcast_in_dim.20), calls=%async_computation.1 | async-start | bytes 98304 | tf_op jit(solution)/shard_map/all_to_all | solution.py:358
  37.0 4.8 %all-to-all-done.1.refs_7_.mod = f32[8,2,768]{2,1,0:T(2,128)S(1)} async-done(((f32[8,2,768]{2,1,0:T(2,128)}), f32[8,2,768]{2,1,0:T(2,128)S(1)}, u32[]{:S(2)}, u32[]{:S(2)}) %all-to-all-start.1) | async-done | bytes 49184 | tf_op jit(solution)/shard_map/all_to_all | solution.py:358
  45.1 4.0 %project.1 = (bf16[2,512,128]{2,1,0:T(8,128)(2,1)S(1)}, bf16[528,256]{1,0:T(8,128)(2,1)S(1)}) custom-call(bf16[64,2048]{1,0:T(8,128)(2,1)S(1)} %collective-permute-done.refs_0_, bf16[64,2048]{1,0:T(8,128)(2,1)S(1)} %collective-permute-done.1.refs_1_, bf16[64,2048]{1,0:T(8,128)(2,1)S(1)} %collective-permute-done.2.refs_2_, ...), custom_call_target="tpu_custom_call" | custom-call | flops 1107296256 | bytes 4194304 | tf_op jit(solution)/shard_map/project/pallas_call | solution.py:364
  49.6 2.4 %collective-permute-start.23 = (bf16[256,2048]{1,0:T(8,128)(2,1)S(1)}, bf16[256,2048]{1,0:T(8,128)(2,1)}, u32[]{:S(2)}, u32[]{:S(2)}) collective-permute-start(bf16[256,2048]{1,0:T(8,128)(2,1)S(1)} %collective-permute-done.21.w1), channel_id=1, source_target_pairs={{0,2},{1,7},{2,4},{3,1},{4,6},{5,3},{6,0},{7,5},{8,10},{9,15},{10,... | collective-permute-start | bytes 3145736 | tf_op jit(solution)/shard_map/ppermute | solution.py:392
  52.8 2.4 %collective-permute-start.11 = (bf16[528,256]{1,0:T(8,128)(2,1)S(1)}, bf16[528,256]{1,0:T(8,128)(2,1)S(1)}, u32[]{:S(2)}, u32[]{:S(2)}) collective-permute-start(bf16[528,256]{1,0:T(8,128)(2,1)S(1)} %get-tuple-element.20.kv.refs_8_), channel_id=1, source_target_pairs={{0,224},{32,0},{64,32},{96,64},{128,96},{160,128},{192,160},{224,1... | collective-permute-start | bytes 811016 | tf_op jit(solution)/shard_map/ppermute | solution.py:383
  55.2 2.4 %collective-permute-done.7.q1 = bf16[2,512,128]{2,1,0:T(8,128)(2,1)S(1)} collective-permute-done((bf16[2,512,128]{2,1,0:T(8,128)(2,1)S(1)}, bf16[2,512,128]{2,1,0:T(8,128)(2,1)S(1)}, u32[]{:S(2)}, u32[]{:S(2)}) %collective-permute-start.7) | collective-permute-done | bytes 262176 | tf_op jit(solution)/shard_map/ppermute | solution.py:334
  57.6 4.2 %collective-permute-done.10.up.refs_9_ = bf16[528,256]{1,0:T(8,128)(2,1)S(1)} collective-permute-done((bf16[528,256]{1,0:T(8,128)(2,1)S(1)}, bf16[528,256]{1,0:T(8,128)(2,1)S(1)}, u32[]{:S(2)}, u32[]{:S(2)}) %collective-permute-start.10) | collective-permute-done | bytes 270368 | tf_op jit(solution)/shard_map/ppermute | solution.py:382
  61.8 2.7 %collective-permute-start.13 = (bf16[528,256]{1,0:T(8,128)(2,1)S(1)}, bf16[528,256]{1,0:T(8,128)(2,1)S(1)}, u32[]{:S(2)}, u32[]{:S(2)}) collective-permute-start(bf16[528,256]{1,0:T(8,128)(2,1)S(1)} %collective-permute-done.11.down.refs_12_), channel_id=1, source_target_pairs={{0,224},{32,0},{64,32},{96,64},{128,96},{160,128},{192,160},{224,1... | collective-permute-start | bytes 811016 | tf_op jit(solution)/shard_map/ppermute | solution.py:387
  64.5 2.5 %collective-permute-start.9 = (bf16[2,512,128]{2,1,0:T(8,128)(2,1)S(1)}, bf16[2,512,128]{2,1,0:T(8,128)(2,1)S(1)}, u32[]{:S(2)}, u32[]{:S(2)}) collective-permute-start(bf16[2,512,128]{2,1,0:T(8,128)(2,1)S(1)} %get-tuple-element.19.q.q0), channel_id=1, source_target_pairs={{0,16},{8,24},{16,0},{24,8},{1,17},{9,25},{17,1},{25,9},{2,18},{10... | collective-permute-start | bytes 786440 | tf_op jit(solution)/shard_map/ppermute | solution.py:336
  66.9 3.4 %collective-permute-done.12.up.refs_10_ = bf16[528,256]{1,0:T(8,128)(2,1)S(1)} collective-permute-done((bf16[528,256]{1,0:T(8,128)(2,1)S(1)}, bf16[528,256]{1,0:T(8,128)(2,1)S(1)}, u32[]{:S(2)}, u32[]{:S(2)}) %collective-permute-start.12) | collective-permute-done | bytes 270368 | tf_op jit(solution)/shard_map/ppermute | solution.py:386
  70.3 2.7 %collective-permute-start.15 = (bf16[528,256]{1,0:T(8,128)(2,1)S(1)}, bf16[528,256]{1,0:T(8,128)(2,1)S(1)}, u32[]{:S(2)}, u32[]{:S(2)}) collective-permute-start(bf16[528,256]{1,0:T(8,128)(2,1)S(1)} %collective-permute-done.13.down.refs_13_), channel_id=1, source_target_pairs={{0,224},{32,0},{64,32},{96,64},{128,96},{160,128},{192,160},{224,1... | collective-permute-start | bytes 811016 | tf_op jit(solution)/shard_map/ppermute | solution.py:387
  73.0 3.6 %shard_map.136 = (f32[1024,128]{1,0:T(8,128)S(1)}, f32[1024,128]{1,0:T(8,128)S(1)}, f32[1024,128]{1,0:T(8,128)S(1)}) custom-call(bf16[2,512,128]{2,1,0:T(8,128)(2,1)S(1)} %get-tuple-element.19.q.q0, bf16[528,256]{1,0:T(8,128)(2,1)S(1)} %get-tuple-element.20.kv.refs_8_, bf16[528,256]{1,0:T(8,128)(2,1)S(1)} %collective-permute-done.10.up.refs_9_, ...), custom_call_target="tpu_custom_call" | custom-call | flops 805306368 | bytes 1048576 | tf_op jit(solution)/shard_map/pallas_call | solution.py:298
  76.5 2.3 %collective-permute-start.24 = (bf16[256,2048]{1,0:T(8,128)(2,1)S(1)}, bf16[256,2048]{1,0:T(8,128)(2,1)}, u32[]{:S(2)}, u32[]{:S(2)}) collective-permute-start(bf16[256,2048]{1,0:T(8,128)(2,1)S(1)} %copy-done), channel_id=1, source_target_pairs={{0,1},{1,0},{2,3},{3,2},{4,5},{5,4},{6,7},{7,6},{8,9},{9,8},{10,11... | collective-permute-start | bytes 3145736 | tf_op jit(solution)/shard_map/ppermute | solution.py:340
  78.8 8.4 %shard_map.137 = (bf16[4096,128]{1,0:T(8,128)(2,1)S(1)}, f32[4096,128]{1,0:T(8,128)S(1)}, f32[4096,128]{1,0:T(8,128)S(1)}, f32[4096,128]{1,0:T(8,128)S(1)}) custom-call(bf16[2,512,128]{2,1,0:T(8,128)(2,1)S(1)} %get-tuple-element.19.q.q0, bf16[2,512,128]{2,1,0:T(8,128)(2,1)S(1)} %collective-permute-done.7.q1, ...), custom_call_target="tpu_custom_call" | custom-call | flops 2415919104 | bytes 1048576 | tf_op jit(solution)/shard_map/pallas_call | solution.py:298
  87.3 2.7 %collective-permute-start.17 = (bf16[528,128]{1,0:T(8,128)(2,1)S(1)}, bf16[528,128]{1,0:T(8,128)(2,1)S(1)}, u32[]{:S(2)}, u32[]{:S(2)}) collective-permute-start(bf16[528,128]{1,0:T(8,128)(2,1)S(1)} %slice.9), channel_id=1, source_target_pairs={{0,224},{32,0},{64,32},{96,64},{128,96},{160,128},{192,160},{224,1... | collective-permute-start | bytes 405512 | tf_op jit(solution)/shard_map/ppermute | solution.py:389
  90.1 7.9 %shard_map.138 = (f32[4096,128]{1,0:T(8,128)S(1)}, f32[4096,128]{1,0:T(8,128)S(1)}, f32[4096,128]{1,0:T(8,128)S(1)}) custom-call(bf16[4096,128]{1,0:T(8,128)(2,1)S(1)} %get-tuple-element.24.q_all.refs_0_, f32[4096,128]{1,0:T(8,128)S(1)} %get-tuple-element.25.m_in, ...), custom_call_target="tpu_custom_call", output_to_operand_aliasing={{0}: (1, {}), {1}: (2, {}), {2}: (3, {})} | custom-call | flops 2147483648 | bytes 1048576 | tf_op jit(solution)/shard_map/pallas_call | solution.py:298
  99.2 7.5 %shard_map.140 = (bf16[2,528,128]{2,1,0:T(8,128)(2,1)S(1)}, bf16[2,528,128]{2,1,0:T(8,128)(2,1)S(1)}) custom-call(bf16[4096,128]{1,0:T(8,128)(2,1)S(1)} %get-tuple-element.24.q_all.refs_0_, f32[4096,128]{1,0:T(8,128)S(1)} %get-tuple-element.28.refs_1_, f32[4096,128]{1,0:T(8,128)S(1)} %get-tuple-element.29.refs_2_, ...), custom_call_target="tpu_custom_call" | custom-call | flops 1879048192 | bytes 1048576 | tf_op jit(solution)/shard_map/pallas_call | solution.py:298
  106.7 1.8 %collective-permute-start.19 = (bf16[2,528,128]{2,1,0:T(8,128)(2,1)S(1)}, bf16[2,528,128]{2,1,0:T(8,128)(2,1)S(1)}, u32[]{:S(2)}, u32[]{:S(2)}) collective-permute-start(bf16[2,528,128]{2,1,0:T(8,128)(2,1)S(1)} %get-tuple-element.31), channel_id=1, source_target_pairs={{0,24},{8,0},{16,8},{24,16},{1,25},{9,1},{17,9},{25,17},{2,26},{10... | collective-permute-start | bytes 811016 | tf_op jit(solution)/shard_map/ppermute | solution.py:419
  108.5 6.0 %collective-permute-done.19.p1 = bf16[2,528,128]{2,1,0:T(8,128)(2,1)S(1)} collective-permute-done((bf16[2,528,128]{2,1,0:T(8,128)(2,1)S(1)}, bf16[2,528,128]{2,1,0:T(8,128)(2,1)S(1)}, u32[]{:S(2)}, u32[]{:S(2)}) %collective-permute-start.19) | collective-permute-done | bytes 270368 | tf_op jit(solution)/shard_map/ppermute | solution.py:419
  115.7 3.8 %shard_map.139 = bf16[2,528,128]{2,1,0:T(8,128)(2,1)S(1)} custom-call(bf16[4096,128]{1,0:T(8,128)(2,1)S(1)} %get-tuple-element.24.q_all.refs_0_, f32[4096,128]{1,0:T(8,128)S(1)} %get-tuple-element.28.refs_1_, f32[4096,128]{1,0:T(8,128)S(1)} %get-tuple-element.29.refs_2_, f32[4096,128]{1,0:T(8,128)S(1)} %get-tuple-element.30.refs_3_, ...), custom_call_target="tpu_custom_call" | custom-call | flops 939524096 | bytes 1048576 | tf_op jit(solution)/shard_map/pallas_call | solution.py:298
  119.6 3.6 %collective-permute-done.20.p2 = bf16[2,528,128]{2,1,0:T(8,128)(2,1)S(1)} collective-permute-done((bf16[2,528,128]{2,1,0:T(8,128)(2,1)S(1)}, bf16[2,528,128]{2,1,0:T(8,128)(2,1)S(1)}, u32[]{:S(2)}, u32[]{:S(2)}) %collective-permute-start.20) | collective-permute-done | bytes 270368 | tf_op jit(solution)/shard_map/ppermute | solution.py:420
  123.9 3.8 %shard_map.141.p3 = bf16[2,528,128]{2,1,0:T(8,128)(2,1)S(1)} custom-call(bf16[4096,128]{1,0:T(8,128)(2,1)S(1)} %get-tuple-element.24.q_all.refs_0_, f32[4096,128]{1,0:T(8,128)S(1)} %get-tuple-element.28.refs_1_, f32[4096,128]{1,0:T(8,128)S(1)} %get-tuple-element.29.refs_2_, f32[4096,128]{1,0:T(8,128)S(1)} %get-tuple-element.30.refs_3_, ...), custom_call_target="tpu_custom_call" | custom-call | flops 939524096 | bytes 1048576 | tf_op jit(solution)/shard_map/pallas_call | solution.py:298
  127.7 3.3 %collective-permute-done.18.p0 = bf16[2,528,128]{2,1,0:T(8,128)(2,1)S(1)} collective-permute-done((bf16[2,528,128]{2,1,0:T(8,128)(2,1)S(1)}, bf16[2,528,128]{2,1,0:T(8,128)(2,1)S(1)}, u32[]{:S(2)}, u32[]{:S(2)}) %collective-permute-start.18) | collective-permute-done | bytes 270368 | tf_op jit(solution)/shard_map/ppermute | solution.py:417
  132.3 6.5 %all-to-all-start.2 = ((bf16[8,64,256]{2,1,0:T(8,128)(2,1)}), bf16[8,64,256]{2,1,0:T(8,128)(2,1)}, u32[]{:S(2)}, u32[]{:S(2)}) async-start(bf16[8,64,256]{2,1,0:T(8,128)(2,1)} %copy-done.2), calls=%async_computation.2 | async-start | bytes 524288 | tf_op jit(solution)/shard_map/all_to_all | solution.py:423
  138.8 6.6 %all-to-all-done.2.got = bf16[8,64,256]{2,1,0:T(8,128)(2,1)} async-done(((bf16[8,64,256]{2,1,0:T(8,128)(2,1)}), bf16[8,64,256]{2,1,0:T(8,128)(2,1)}, u32[]{:S(2)}, u32[]{:S(2)}) %all-to-all-start.2) | async-done | bytes 262176 | tf_op jit(solution)/shard_map/all_to_all | solution.py:423
  145.5 5.0 %finish.1 = bf16[64,2048]{1,0:T(8,128)(2,1)} custom-call(bf16[8,64,256]{2,1,0:T(8,128)(2,1)} %all-to-all-done.2.got, bf16[256,2048]{1,0:T(8,128)(2,1)S(1)} %copy-done, bf16[256,2048]{1,0:T(8,128)(2,1)S(1)} %collective-permute-done.21.w1, bf16[256,2048]{1,0:T(8,128)(2,1)S(1)} %collective-permute-done.22.w2, bf16[256,2048]{1,0:T(8,128)(2,1)} %collective-permute-done.23.w3, ...), custom_call_target="tpu_custom_call" | custom-call | flops 536870912 | bytes 10485760 | tf_op jit(solution)/shard_map/finish/pallas_call | solution.py:425
  (58 shorter events, 10.4 us)
Async XLA Ops:
  0.0 49.6 %collective-permute-start.21 = (bf16[256,2048]{1,0:T(8,128)(2,1)}, bf16[256,2048]{1,0:T(8,128)(2,1)S(1)}, u32[]{:S(2)}, u32[]{:S(2)}) collective-permute-start(bf16[256,2048]{1,0:T(8,128)(2,1)} %w0.1), channel_id=1, source_target_pairs={{0,2},{1,7},{2,4},{3,1},{4,6},{5,3},{6,0},{7,5},{8,10},{9,15},{10,... | collective-permute-start | bytes 3145736 | tf_op jit(solution)/shard_map/ppermute | solution.py:390
  3.6 17.8 %collective-permute-start = (bf16[64,2048]{1,0:T(8,128)(2,1)}, bf16[64,2048]{1,0:T(8,128)(2,1)S(1)}, u32[]{:S(2)}, u32[]{:S(2)}) collective-permute-start(bf16[64,2048]{1,0:T(8,128)(2,1)} %lat.1), channel_id=1, source_target_pairs={{0,2},{2,4},{4,6},{6,0},{1,3},{3,5},{5,7},{7,1},{8,10},{10,12},{12... | collective-permute-start | bytes 786440 | tf_op jit(solution)/shard_map/ppermute | solution.py:334
  3.6 27.0 %collective-permute-start.1 = (bf16[64,2048]{1,0:T(8,128)(2,1)}, bf16[64,2048]{1,0:T(8,128)(2,1)S(1)}, u32[]{:S(2)}, u32[]{:S(2)}) collective-permute-start(bf16[64,2048]{1,0:T(8,128)(2,1)} %lat.1), channel_id=1, source_target_pairs={{0,6},{2,0},{4,2},{6,4},{1,7},{3,1},{5,3},{7,5},{8,14},{10,8},{12,... | collective-permute-start | bytes 786440 | tf_op jit(solution)/shard_map/ppermute | solution.py:335
  6.2 24.3 %collective-permute-start.2 = (bf16[64,2048]{1,0:T(8,128)(2,1)}, bf16[64,2048]{1,0:T(8,128)(2,1)S(1)}, u32[]{:S(2)}, u32[]{:S(2)}) collective-permute-start(bf16[64,2048]{1,0:T(8,128)(2,1)} %lat.1), channel_id=1, source_target_pairs={{0,4},{2,6},{4,0},{6,2},{1,5},{3,7},{5,1},{7,3},{8,12},{10,14},{12... | collective-permute-start | bytes 786440 | tf_op jit(solution)/shard_map/ppermute | solution.py:336
  8.1 23.0 %all-to-all-start = ((f32[32,2,768]{2,1,0:T(2,128)}), f32[32,2,768]{2,1,0:T(2,128)S(1)}, u32[]{:S(2)}, u32[]{:S(2)}) async-start(f32[32,2,768]{2,1,0:T(2,128)} %share.1), calls=%async_computation | async-start | bytes 393216 | tf_op jit(solution)/shard_map/all_to_all | solution.py:355
  19.2 17.8 %collective-permute-start.3 = (bf16[64,2048]{1,0:T(8,128)(2,1)}, bf16[64,2048]{1,0:T(8,128)(2,1)S(1)}, u32[]{:S(2)}, u32[]{:S(2)}) collective-permute-start(bf16[64,2048]{1,0:T(8,128)(2,1)} %lat.1), channel_id=1, source_target_pairs={{0,1},{1,0},{2,3},{3,2},{4,5},{5,4},{6,7},{7,6},{8,9},{9,8},{10,11... | collective-permute-start | bytes 786440 | tf_op jit(solution)/shard_map/ppermute | solution.py:340
  21.3 20.4 %collective-permute-start.4 = (bf16[64,2048]{1,0:T(8,128)(2,1)S(1)}, bf16[64,2048]{1,0:T(8,128)(2,1)S(1)}, u32[]{:S(2)}, u32[]{:S(2)}) collective-permute-start(bf16[64,2048]{1,0:T(8,128)(2,1)S(1)} %collective-permute-done.refs_0_), channel_id=1, source_target_pairs={{0,1},{1,0},{2,3},{3,2},{4,5},{5,4},{6,7},{7,6},{8,9},{9,8},{10,11... | collective-permute-start | bytes 786440 | tf_op jit(solution)/shard_map/ppermute | solution.py:340
  30.6 11.2 %collective-permute-start.5 = (bf16[64,2048]{1,0:T(8,128)(2,1)S(1)}, bf16[64,2048]{1,0:T(8,128)(2,1)S(1)}, u32[]{:S(2)}, u32[]{:S(2)}) collective-permute-start(bf16[64,2048]{1,0:T(8,128)(2,1)S(1)} %collective-permute-done.1.refs_1_), channel_id=1, source_target_pairs={{0,1},{1,0},{2,3},{3,2},{4,5},{5,4},{6,7},{7,6},{8,9},{9,8},{10,11... | collective-permute-start | bytes 786440 | tf_op jit(solution)/shard_map/ppermute | solution.py:340
  30.6 11.9 %collective-permute-start.6 = (bf16[64,2048]{1,0:T(8,128)(2,1)S(1)}, bf16[64,2048]{1,0:T(8,128)(2,1)S(1)}, u32[]{:S(2)}, u32[]{:S(2)}) collective-permute-start(bf16[64,2048]{1,0:T(8,128)(2,1)S(1)} %collective-permute-done.2.refs_2_), channel_id=1, source_target_pairs={{0,1},{1,0},{2,3},{3,2},{4,5},{5,4},{6,7},{7,6},{8,9},{9,8},{10,11... | collective-permute-start | bytes 786440 | tf_op jit(solution)/shard_map/ppermute | solution.py:340
  31.8 10.0 %all-to-all-start.1 = ((f32[8,2,768]{2,1,0:T(2,128)}), f32[8,2,768]{2,1,0:T(2,128)S(1)}, u32[]{:S(2)}, u32[]{:S(2)}) async-start(f32[8,2,768]{2,1,0:T(2,128)} %broadcast_in_dim.20), calls=%async_computation.1 | async-start | bytes 98304 | tf_op jit(solution)/shard_map/all_to_all | solution.py:358
  49.1 8.5 %collective-permute-start.7 = (bf16[2,512,128]{2,1,0:T(8,128)(2,1)S(1)}, bf16[2,512,128]{2,1,0:T(8,128)(2,1)S(1)}, u32[]{:S(2)}, u32[]{:S(2)}) collective-permute-start(bf16[2,512,128]{2,1,0:T(8,128)(2,1)S(1)} %get-tuple-element.19.q.q0), channel_id=1, source_target_pairs={{0,8},{8,16},{16,24},{24,0},{1,9},{9,17},{17,25},{25,1},{2,10},{10... | collective-permute-start | bytes 786440 | tf_op jit(solution)/shard_map/ppermute | solution.py:334
  49.2 48.8 %collective-permute-start.22 = (bf16[256,2048]{1,0:T(8,128)(2,1)S(1)}, bf16[256,2048]{1,0:T(8,128)(2,1)S(1)}, u32[]{:S(2)}, u32[]{:S(2)}) collective-permute-start(bf16[256,2048]{1,0:T(8,128)(2,1)S(1)} %copy-done), channel_id=1, source_target_pairs={{2,0},{7,1},{4,2},{1,3},{6,4},{3,5},{0,6},{5,7},{10,8},{15,9},{12,... | collective-permute-start | bytes 3145736 | tf_op jit(solution)/shard_map/ppermute | solution.py:391
  49.6 49.2 %collective-permute-start.23 = (bf16[256,2048]{1,0:T(8,128)(2,1)S(1)}, bf16[256,2048]{1,0:T(8,128)(2,1)}, u32[]{:S(2)}, u32[]{:S(2)}) collective-permute-start(bf16[256,2048]{1,0:T(8,128)(2,1)S(1)} %collective-permute-done.21.w1), channel_id=1, source_target_pairs={{0,2},{1,7},{2,4},{3,1},{4,6},{5,3},{6,0},{7,5},{8,10},{9,15},{10,... | collective-permute-start | bytes 3145736 | tf_op jit(solution)/shard_map/ppermute | solution.py:392
  52.0 9.8 %collective-permute-start.10 = (bf16[528,256]{1,0:T(8,128)(2,1)S(1)}, bf16[528,256]{1,0:T(8,128)(2,1)S(1)}, u32[]{:S(2)}, u32[]{:S(2)}) collective-permute-start(bf16[528,256]{1,0:T(8,128)(2,1)S(1)} %get-tuple-element.20.kv.refs_8_), channel_id=1, source_target_pairs={{0,32},{32,64},{64,96},{96,128},{128,160},{160,192},{192,224},{224... | collective-permute-start | bytes 811016 | tf_op jit(solution)/shard_map/ppermute | solution.py:382
  52.8 9.0 %collective-permute-start.11 = (bf16[528,256]{1,0:T(8,128)(2,1)S(1)}, bf16[528,256]{1,0:T(8,128)(2,1)S(1)}, u32[]{:S(2)}, u32[]{:S(2)}) collective-permute-start(bf16[528,256]{1,0:T(8,128)(2,1)S(1)} %get-tuple-element.20.kv.refs_8_), channel_id=1, source_target_pairs={{0,224},{32,0},{64,32},{96,64},{128,96},{160,128},{192,160},{224,1... | collective-permute-start | bytes 811016 | tf_op jit(solution)/shard_map/ppermute | solution.py:383
  57.6 6.8 %collective-permute-start.8 = (bf16[2,512,128]{2,1,0:T(8,128)(2,1)S(1)}, bf16[2,512,128]{2,1,0:T(8,128)(2,1)S(1)}, u32[]{:S(2)}, u32[]{:S(2)}) collective-permute-start(bf16[2,512,128]{2,1,0:T(8,128)(2,1)S(1)} %get-tuple-element.19.q.q0), channel_id=1, source_target_pairs={{0,24},{8,0},{16,8},{24,16},{1,25},{9,1},{17,9},{25,17},{2,26},{10... | collective-permute-start | bytes 786440 | tf_op jit(solution)/shard_map/ppermute | solution.py:335
  61.8 8.5 %collective-permute-start.12 = (bf16[528,256]{1,0:T(8,128)(2,1)S(1)}, bf16[528,256]{1,0:T(8,128)(2,1)S(1)}, u32[]{:S(2)}, u32[]{:S(2)}) collective-permute-start(bf16[528,256]{1,0:T(8,128)(2,1)S(1)} %collective-permute-done.10.up.refs_9_), channel_id=1, source_target_pairs={{0,32},{32,64},{64,96},{96,128},{128,160},{160,192},{192,224},{224... | collective-permute-start | bytes 811016 | tf_op jit(solution)/shard_map/ppermute | solution.py:386
  61.8 8.5 %collective-permute-start.13 = (bf16[528,256]{1,0:T(8,128)(2,1)S(1)}, bf16[528,256]{1,0:T(8,128)(2,1)S(1)}, u32[]{:S(2)}, u32[]{:S(2)}) collective-permute-start(bf16[528,256]{1,0:T(8,128)(2,1)S(1)} %collective-permute-done.11.down.refs_12_), channel_id=1, source_target_pairs={{0,224},{32,0},{64,32},{96,64},{128,96},{160,128},{192,160},{224,1... | collective-permute-start | bytes 811016 | tf_op jit(solution)/shard_map/ppermute | solution.py:387
  64.5 12.1 %collective-permute-start.9 = (bf16[2,512,128]{2,1,0:T(8,128)(2,1)S(1)}, bf16[2,512,128]{2,1,0:T(8,128)(2,1)S(1)}, u32[]{:S(2)}, u32[]{:S(2)}) collective-permute-start(bf16[2,512,128]{2,1,0:T(8,128)(2,1)S(1)} %get-tuple-element.19.q.q0), channel_id=1, source_target_pairs={{0,16},{8,24},{16,0},{24,8},{1,17},{9,25},{17,1},{25,9},{2,18},{10... | collective-permute-start | bytes 786440 | tf_op jit(solution)/shard_map/ppermute | solution.py:336
  70.3 16.9 %collective-permute-start.14 = (bf16[528,256]{1,0:T(8,128)(2,1)S(1)}, bf16[528,256]{1,0:T(8,128)(2,1)S(1)}, u32[]{:S(2)}, u32[]{:S(2)}) collective-permute-start(bf16[528,256]{1,0:T(8,128)(2,1)S(1)} %collective-permute-done.12.up.refs_10_), channel_id=1, source_target_pairs={{0,32},{32,64},{64,96},{96,128},{128,160},{160,192},{192,224},{224... | collective-permute-start | bytes 811016 | tf_op jit(solution)/shard_map/ppermute | solution.py:386
  70.3 17.0 %collective-permute-start.15 = (bf16[528,256]{1,0:T(8,128)(2,1)S(1)}, bf16[528,256]{1,0:T(8,128)(2,1)S(1)}, u32[]{:S(2)}, u32[]{:S(2)}) collective-permute-start(bf16[528,256]{1,0:T(8,128)(2,1)S(1)} %collective-permute-done.13.down.refs_13_), channel_id=1, source_target_pairs={{0,224},{32,0},{64,32},{96,64},{128,96},{160,128},{192,160},{224,1... | collective-permute-start | bytes 811016 | tf_op jit(solution)/shard_map/ppermute | solution.py:387
  76.5 62.3 %collective-permute-start.24 = (bf16[256,2048]{1,0:T(8,128)(2,1)S(1)}, bf16[256,2048]{1,0:T(8,128)(2,1)}, u32[]{:S(2)}, u32[]{:S(2)}) collective-permute-start(bf16[256,2048]{1,0:T(8,128)(2,1)S(1)} %copy-done), channel_id=1, source_target_pairs={{0,1},{1,0},{2,3},{3,2},{4,5},{5,4},{6,7},{7,6},{8,9},{9,8},{10,11... | collective-permute-start | bytes 3145736 | tf_op jit(solution)/shard_map/ppermute | solution.py:340
  87.2 11.5 %collective-permute-start.16 = (bf16[528,128]{1,0:T(8,128)(2,1)S(1)}, bf16[528,128]{1,0:T(8,128)(2,1)S(1)}, u32[]{:S(2)}, u32[]{:S(2)}) collective-permute-start(bf16[528,128]{1,0:T(8,128)(2,1)S(1)} %slice.8), channel_id=1, source_target_pairs={{0,32},{32,64},{64,96},{96,128},{128,160},{160,192},{192,224},{224... | collective-permute-start | bytes 405512 | tf_op jit(solution)/shard_map/ppermute | solution.py:388
  87.3 11.9 %collective-permute-start.17 = (bf16[528,128]{1,0:T(8,128)(2,1)S(1)}, bf16[528,128]{1,0:T(8,128)(2,1)S(1)}, u32[]{:S(2)}, u32[]{:S(2)}) collective-permute-start(bf16[528,128]{1,0:T(8,128)(2,1)S(1)} %slice.9), channel_id=1, source_target_pairs={{0,224},{32,0},{64,32},{96,64},{128,96},{160,128},{192,160},{224,1... | collective-permute-start | bytes 405512 | tf_op jit(solution)/shard_map/ppermute | solution.py:389
  98.0 47.4 %collective-permute-start.25 = (bf16[256,2048]{1,0:T(8,128)(2,1)S(1)}, bf16[256,2048]{1,0:T(8,128)(2,1)}, u32[]{:S(2)}, u32[]{:S(2)}) collective-permute-start(bf16[256,2048]{1,0:T(8,128)(2,1)S(1)} %collective-permute-done.21.w1), channel_id=1, source_target_pairs={{0,1},{1,0},{2,3},{3,2},{4,5},{5,4},{6,7},{7,6},{8,9},{9,8},{10,11... | collective-permute-start | bytes 3145736 | tf_op jit(solution)/shard_map/ppermute | solution.py:340
  98.7 46.7 %collective-permute-start.26 = (bf16[256,2048]{1,0:T(8,128)(2,1)S(1)}, bf16[256,2048]{1,0:T(8,128)(2,1)}, u32[]{:S(2)}, u32[]{:S(2)}) collective-permute-start(bf16[256,2048]{1,0:T(8,128)(2,1)S(1)} %collective-permute-done.22.w2), channel_id=1, source_target_pairs={{0,1},{1,0},{2,3},{3,2},{4,5},{5,4},{6,7},{7,6},{8,9},{9,8},{10,11... | collective-permute-start | bytes 3145736 | tf_op jit(solution)/shard_map/ppermute | solution.py:340
  98.8 46.6 %collective-permute-start.27 = (bf16[256,2048]{1,0:T(8,128)(2,1)}, bf16[256,2048]{1,0:T(8,128)(2,1)}, u32[]{:S(2)}, u32[]{:S(2)}) collective-permute-start(bf16[256,2048]{1,0:T(8,128)(2,1)} %collective-permute-done.23.w3), channel_id=1, source_target_pairs={{0,1},{1,0},{2,3},{3,2},{4,5},{5,4},{6,7},{7,6},{8,9},{9,8},{10,11... | collective-permute-start | bytes 3145736 | tf_op jit(solution)/shard_map/ppermute | solution.py:340
  106.7 7.8 %collective-permute-start.19 = (bf16[2,528,128]{2,1,0:T(8,128)(2,1)S(1)}, bf16[2,528,128]{2,1,0:T(8,128)(2,1)S(1)}, u32[]{:S(2)}, u32[]{:S(2)}) collective-permute-start(bf16[2,528,128]{2,1,0:T(8,128)(2,1)S(1)} %get-tuple-element.31), channel_id=1, source_target_pairs={{0,24},{8,0},{16,8},{24,16},{1,25},{9,1},{17,9},{25,17},{2,26},{10... | collective-permute-start | bytes 811016 | tf_op jit(solution)/shard_map/ppermute | solution.py:419
  114.5 8.6 %collective-permute-start.20 = (bf16[2,528,128]{2,1,0:T(8,128)(2,1)S(1)}, bf16[2,528,128]{2,1,0:T(8,128)(2,1)S(1)}, u32[]{:S(2)}, u32[]{:S(2)}) collective-permute-start(bf16[2,528,128]{2,1,0:T(8,128)(2,1)S(1)} %get-tuple-element.32), channel_id=1, source_target_pairs={{0,8},{8,16},{16,24},{24,0},{1,9},{9,17},{17,25},{25,1},{2,10},{10... | collective-permute-start | bytes 811016 | tf_op jit(solution)/shard_map/ppermute | solution.py:420
  119.5 25.9 %copy-start.1 = (bf16[64,2048]{1,0:T(8,128)(2,1)S(1)}, bf16[64,2048]{1,0:T(8,128)(2,1)}, u32[]{:S(2)}) copy-start(bf16[64,2048]{1,0:T(8,128)(2,1)} %lat.1) | copy-start | bytes 786436
  123.2 7.8 %collective-permute-start.18 = (bf16[2,528,128]{2,1,0:T(8,128)(2,1)S(1)}, bf16[2,528,128]{2,1,0:T(8,128)(2,1)S(1)}, u32[]{:S(2)}, u32[]{:S(2)}) collective-permute-start(bf16[2,528,128]{2,1,0:T(8,128)(2,1)S(1)} %shard_map.139), channel_id=1, source_target_pairs={{0,16},{8,24},{16,0},{24,8},{1,17},{9,25},{17,1},{25,9},{2,18},{10... | collective-permute-start | bytes 811016 | tf_op jit(solution)/shard_map/ppermute | solution.py:417
  132.3 13.1 %all-to-all-start.2 = ((bf16[8,64,256]{2,1,0:T(8,128)(2,1)}), bf16[8,64,256]{2,1,0:T(8,128)(2,1)}, u32[]{:S(2)}, u32[]{:S(2)}) async-start(bf16[8,64,256]{2,1,0:T(8,128)(2,1)} %copy-done.2), calls=%async_computation.2 | async-start | bytes 524288 | tf_op jit(solution)/shard_map/all_to_all | solution.py:423
  (6 other events, 8.1 us)

commit v3 on v2

--- a/solution.py
+++ b/solution.py
@@ -389,9 +389,8 @@
     v_far = lax.ppermute(down[3][:, HD:], "z", shift(8, -1))
     first = lax.ppermute(out_weight, TP, ahead)
     second = lax.ppermute(out_weight, TP, behind)
-    weights = [out_weight, first, second, lax.ppermute(first, TP, ahead)]
-    weights += [swap(out_weight), swap(first), swap(second)]
-    weights.append(swap(weights[3]))
+    weights = [out_weight, first, second, lax.ppermute(out_weight, "y", shift(4, 2))]
+    weights += [swap(v) for v in weights]
 
     rows = 8 * CHUNK
     state_of = lambda n: [pltpu.VMEM((n, HD), F32)] * 3

time: 151 us -> 160 us (1.060)
  waiting for transfers between devices: 34.3 us -> 52.3 us
  starting transfers between devices: 64.7 us -> 59.3 us
  local copies, waits for them, and re-layouts: 4.67 us -> 1.37 us
    all_to_all x1, waiting for transfers between devices: 0.01 us -> 7.36 us  [body(): shares = lax.all_to_all(shares, SP, 0, 0)]
    ppermute x2, waiting for transfers between devices: 0.01 us -> 3.4 us  [over_four(): lax.ppermute(v, axis, shift(4, 2))]
    unnamed x14 -> x6, local copies, waits for them, and re-layouts: 4.01 us -> 0.71 us
    ppermute x1, starting transfers between devices: 3.55 us -> 0.87 us  [body(): first = lax.ppermute(out_weight, TP, ahead)]
    ppermute x1, waiting for transfers between devices: 0.01 us -> 2.51 us  [body(): down.append(lax.ppermute(kv, 'z', shift(8, -1)))]
    ppermute x2, waiting for transfers between devices: 2.41 us -> 4.75 us  [over_four(): lax.ppermute(v, axis, shift(4, 1))]
    ppermute x2, starting transfers between devices: 0.09 us -> 2.2 us  [over_four(): lax.ppermute(v, axis, shift(4, 1))]
    ppermute x1, starting transfers between devices: 2.39 us -> 0.45 us  [body(): down.append(lax.ppermute(kv, 'z', shift(8, -1)))]
  transfers between devices with their start and end apart: 31 -> 31, of which waited for: 8 -> 12; matrix products, arithmetic and copies ran while one was open for 0% -> 0% of each run, Pallas kernels for 28% -> 23%
where the time goes in v3:
time: 160 us
  starting transfers between devices  59.3 us (37%)
  waiting for transfers between devices  52.3 us (33%)
  Pallas kernels  46.5 us (29%)
    pallas_call x7, Pallas kernels, call(): pl.pallas_call(kernel, out_shape=shape, in_specs=[VMEM] * len(operands),...  35.6 us
    ppermute x8, starting transfers between devices, swap(): return lax.ppermute(v, 'c', [(0, 1), (1, 0)])  14.4 us
    all_to_all x1, starting transfers between devices, body(): shares = lax.all_to_all(shares, SP, 0, 0)  11 us
    all_to_all x1, waiting for transfers between devices, body(): shares = lax.all_to_all(shares, SP, 0, 0)  7.36 us
    all_to_all x1, waiting for transfers between devices, body(): got = lax.all_to_all(sent, TP, 0, 0)  6.6 us
    all_to_all x1, starting transfers between devices, body(): got = lax.all_to_all(sent, TP, 0, 0)  6.53 us
    all_to_all x1, starting transfers between devices, body(): lax.all_to_all(jnp.broadcast_to(summed[None], (8,) + summed.shape), TP, 0...  6.4 us
    ppermute x1, waiting for transfers between devices, body(): partials.append(lax.ppermute(to_down, 'x', shift(4, -1)))  6.22 us
  transfers between devices with their start and end apart: 31, of which 12 were waited for; matrix products, arithmetic and copies ran while one was open for 0% of the time, Pallas kernels for 23%

profile of v3, /device:TPU:1, one launch (start us, length us, event | category | flops | bytes accessed | tf_op | source)
XLA Modules:
  0.0 159.7 jit_solution(12593337597868810200)
XLA Ops:
  0.0 2.1 %collective-permute-start = (bf16[64,2048]{1,0:T(8,128)(2,1)}, bf16[64,2048]{1,0:T(8,128)(2,1)S(1)}, u32[]{:S(2)}, u32[]{:S(2)}) collective-permute-start(bf16[64,2048]{1,0:T(8,128)(2,1)} %lat.1), channel_id=1, source_target_pairs={{0,2},{2,4},{4,6},{6,0},{1,3},{3,5},{5,7},{7,1},{8,10},{10,12},{12... | collective-permute-start | bytes 786440 | tf_op jit(solution)/shard_map/ppermute | solution.py:334
  3.6 1.6 %collective-permute-start.2 = (bf16[64,2048]{1,0:T(8,128)(2,1)}, bf16[64,2048]{1,0:T(8,128)(2,1)S(1)}, u32[]{:S(2)}, u32[]{:S(2)}) collective-permute-start(bf16[64,2048]{1,0:T(8,128)(2,1)} %lat.1), channel_id=1, source_target_pairs={{0,4},{2,6},{4,0},{6,2},{1,5},{3,7},{5,1},{7,3},{8,12},{10,14},{12... | collective-permute-start | bytes 786440 | tf_op jit(solution)/shard_map/ppermute | solution.py:336
  5.2 1.9 %share.1 = f32[32,2,768]{2,1,0:T(2,128)} custom-call(f32[1,64]{1,0:T(1,128)} %bitcast.4, f32[1,64]{1,0:T(1,128)} %bitcast.5, f32[64,768]{1,0:T(8,128)} %refs_2_.1), custom_call_target="tpu_custom_call" | custom-call | tf_op jit(solution)/shard_map/share/pallas_call | solution.py:347
  7.1 11.0 %all-to-all-start = ((f32[32,2,768]{2,1,0:T(2,128)}), f32[32,2,768]{2,1,0:T(2,128)S(1)}, u32[]{:S(2)}, u32[]{:S(2)}) async-start(f32[32,2,768]{2,1,0:T(2,128)} %share.1), calls=%async_computation | async-start | bytes 393216 | tf_op jit(solution)/shard_map/all_to_all | solution.py:355
  18.1 1.9 %collective-permute-start.3 = (bf16[64,2048]{1,0:T(8,128)(2,1)}, bf16[64,2048]{1,0:T(8,128)(2,1)S(1)}, u32[]{:S(2)}, u32[]{:S(2)}) collective-permute-start(bf16[64,2048]{1,0:T(8,128)(2,1)} %lat.1), channel_id=1, source_target_pairs={{0,1},{1,0},{2,3},{3,2},{4,5},{5,4},{6,7},{7,6},{8,9},{9,8},{10,11... | collective-permute-start | bytes 786440 | tf_op jit(solution)/shard_map/ppermute | solution.py:340
  20.7 7.4 %all-to-all-done = f32[32,2,768]{2,1,0:T(2,128)S(1)} async-done(((f32[32,2,768]{2,1,0:T(2,128)}), f32[32,2,768]{2,1,0:T(2,128)S(1)}, u32[]{:S(2)}, u32[]{:S(2)}) %all-to-all-start) | async-done | bytes 196640 | tf_op jit(solution)/shard_map/all_to_all | solution.py:355
  28.7 6.4 %all-to-all-start.1 = ((f32[8,2,768]{2,1,0:T(2,128)}), f32[8,2,768]{2,1,0:T(2,128)S(1)}, u32[]{:S(2)}, u32[]{:S(2)}) async-start(f32[8,2,768]{2,1,0:T(2,128)} %broadcast_in_dim.20), calls=%async_computation.1 | async-start | bytes 98304 | tf_op jit(solution)/shard_map/all_to_all | solution.py:358
  35.1 4.8 %all-to-all-done.1.refs_7_.mod = f32[8,2,768]{2,1,0:T(2,128)S(1)} async-done(((f32[8,2,768]{2,1,0:T(2,128)}), f32[8,2,768]{2,1,0:T(2,128)S(1)}, u32[]{:S(2)}, u32[]{:S(2)}) %all-to-all-start.1) | async-done | bytes 49184 | tf_op jit(solution)/shard_map/all_to_all | solution.py:358
  40.0 4.0 %project.1 = (bf16[2,512,128]{2,1,0:T(8,128)(2,1)S(1)}, bf16[528,256]{1,0:T(8,128)(2,1)S(1)}) custom-call(bf16[64,2048]{1,0:T(8,128)(2,1)S(1)} %collective-permute-done.refs_0_, bf16[64,2048]{1,0:T(8,128)(2,1)S(1)} %collective-permute-done.1.refs_1_, bf16[64,2048]{1,0:T(8,128)(2,1)S(1)} %collective-permute-done.2.refs_2_, ...), custom_call_target="tpu_custom_call" | custom-call | flops 1107296256 | bytes 4194304 | tf_op jit(solution)/shard_map/project/pallas_call | solution.py:364
  44.1 2.7 %collective-permute-start.8 = (bf16[2,512,128]{2,1,0:T(8,128)(2,1)S(1)}, bf16[2,512,128]{2,1,0:T(8,128)(2,1)S(1)}, u32[]{:S(2)}, u32[]{:S(2)}) collective-permute-start(bf16[2,512,128]{2,1,0:T(8,128)(2,1)S(1)} %get-tuple-element.19.q.q0), channel_id=1, source_target_pairs={{0,24},{8,0},{16,8},{24,16},{1,25},{9,1},{17,9},{25,17},{2,26},{10... | collective-permute-start | bytes 786440 | tf_op jit(solution)/shard_map/ppermute | solution.py:335
  48.2 4.7 %collective-permute-done.7.q1 = bf16[2,512,128]{2,1,0:T(8,128)(2,1)S(1)} collective-permute-done((bf16[2,512,128]{2,1,0:T(8,128)(2,1)S(1)}, bf16[2,512,128]{2,1,0:T(8,128)(2,1)S(1)}, u32[]{:S(2)}, u32[]{:S(2)}) %collective-permute-start.7) | collective-permute-done | bytes 262176 | tf_op jit(solution)/shard_map/ppermute | solution.py:334
  54.1 3.4 %collective-permute-done.9.q3 = bf16[2,512,128]{2,1,0:T(8,128)(2,1)S(1)} collective-permute-done((bf16[2,512,128]{2,1,0:T(8,128)(2,1)S(1)}, bf16[2,512,128]{2,1,0:T(8,128)(2,1)S(1)}, u32[]{:S(2)}, u32[]{:S(2)}) %collective-permute-start.9) | collective-permute-done | bytes 262176 | tf_op jit(solution)/shard_map/ppermute | solution.py:336
  57.9 2.6 %collective-permute-done.10.up.refs_9_ = bf16[528,256]{1,0:T(8,128)(2,1)S(1)} collective-permute-done((bf16[528,256]{1,0:T(8,128)(2,1)S(1)}, bf16[528,256]{1,0:T(8,128)(2,1)S(1)}, u32[]{:S(2)}, u32[]{:S(2)}) %collective-permute-start.10) | collective-permute-done | bytes 270368 | tf_op jit(solution)/shard_map/ppermute | solution.py:382
  60.6 2.5 %collective-permute-done.11.down.refs_12_ = bf16[528,256]{1,0:T(8,128)(2,1)S(1)} collective-permute-done((bf16[528,256]{1,0:T(8,128)(2,1)S(1)}, bf16[528,256]{1,0:T(8,128)(2,1)S(1)}, u32[]{:S(2)}, u32[]{:S(2)}) %collective-permute-start.11) | collective-permute-done | bytes 270368 | tf_op jit(solution)/shard_map/ppermute | solution.py:383
  63.1 1.7 %collective-permute-start.13 = (bf16[528,256]{1,0:T(8,128)(2,1)S(1)}, bf16[528,256]{1,0:T(8,128)(2,1)S(1)}, u32[]{:S(2)}, u32[]{:S(2)}) collective-permute-start(bf16[528,256]{1,0:T(8,128)(2,1)S(1)} %collective-permute-done.11.down.refs_12_), channel_id=1, source_target_pairs={{0,224},{32,0},{64,32},{96,64},{128,96},{160,128},{192,160},{224,1... | collective-permute-start | bytes 811016 | tf_op jit(solution)/shard_map/ppermute | solution.py:387
  64.8 5.0 %collective-permute-done.12.up.refs_10_ = bf16[528,256]{1,0:T(8,128)(2,1)S(1)} collective-permute-done((bf16[528,256]{1,0:T(8,128)(2,1)S(1)}, bf16[528,256]{1,0:T(8,128)(2,1)S(1)}, u32[]{:S(2)}, u32[]{:S(2)}) %collective-permute-start.12) | collective-permute-done | bytes 270368 | tf_op jit(solution)/shard_map/ppermute | solution.py:386
  70.4 3.4 %collective-permute-start.15 = (bf16[528,256]{1,0:T(8,128)(2,1)S(1)}, bf16[528,256]{1,0:T(8,128)(2,1)S(1)}, u32[]{:S(2)}, u32[]{:S(2)}) collective-permute-start(bf16[528,256]{1,0:T(8,128)(2,1)S(1)} %collective-permute-done.13.down.refs_13_), channel_id=1, source_target_pairs={{0,224},{32,0},{64,32},{96,64},{128,96},{160,128},{192,160},{224,1... | collective-permute-start | bytes 811016 | tf_op jit(solution)/shard_map/ppermute | solution.py:387
  73.8 3.6 %shard_map.136 = (f32[1024,128]{1,0:T(8,128)S(1)}, f32[1024,128]{1,0:T(8,128)S(1)}, f32[1024,128]{1,0:T(8,128)S(1)}) custom-call(bf16[2,512,128]{2,1,0:T(8,128)(2,1)S(1)} %get-tuple-element.19.q.q0, bf16[528,256]{1,0:T(8,128)(2,1)S(1)} %get-tuple-element.20.kv.refs_8_, bf16[528,256]{1,0:T(8,128)(2,1)S(1)} %collective-permute-done.10.up.refs_9_, ...), custom_call_target="tpu_custom_call" | custom-call | flops 805306368 | bytes 1048576 | tf_op jit(solution)/shard_map/pallas_call | solution.py:298
  77.4 8.4 %shard_map.137 = (bf16[4096,128]{1,0:T(8,128)(2,1)S(1)}, f32[4096,128]{1,0:T(8,128)S(1)}, f32[4096,128]{1,0:T(8,128)S(1)}, f32[4096,128]{1,0:T(8,128)S(1)}) custom-call(bf16[2,512,128]{2,1,0:T(8,128)(2,1)S(1)} %get-tuple-element.19.q.q0, bf16[2,512,128]{2,1,0:T(8,128)(2,1)S(1)} %collective-permute-done.7.q1, ...), custom_call_target="tpu_custom_call" | custom-call | flops 2415919104 | bytes 1048576 | tf_op jit(solution)/shard_map/pallas_call | solution.py:298
  85.9 2.7 %collective-permute-start.17 = (bf16[528,128]{1,0:T(8,128)(2,1)S(1)}, bf16[528,128]{1,0:T(8,128)(2,1)S(1)}, u32[]{:S(2)}, u32[]{:S(2)}) collective-permute-start(bf16[528,128]{1,0:T(8,128)(2,1)S(1)} %slice.9), channel_id=1, source_target_pairs={{0,224},{32,0},{64,32},{96,64},{128,96},{160,128},{192,160},{224,1... | collective-permute-start | bytes 405512 | tf_op jit(solution)/shard_map/ppermute | solution.py:389
  88.7 7.9 %shard_map.138 = (f32[4096,128]{1,0:T(8,128)S(1)}, f32[4096,128]{1,0:T(8,128)S(1)}, f32[4096,128]{1,0:T(8,128)S(1)}) custom-call(bf16[4096,128]{1,0:T(8,128)(2,1)S(1)} %get-tuple-element.24.q_all.refs_0_, f32[4096,128]{1,0:T(8,128)S(1)} %get-tuple-element.25.m_in, ...), custom_call_target="tpu_custom_call", output_to_operand_aliasing={{0}: (1, {}), {1}: (2, {}), {2}: (3, {})} | custom-call | flops 2147483648 | bytes 1048576 | tf_op jit(solution)/shard_map/pallas_call | solution.py:298
  96.6 11.0 %collective-permute-start.24 = (bf16[256,2048]{1,0:T(8,128)(2,1)S(1)}, bf16[256,2048]{1,0:T(8,128)(2,1)}, u32[]{:S(2)}, u32[]{:S(2)}) collective-permute-start(bf16[256,2048]{1,0:T(8,128)(2,1)S(1)} %copy-done), channel_id=1, source_target_pairs={{0,1},{1,0},{2,3},{3,2},{4,5},{5,4},{6,7},{7,6},{8,9},{9,8},{10,11... | collective-permute-start | bytes 3145736 | tf_op jit(solution)/shard_map/ppermute | solution.py:340
  108.5 7.5 %shard_map.140 = (bf16[2,528,128]{2,1,0:T(8,128)(2,1)S(1)}, bf16[2,528,128]{2,1,0:T(8,128)(2,1)S(1)}) custom-call(bf16[4096,128]{1,0:T(8,128)(2,1)S(1)} %get-tuple-element.24.q_all.refs_0_, f32[4096,128]{1,0:T(8,128)S(1)} %get-tuple-element.28.refs_1_, f32[4096,128]{1,0:T(8,128)S(1)} %get-tuple-element.29.refs_2_, ...), custom_call_target="tpu_custom_call" | custom-call | flops 1879048192 | bytes 1048576 | tf_op jit(solution)/shard_map/pallas_call | solution.py:298
  116.0 1.7 %collective-permute-start.19 = (bf16[2,528,128]{2,1,0:T(8,128)(2,1)S(1)}, bf16[2,528,128]{2,1,0:T(8,128)(2,1)S(1)}, u32[]{:S(2)}, u32[]{:S(2)}) collective-permute-start(bf16[2,528,128]{2,1,0:T(8,128)(2,1)S(1)} %get-tuple-element.31), channel_id=1, source_target_pairs={{0,24},{8,0},{16,8},{24,16},{1,25},{9,1},{17,9},{25,17},{2,26},{10... | collective-permute-start | bytes 811016 | tf_op jit(solution)/shard_map/ppermute | solution.py:418
  117.7 6.2 %collective-permute-done.19.p1 = bf16[2,528,128]{2,1,0:T(8,128)(2,1)S(1)} collective-permute-done((bf16[2,528,128]{2,1,0:T(8,128)(2,1)S(1)}, bf16[2,528,128]{2,1,0:T(8,128)(2,1)S(1)}, u32[]{:S(2)}, u32[]{:S(2)}) %collective-permute-start.19) | collective-permute-done | bytes 270368 | tf_op jit(solution)/shard_map/ppermute | solution.py:418
  123.9 3.8 %shard_map.139 = bf16[2,528,128]{2,1,0:T(8,128)(2,1)S(1)} custom-call(bf16[4096,128]{1,0:T(8,128)(2,1)S(1)} %get-tuple-element.24.q_all.refs_0_, f32[4096,128]{1,0:T(8,128)S(1)} %get-tuple-element.28.refs_1_, f32[4096,128]{1,0:T(8,128)S(1)} %get-tuple-element.29.refs_2_, f32[4096,128]{1,0:T(8,128)S(1)} %get-tuple-element.30.refs_3_, ...), custom_call_target="tpu_custom_call" | custom-call | flops 939524096 | bytes 1048576 | tf_op jit(solution)/shard_map/pallas_call | solution.py:298
  127.8 4.7 %collective-permute-done.20.p2 = bf16[2,528,128]{2,1,0:T(8,128)(2,1)S(1)} collective-permute-done((bf16[2,528,128]{2,1,0:T(8,128)(2,1)S(1)}, bf16[2,528,128]{2,1,0:T(8,128)(2,1)S(1)}, u32[]{:S(2)}, u32[]{:S(2)}) %collective-permute-start.20) | collective-permute-done | bytes 270368 | tf_op jit(solution)/shard_map/ppermute | solution.py:419
  132.8 3.8 %shard_map.141.p3 = bf16[2,528,128]{2,1,0:T(8,128)(2,1)S(1)} custom-call(bf16[4096,128]{1,0:T(8,128)(2,1)S(1)} %get-tuple-element.24.q_all.refs_0_, f32[4096,128]{1,0:T(8,128)S(1)} %get-tuple-element.28.refs_1_, f32[4096,128]{1,0:T(8,128)S(1)} %get-tuple-element.29.refs_2_, f32[4096,128]{1,0:T(8,128)S(1)} %get-tuple-element.30.refs_3_, ...), custom_call_target="tpu_custom_call" | custom-call | flops 939524096 | bytes 1048576 | tf_op jit(solution)/shard_map/pallas_call | solution.py:298
  136.6 3.6 %collective-permute-done.18.p0 = bf16[2,528,128]{2,1,0:T(8,128)(2,1)S(1)} collective-permute-done((bf16[2,528,128]{2,1,0:T(8,128)(2,1)S(1)}, bf16[2,528,128]{2,1,0:T(8,128)(2,1)S(1)}, u32[]{:S(2)}, u32[]{:S(2)}) %collective-permute-start.18) | collective-permute-done | bytes 270368 | tf_op jit(solution)/shard_map/ppermute | solution.py:416
  141.6 6.5 %all-to-all-start.2 = ((bf16[8,64,256]{2,1,0:T(8,128)(2,1)}), bf16[8,64,256]{2,1,0:T(8,128)(2,1)}, u32[]{:S(2)}, u32[]{:S(2)}) async-start(bf16[8,64,256]{2,1,0:T(8,128)(2,1)} %copy-done.2), calls=%async_computation.2 | async-start | bytes 524288 | tf_op jit(solution)/shard_map/all_to_all | solution.py:422
  148.1 6.6 %all-to-all-done.2.got = bf16[8,64,256]{2,1,0:T(8,128)(2,1)} async-done(((bf16[8,64,256]{2,1,0:T(8,128)(2,1)}), bf16[8,64,256]{2,1,0:T(8,128)(2,1)}, u32[]{:S(2)}, u32[]{:S(2)}) %all-to-all-start.2) | async-done | bytes 262176 | tf_op jit(solution)/shard_map/all_to_all | solution.py:422
  154.7 5.0 %finish.1 = bf16[64,2048]{1,0:T(8,128)(2,1)} custom-call(bf16[8,64,256]{2,1,0:T(8,128)(2,1)} %all-to-all-done.2.got, bf16[256,2048]{1,0:T(8,128)(2,1)S(1)} %copy-done, bf16[256,2048]{1,0:T(8,128)(2,1)S(1)} %collective-permute-done.21.w1, bf16[256,2048]{1,0:T(8,128)(2,1)S(1)} %collective-permute-done.22.w2, bf16[256,2048]{1,0:T(8,128)(2,1)} %collective-permute-done.23.w3, ...), custom_call_target="tpu_custom_call" | custom-call | flops 536870912 | bytes 10485760 | tf_op jit(solution)/shard_map/finish/pallas_call | solution.py:424
  (50 shorter events, 9.3 us)
Async XLA Ops:
  0.0 20.0 %collective-permute-start = (bf16[64,2048]{1,0:T(8,128)(2,1)}, bf16[64,2048]{1,0:T(8,128)(2,1)S(1)}, u32[]{:S(2)}, u32[]{:S(2)}) collective-permute-start(bf16[64,2048]{1,0:T(8,128)(2,1)} %lat.1), channel_id=1, source_target_pairs={{0,2},{2,4},{4,6},{6,0},{1,3},{3,5},{5,7},{7,1},{8,10},{10,12},{12... | collective-permute-start | bytes 786440 | tf_op jit(solution)/shard_map/ppermute | solution.py:334
  2.1 18.0 %collective-permute-start.1 = (bf16[64,2048]{1,0:T(8,128)(2,1)}, bf16[64,2048]{1,0:T(8,128)(2,1)S(1)}, u32[]{:S(2)}, u32[]{:S(2)}) collective-permute-start(bf16[64,2048]{1,0:T(8,128)(2,1)} %lat.1), channel_id=1, source_target_pairs={{0,6},{2,0},{4,2},{6,4},{1,7},{3,1},{5,3},{7,5},{8,14},{10,8},{12,... | collective-permute-start | bytes 786440 | tf_op jit(solution)/shard_map/ppermute | solution.py:335
  3.6 17.0 %collective-permute-start.2 = (bf16[64,2048]{1,0:T(8,128)(2,1)}, bf16[64,2048]{1,0:T(8,128)(2,1)S(1)}, u32[]{:S(2)}, u32[]{:S(2)}) collective-permute-start(bf16[64,2048]{1,0:T(8,128)(2,1)} %lat.1), channel_id=1, source_target_pairs={{0,4},{2,6},{4,0},{6,2},{1,5},{3,7},{5,1},{7,3},{8,12},{10,14},{12... | collective-permute-start | bytes 786440 | tf_op jit(solution)/shard_map/ppermute | solution.py:336
  7.1 20.9 %all-to-all-start = ((f32[32,2,768]{2,1,0:T(2,128)}), f32[32,2,768]{2,1,0:T(2,128)S(1)}, u32[]{:S(2)}, u32[]{:S(2)}) async-start(f32[32,2,768]{2,1,0:T(2,128)} %share.1), calls=%async_computation | async-start | bytes 393216 | tf_op jit(solution)/shard_map/all_to_all | solution.py:355
  18.1 17.0 %collective-permute-start.3 = (bf16[64,2048]{1,0:T(8,128)(2,1)}, bf16[64,2048]{1,0:T(8,128)(2,1)S(1)}, u32[]{:S(2)}, u32[]{:S(2)}) collective-permute-start(bf16[64,2048]{1,0:T(8,128)(2,1)} %lat.1), channel_id=1, source_target_pairs={{0,1},{1,0},{2,3},{3,2},{4,5},{5,4},{6,7},{7,6},{8,9},{9,8},{10,11... | collective-permute-start | bytes 786440 | tf_op jit(solution)/shard_map/ppermute | solution.py:340
  20.0 19.9 %collective-permute-start.4 = (bf16[64,2048]{1,0:T(8,128)(2,1)S(1)}, bf16[64,2048]{1,0:T(8,128)(2,1)S(1)}, u32[]{:S(2)}, u32[]{:S(2)}) collective-permute-start(bf16[64,2048]{1,0:T(8,128)(2,1)S(1)} %collective-permute-done.refs_0_), channel_id=1, source_target_pairs={{0,1},{1,0},{2,3},{3,2},{4,5},{5,4},{6,7},{7,6},{8,9},{9,8},{10,11... | collective-permute-start | bytes 786440 | tf_op jit(solution)/shard_map/ppermute | solution.py:340
  20.1 19.8 %collective-permute-start.5 = (bf16[64,2048]{1,0:T(8,128)(2,1)S(1)}, bf16[64,2048]{1,0:T(8,128)(2,1)S(1)}, u32[]{:S(2)}, u32[]{:S(2)}) collective-permute-start(bf16[64,2048]{1,0:T(8,128)(2,1)S(1)} %collective-permute-done.1.refs_1_), channel_id=1, source_target_pairs={{0,1},{1,0},{2,3},{3,2},{4,5},{5,4},{6,7},{7,6},{8,9},{9,8},{10,11... | collective-permute-start | bytes 786440 | tf_op jit(solution)/shard_map/ppermute | solution.py:340
  20.5 19.4 %collective-permute-start.6 = (bf16[64,2048]{1,0:T(8,128)(2,1)S(1)}, bf16[64,2048]{1,0:T(8,128)(2,1)S(1)}, u32[]{:S(2)}, u32[]{:S(2)}) collective-permute-start(bf16[64,2048]{1,0:T(8,128)(2,1)S(1)} %collective-permute-done.2.refs_2_), channel_id=1, source_target_pairs={{0,1},{1,0},{2,3},{3,2},{4,5},{5,4},{6,7},{7,6},{8,9},{9,8},{10,11... | collective-permute-start | bytes 786440 | tf_op jit(solution)/shard_map/ppermute | solution.py:340
  28.7 11.2 %all-to-all-start.1 = ((f32[8,2,768]{2,1,0:T(2,128)}), f32[8,2,768]{2,1,0:T(2,128)S(1)}, u32[]{:S(2)}, u32[]{:S(2)}) async-start(f32[8,2,768]{2,1,0:T(2,128)} %broadcast_in_dim.20), calls=%async_computation.1 | async-start | bytes 98304 | tf_op jit(solution)/shard_map/all_to_all | solution.py:358
  44.0 9.0 %collective-permute-start.7 = (bf16[2,512,128]{2,1,0:T(8,128)(2,1)S(1)}, bf16[2,512,128]{2,1,0:T(8,128)(2,1)S(1)}, u32[]{:S(2)}, u32[]{:S(2)}) collective-permute-start(bf16[2,512,128]{2,1,0:T(8,128)(2,1)S(1)} %get-tuple-element.19.q.q0), channel_id=1, source_target_pairs={{0,8},{8,16},{16,24},{24,0},{1,9},{9,17},{17,25},{25,1},{2,10},{10... | collective-permute-start | bytes 786440 | tf_op jit(solution)/shard_map/ppermute | solution.py:334
  44.1 9.7 %collective-permute-start.8 = (bf16[2,512,128]{2,1,0:T(8,128)(2,1)S(1)}, bf16[2,512,128]{2,1,0:T(8,128)(2,1)S(1)}, u32[]{:S(2)}, u32[]{:S(2)}) collective-permute-start(bf16[2,512,128]{2,1,0:T(8,128)(2,1)S(1)} %get-tuple-element.19.q.q0), channel_id=1, source_target_pairs={{0,24},{8,0},{16,8},{24,16},{1,25},{9,1},{17,9},{25,17},{2,26},{10... | collective-permute-start | bytes 786440 | tf_op jit(solution)/shard_map/ppermute | solution.py:335
  46.8 10.7 %collective-permute-start.9 = (bf16[2,512,128]{2,1,0:T(8,128)(2,1)S(1)}, bf16[2,512,128]{2,1,0:T(8,128)(2,1)S(1)}, u32[]{:S(2)}, u32[]{:S(2)}) collective-permute-start(bf16[2,512,128]{2,1,0:T(8,128)(2,1)S(1)} %get-tuple-element.19.q.q0), channel_id=1, source_target_pairs={{0,16},{8,24},{16,0},{24,8},{1,17},{9,25},{17,1},{25,9},{2,18},{10... | collective-permute-start | bytes 786440 | tf_op jit(solution)/shard_map/ppermute | solution.py:336
  46.8 49.9 %collective-permute-start.21 = (bf16[256,2048]{1,0:T(8,128)(2,1)S(1)}, bf16[256,2048]{1,0:T(8,128)(2,1)S(1)}, u32[]{:S(2)}, u32[]{:S(2)}) collective-permute-start(bf16[256,2048]{1,0:T(8,128)(2,1)S(1)} %copy-done), channel_id=1, source_target_pairs={{0,2},{1,7},{2,4},{3,1},{4,6},{5,3},{6,0},{7,5},{8,10},{9,15},{10,... | collective-permute-start | bytes 3145736 | tf_op jit(solution)/shard_map/ppermute | solution.py:390
  47.6 60.0 %collective-permute-start.22 = (bf16[256,2048]{1,0:T(8,128)(2,1)S(1)}, bf16[256,2048]{1,0:T(8,128)(2,1)S(1)}, u32[]{:S(2)}, u32[]{:S(2)}) collective-permute-start(bf16[256,2048]{1,0:T(8,128)(2,1)S(1)} %copy-done), channel_id=1, source_target_pairs={{2,0},{7,1},{4,2},{1,3},{6,4},{3,5},{0,6},{5,7},{10,8},{15,9},{12,... | collective-permute-start | bytes 3145736 | tf_op jit(solution)/shard_map/ppermute | solution.py:391
  53.0 54.8 %collective-permute-start.23 = (bf16[256,2048]{1,0:T(8,128)(2,1)S(1)}, bf16[256,2048]{1,0:T(8,128)(2,1)}, u32[]{:S(2)}, u32[]{:S(2)}) collective-permute-start(bf16[256,2048]{1,0:T(8,128)(2,1)S(1)} %copy-done), channel_id=1, source_target_pairs={{0,4},{2,6},{4,0},{6,2},{1,5},{3,7},{5,1},{7,3},{8,12},{10,14},{12... | collective-permute-start | bytes 3145736 | tf_op jit(solution)/shard_map/ppermute | solution.py:392
  53.8 6.8 %collective-permute-start.10 = (bf16[528,256]{1,0:T(8,128)(2,1)S(1)}, bf16[528,256]{1,0:T(8,128)(2,1)S(1)}, u32[]{:S(2)}, u32[]{:S(2)}) collective-permute-start(bf16[528,256]{1,0:T(8,128)(2,1)S(1)} %get-tuple-element.20.kv.refs_8_), channel_id=1, source_target_pairs={{0,32},{32,64},{64,96},{96,128},{128,160},{160,192},{192,224},{224... | collective-permute-start | bytes 811016 | tf_op jit(solution)/shard_map/ppermute | solution.py:382
  57.5 5.6 %collective-permute-start.11 = (bf16[528,256]{1,0:T(8,128)(2,1)S(1)}, bf16[528,256]{1,0:T(8,128)(2,1)S(1)}, u32[]{:S(2)}, u32[]{:S(2)}) collective-permute-start(bf16[528,256]{1,0:T(8,128)(2,1)S(1)} %get-tuple-element.20.kv.refs_8_), channel_id=1, source_target_pairs={{0,224},{32,0},{64,32},{96,64},{128,96},{160,128},{192,160},{224,1... | collective-permute-start | bytes 811016 | tf_op jit(solution)/shard_map/ppermute | solution.py:383
  60.6 9.1 %collective-permute-start.12 = (bf16[528,256]{1,0:T(8,128)(2,1)S(1)}, bf16[528,256]{1,0:T(8,128)(2,1)S(1)}, u32[]{:S(2)}, u32[]{:S(2)}) collective-permute-start(bf16[528,256]{1,0:T(8,128)(2,1)S(1)} %collective-permute-done.10.up.refs_9_), channel_id=1, source_target_pairs={{0,32},{32,64},{64,96},{96,128},{128,160},{160,192},{192,224},{224... | collective-permute-start | bytes 811016 | tf_op jit(solution)/shard_map/ppermute | solution.py:386
  63.1 7.3 %collective-permute-start.13 = (bf16[528,256]{1,0:T(8,128)(2,1)S(1)}, bf16[528,256]{1,0:T(8,128)(2,1)S(1)}, u32[]{:S(2)}, u32[]{:S(2)}) collective-permute-start(bf16[528,256]{1,0:T(8,128)(2,1)S(1)} %collective-permute-done.11.down.refs_12_), channel_id=1, source_target_pairs={{0,224},{32,0},{64,32},{96,64},{128,96},{160,128},{192,160},{224,1... | collective-permute-start | bytes 811016 | tf_op jit(solution)/shard_map/ppermute | solution.py:387
  69.7 16.1 %collective-permute-start.14 = (bf16[528,256]{1,0:T(8,128)(2,1)S(1)}, bf16[528,256]{1,0:T(8,128)(2,1)S(1)}, u32[]{:S(2)}, u32[]{:S(2)}) collective-permute-start(bf16[528,256]{1,0:T(8,128)(2,1)S(1)} %collective-permute-done.12.up.refs_10_), channel_id=1, source_target_pairs={{0,32},{32,64},{64,96},{96,128},{128,160},{160,192},{192,224},{224... | collective-permute-start | bytes 811016 | tf_op jit(solution)/shard_map/ppermute | solution.py:386
  70.4 15.5 %collective-permute-start.15 = (bf16[528,256]{1,0:T(8,128)(2,1)S(1)}, bf16[528,256]{1,0:T(8,128)(2,1)S(1)}, u32[]{:S(2)}, u32[]{:S(2)}) collective-permute-start(bf16[528,256]{1,0:T(8,128)(2,1)S(1)} %collective-permute-done.13.down.refs_13_), channel_id=1, source_target_pairs={{0,224},{32,0},{64,32},{96,64},{128,96},{160,128},{192,160},{224,1... | collective-permute-start | bytes 811016 | tf_op jit(solution)/shard_map/ppermute | solution.py:387
  85.8 22.4 %collective-permute-start.16 = (bf16[528,128]{1,0:T(8,128)(2,1)S(1)}, bf16[528,128]{1,0:T(8,128)(2,1)S(1)}, u32[]{:S(2)}, u32[]{:S(2)}) collective-permute-start(bf16[528,128]{1,0:T(8,128)(2,1)S(1)} %slice.8), channel_id=1, source_target_pairs={{0,32},{32,64},{64,96},{96,128},{128,160},{160,192},{192,224},{224... | collective-permute-start | bytes 405512 | tf_op jit(solution)/shard_map/ppermute | solution.py:388
  85.9 22.6 %collective-permute-start.17 = (bf16[528,128]{1,0:T(8,128)(2,1)S(1)}, bf16[528,128]{1,0:T(8,128)(2,1)S(1)}, u32[]{:S(2)}, u32[]{:S(2)}) collective-permute-start(bf16[528,128]{1,0:T(8,128)(2,1)S(1)} %slice.9), channel_id=1, source_target_pairs={{0,224},{32,0},{64,32},{96,64},{128,96},{160,128},{192,160},{224,1... | collective-permute-start | bytes 405512 | tf_op jit(solution)/shard_map/ppermute | solution.py:389
  96.6 51.5 %collective-permute-start.24 = (bf16[256,2048]{1,0:T(8,128)(2,1)S(1)}, bf16[256,2048]{1,0:T(8,128)(2,1)}, u32[]{:S(2)}, u32[]{:S(2)}) collective-permute-start(bf16[256,2048]{1,0:T(8,128)(2,1)S(1)} %copy-done), channel_id=1, source_target_pairs={{0,1},{1,0},{2,3},{3,2},{4,5},{5,4},{6,7},{7,6},{8,9},{9,8},{10,11... | collective-permute-start | bytes 3145736 | tf_op jit(solution)/shard_map/ppermute | solution.py:340
  107.7 47.0 %collective-permute-start.25 = (bf16[256,2048]{1,0:T(8,128)(2,1)S(1)}, bf16[256,2048]{1,0:T(8,128)(2,1)}, u32[]{:S(2)}, u32[]{:S(2)}) collective-permute-start(bf16[256,2048]{1,0:T(8,128)(2,1)S(1)} %collective-permute-done.21.w1), channel_id=1, source_target_pairs={{0,1},{1,0},{2,3},{3,2},{4,5},{5,4},{6,7},{7,6},{8,9},{9,8},{10,11... | collective-permute-start | bytes 3145736 | tf_op jit(solution)/shard_map/ppermute | solution.py:340
  107.8 46.9 %collective-permute-start.26 = (bf16[256,2048]{1,0:T(8,128)(2,1)S(1)}, bf16[256,2048]{1,0:T(8,128)(2,1)}, u32[]{:S(2)}, u32[]{:S(2)}) collective-permute-start(bf16[256,2048]{1,0:T(8,128)(2,1)S(1)} %collective-permute-done.22.w2), channel_id=1, source_target_pairs={{0,1},{1,0},{2,3},{3,2},{4,5},{5,4},{6,7},{7,6},{8,9},{9,8},{10,11... | collective-permute-start | bytes 3145736 | tf_op jit(solution)/shard_map/ppermute | solution.py:340
  108.2 46.5 %collective-permute-start.27 = (bf16[256,2048]{1,0:T(8,128)(2,1)}, bf16[256,2048]{1,0:T(8,128)(2,1)}, u32[]{:S(2)}, u32[]{:S(2)}) collective-permute-start(bf16[256,2048]{1,0:T(8,128)(2,1)} %collective-permute-done.23.w3), channel_id=1, source_target_pairs={{0,1},{1,0},{2,3},{3,2},{4,5},{5,4},{6,7},{7,6},{8,9},{9,8},{10,11... | collective-permute-start | bytes 3145736 | tf_op jit(solution)/shard_map/ppermute | solution.py:340
  116.0 7.9 %collective-permute-start.19 = (bf16[2,528,128]{2,1,0:T(8,128)(2,1)S(1)}, bf16[2,528,128]{2,1,0:T(8,128)(2,1)S(1)}, u32[]{:S(2)}, u32[]{:S(2)}) collective-permute-start(bf16[2,528,128]{2,1,0:T(8,128)(2,1)S(1)} %get-tuple-element.31), channel_id=1, source_target_pairs={{0,24},{8,0},{16,8},{24,16},{1,25},{9,1},{17,9},{25,17},{2,26},{10... | collective-permute-start | bytes 811016 | tf_op jit(solution)/shard_map/ppermute | solution.py:418
  123.9 8.5 %collective-permute-start.20 = (bf16[2,528,128]{2,1,0:T(8,128)(2,1)S(1)}, bf16[2,528,128]{2,1,0:T(8,128)(2,1)S(1)}, u32[]{:S(2)}, u32[]{:S(2)}) collective-permute-start(bf16[2,528,128]{2,1,0:T(8,128)(2,1)S(1)} %get-tuple-element.32), channel_id=1, source_target_pairs={{0,8},{8,16},{16,24},{24,0},{1,9},{9,17},{17,25},{25,1},{2,10},{10... | collective-permute-start | bytes 811016 | tf_op jit(solution)/shard_map/ppermute | solution.py:419
  127.7 27.0 %copy-start.1 = (bf16[64,2048]{1,0:T(8,128)(2,1)S(1)}, bf16[64,2048]{1,0:T(8,128)(2,1)}, u32[]{:S(2)}) copy-start(bf16[64,2048]{1,0:T(8,128)(2,1)} %lat.1) | copy-start | bytes 786436
  132.4 7.8 %collective-permute-start.18 = (bf16[2,528,128]{2,1,0:T(8,128)(2,1)S(1)}, bf16[2,528,128]{2,1,0:T(8,128)(2,1)S(1)}, u32[]{:S(2)}, u32[]{:S(2)}) collective-permute-start(bf16[2,528,128]{2,1,0:T(8,128)(2,1)S(1)} %shard_map.139), channel_id=1, source_target_pairs={{0,16},{8,24},{16,0},{24,8},{1,17},{9,25},{17,1},{25,9},{2,18},{10... | collective-permute-start | bytes 811016 | tf_op jit(solution)/shard_map/ppermute | solution.py:416
  141.6 13.1 %all-to-all-start.2 = ((bf16[8,64,256]{2,1,0:T(8,128)(2,1)}), bf16[8,64,256]{2,1,0:T(8,128)(2,1)}, u32[]{:S(2)}, u32[]{:S(2)}) async-start(bf16[8,64,256]{2,1,0:T(8,128)(2,1)} %copy-done.2), calls=%async_computation.2 | async-start | bytes 524288 | tf_op jit(solution)/shard_map/all_to_all | solution.py:422
  (2 other events, 7.5 us)

commit v4 on v3

--- a/solution.py
+++ b/solution.py
@@ -49,10 +49,10 @@
 def columns_of(mod, row, first, last):
     wide = mod.shape[2]
     found = []
-    for piece in range(mod.shape[0]):
+    for piece in range(8):
         lo, hi = max(first - piece * wide, 0), min(last - piece * wide, wide)
         if lo < hi:
-            found.append(mod[piece, row : row + 1, lo:hi])
+            found.append(tree([mod[8 * x + piece, row : row + 1, lo:hi] for x in range(4)], jnp.add))
     return jnp.concatenate(found, axis=1)
 
 
@@ -74,9 +74,11 @@
     sp = lax.axis_index("z") * 4 + lax.axis_index("x")
     core = lax.axis_index("c")
 
+    vectors = [(columns_of(mod, r, width, 2 * width), columns_of(mod, r, 0, width)) for r in range(2)]
+
     def modulate(v, r):
-        scale = columns_of(mod, r, width, 2 * width)
-        return (rms(v.astype(F32)) * (1.0 + scale) + columns_of(mod, r, 0, width)).astype(BF)
+        scale, offset = vectors[r]
+        return (rms(v.astype(F32)) * (1.0 + scale) + offset).astype(BF)
 
     def turn(v, cos, sin):
         lane = lax.broadcasted_iota(jnp.int32, v.shape, 1)
@@ -163,8 +165,9 @@
     return pl.ds(pl.multiple_of(b * size, size), size)
 
 
-def own_kernel(q, kv, up, down, m, l, acc, k_buf, v_buf):
-    fill(k_buf, v_buf, (kv, up, down))
+def first_kernel(q, *refs):
+    pieces, (m, l, acc, k_buf, v_buf) = refs[:-5], refs[-5:]
+    fill(k_buf, v_buf, pieces)
 
     def step(b, carry):
         at, size = rows_at(b, CHUNK // 2), CHUNK // 2
@@ -174,9 +177,9 @@
     lax.fori_loop(0, 4, step, 0)
 
 
-def rest_kernel(q0, q1, q2, q3, m_own, l_own, acc_own, kv, up, down, q_all, m, l, acc, k_buf, v_buf):
+def near_kernel(q0, q1, q2, m_own, l_own, acc_own, kv, up, down, q_all, m, l, acc, k_buf, v_buf):
     fill(k_buf, v_buf, (kv, up, down))
-    for j, r in enumerate((q0, q1, q2, q3)):
+    for j, r in enumerate((q0, q1, q2)):
         for h in range(2):
             q_all[(2 * j + h) * CHUNK : (2 * j + h + 1) * CHUNK] = r[h]
     for whole, own in ((m, m_own), (l, l_own), (acc, acc_own)):
@@ -187,7 +190,7 @@
         m[at], l[at], acc[at] = softmax_block(q_all[at], k_buf, v_buf, None)
         return carry
 
-    lax.fori_loop(2, 8, step, 0)
+    lax.fori_loop(2, 6, step, 0)
 
 
 def more_kernel(q_all, m_in, l_in, acc_in, up, down, m, l, acc, k_buf, v_buf):
@@ -198,7 +201,7 @@
         m[at], l[at], acc[at] = softmax_block(q_all[at], k_buf, v_buf, (m_in[at], l_in[at], acc_in[at]))
         return carry
 
-    lax.fori_loop(0, 8, step, 0)
+    lax.fori_loop(0, q_all.shape[0] // CHUNK, step, 0)
 
 
 def final_kernel(*refs, parts, lift, size):
@@ -346,16 +349,17 @@
     loaded = [cond[None], ctx_cond[None], mod_weight]
     shares = pl.pallas_call(
         share_kernel,
-        out_shape=jax.ShapeDtypeStruct((32, 2, mod_weight.shape[1]), F32),
+        out_shape=jax.ShapeDtypeStruct((16, 2, mod_weight.shape[1]), F32),
         in_specs=[pl.BlockSpec(memory_space=pltpu.HBM)] * 3,
         out_specs=VMEM,
         scratch_shapes=[pltpu.VMEM(v.shape, F32) for v in loaded] + [pltpu.SemaphoreType.DMA((3,))],
         name="share",
     )(*[pltpu.with_memory_space_constraint(v, pltpu.HBM) for v in loaded])
-    shares = lax.all_to_all(shares, SP, 0, 0)
+    shares = lax.all_to_all(shares, ("z", "c"), 0, 0)
     theirs = [swap(v) for v in mine]
-    summed = jnp.sum(shares, axis=0)
-    modulation = lax.all_to_all(jnp.broadcast_to(summed[None], (8,) + summed.shape), TP, 0, 0)
+    summed = jnp.sum(shares.reshape((8, 2) + shares.shape[1:]), axis=0)
+    pieces = lax.all_to_all(jnp.broadcast_to(summed[None], (16,) + summed.shape), ("x", "y"), 0, 0)
+    modulation = pieces.reshape((32,) + shares.shape[1:])
     count = 16384
     tables = [jnp.asarray(t) for t in rope_tables(count)]
     loaded = [
@@ -392,32 +396,32 @@
     weights = [out_weight, first, second, lax.ppermute(out_weight, "y", shift(4, 2))]
     weights += [swap(v) for v in weights]
 
-    rows = 8 * CHUNK
     state_of = lambda n: [pltpu.VMEM((n, HD), F32)] * 3
     firsts = [kv, up[1], down[1]]
-    own = call(own_kernel, [q, *firsts], state_of(2 * CHUNK), 3 * CHUNK, 2 * CHUNK)
+    own = call(first_kernel, [q, *firsts], state_of(2 * CHUNK), 3 * CHUNK, 2 * CHUNK)
     q_all, *state = call(
-        rest_kernel, [*q_parts, *own, *firsts], [pltpu.VMEM((rows, HD), BF)] + state_of(rows),
-        3 * CHUNK, 6 * CHUNK,
+        near_kernel, [*q_parts[:3], *own, *firsts],
+        [pltpu.VMEM((6 * CHUNK, HD), BF)] + state_of(6 * CHUNK), 3 * CHUNK, 4 * CHUNK,
     )
     state = call(
-        more_kernel, [q_all, *state, up[2], down[2]], state_of(rows), 2 * CHUNK, rows,
+        more_kernel, [q_all, *state, up[2], down[2]], state_of(6 * CHUNK), 2 * CHUNK, 6 * CHUNK,
         {1: 0, 2: 1, 3: 2},
     )
-
-    def final(*parts):
+    far = call(first_kernel, [q_parts[3], *firsts, up[2], down[2]], state_of(2 * CHUNK), 5 * CHUNK, 2 * CHUNK)
+
+    def final(whose, size, *parts):
         return call(
-            functools.partial(final_kernel, parts=parts, lift=lift, size=CHUNK),
-            [q_all, *state, up[3], down[3], k_far, v_far, kv, *up[1:], *down[1:]],
+            functools.partial(final_kernel, parts=parts, lift=lift, size=size),
+            [*whose, up[3], down[3], k_far, v_far, kv, *up[1:], *down[1:]],
             [pltpu.VMEM((2, CHUNK + 16, HD), BF)] * len(parts), 3 * CHUNK + 2 * HD, 2 * CHUNK * len(parts),
         )
 
-    (to_far,) = final(3)
+    (to_far,) = final([q_parts[3].reshape(2 * CHUNK, HD), *far], CHUNK, 0)
     partials = [lax.ppermute(to_far, "x", shift(4, 2))]
-    to_down, to_up = final(1, 2)
+    to_down, to_up = final([q_all, *state], CHUNK, 1, 2)
     partials.append(lax.ppermute(to_down, "x", shift(4, -1)))
     partials.append(lax.ppermute(to_up, "x", shift(4, 1)))
-    partials += final(0)
+    partials += final([q_all, *state], CHUNK // 2, 0)
     (sent,) = call(merge_kernel, partials, [jax.ShapeDtypeStruct((8, GRID_W, 2 * HD), BF)], 0, CHUNK)
     got = lax.all_to_all(sent, TP, 0, 0)
     operands = [got, *weights, latents, modulation]

time: 160 us -> 155 us (0.969)
  waiting for transfers between devices: 52.3 us -> 40.4 us
  starting transfers between devices: 59.3 us -> 64.6 us
    ppermute x1, waiting for transfers between devices: 4.68 us -> 0.01 us  [body(): partials.append(lax.ppermute(to_up, 'x', shift(4, 1)))]
    ppermute x8, starting transfers between devices: 14.4 us -> 18.4 us  [swap(): return lax.ppermute(v, 'c', [(0, 1), (1, 0)])]
    ppermute x2, waiting for transfers between devices: 3.4 us -> 0.01 us  [over_four(): lax.ppermute(v, axis, shift(4, 2))]
    ppermute x2, waiting for transfers between devices: 4.75 us -> 1.83 us  [over_four(): lax.ppermute(v, axis, shift(4, 1))]
    ppermute x1, waiting for transfers between devices: 2.51 us -> 0.01 us  [body(): down.append(lax.ppermute(kv, 'z', shift(8, -1)))]
    all_to_all x2, waiting for transfers between devices: 12.2 us -> 14.5 us  [the longest x1 7.42 us: body(): shares = lax.all_to_all(shares, ('z', 'c'), 0, 0)]
    all_to_all x2, starting transfers between devices: 17.4 us -> 15.1 us  [the longest x1 10 us: body(): shares = lax.all_to_all(shares, ('z', 'c'), 0, 0)]
    ppermute x1, waiting for transfers between devices: 3.6 us -> 1.27 us  [body(): partials = [lax.ppermute(to_far, 'x', shift(4, 2))]]
  transfers between devices with their start and end apart: 31 -> 31, of which waited for: 12 -> 8; matrix products, arithmetic and copies ran while one was open for 0% -> 1% of each run, Pallas kernels for 23% -> 25%
where the time goes in v4:
time: 155 us
  starting transfers between devices  64.6 us (42%)
  Pallas kernels  47.4 us (31%)
  waiting for transfers between devices  40.4 us (26%)
  local copies, waits for them, and re-layouts  2.4 us (2%)
    pallas_call x8, Pallas kernels, call(): pl.pallas_call(kernel, out_shape=shape, in_specs=[VMEM] * len(operands),...  36.6 us
    ppermute x8, starting transfers between devices, swap(): return lax.ppermute(v, 'c', [(0, 1), (1, 0)])  18.4 us
    all_to_all x1, starting transfers between devices, body(): shares = lax.all_to_all(shares, ('z', 'c'), 0, 0)  10 us
    ppermute x1, waiting for transfers between devices, body(): partials.append(lax.ppermute(to_down, 'x', shift(4, -1)))  7.83 us
    all_to_all x1, waiting for transfers between devices, body(): shares = lax.all_to_all(shares, ('z', 'c'), 0, 0)  7.42 us
    all_to_all x1, waiting for transfers between devices, body(): lax.all_to_all(jnp.broadcast_to(summed[None], (16,) + summed.shape), ('x'...  7.12 us
    all_to_all x1, waiting for transfers between devices, body(): got = lax.all_to_all(sent, TP, 0, 0)  6.6 us
    all_to_all x1, starting transfers between devices, body(): got = lax.all_to_all(sent, TP, 0, 0)  6.08 us
  transfers between devices with their start and end apart: 31, of which 8 were waited for; matrix products, arithmetic and copies ran while one was open for 1% of the time, Pallas kernels for 25%

profile of v4, /device:TPU:1, one launch (start us, length us, event | category | flops | bytes accessed | tf_op | source)
XLA Modules:
  0.0 155.0 jit_solution(2699299776691839085)
XLA Ops:
  0.0 2.1 %collective-permute-start = (bf16[64,2048]{1,0:T(8,128)(2,1)}, bf16[64,2048]{1,0:T(8,128)(2,1)S(1)}, u32[]{:S(2)}, u32[]{:S(2)}) collective-permute-start(bf16[64,2048]{1,0:T(8,128)(2,1)} %lat.1), channel_id=1, source_target_pairs={{0,2},{2,4},{4,6},{6,0},{1,3},{3,5},{5,7},{7,1},{8,10},{10,12},{12... | collective-permute-start | bytes 786440 | tf_op jit(solution)/shard_map/ppermute | solution.py:337
  2.1 1.4 collective-permute-start.1
  3.6 1.6 %collective-permute-start.2 = (bf16[64,2048]{1,0:T(8,128)(2,1)}, bf16[64,2048]{1,0:T(8,128)(2,1)S(1)}, u32[]{:S(2)}, u32[]{:S(2)}) collective-permute-start(bf16[64,2048]{1,0:T(8,128)(2,1)} %lat.1), channel_id=1, source_target_pairs={{0,4},{2,6},{4,0},{6,2},{1,5},{3,7},{5,1},{7,3},{8,12},{10,14},{12... | collective-permute-start | bytes 786440 | tf_op jit(solution)/shard_map/ppermute | solution.py:339
  5.2 1.8 %share.1 = f32[16,2,768]{2,1,0:T(2,128)} custom-call(f32[1,64]{1,0:T(1,128)} %bitcast.11, f32[1,64]{1,0:T(1,128)} %bitcast.12, f32[64,768]{1,0:T(8,128)} %refs_2_.1), custom_call_target="tpu_custom_call" | custom-call | tf_op jit(solution)/shard_map/share/pallas_call | solution.py:350
  7.0 10.0 %all-to-all-start = ((f32[16,2,768]{2,1,0:T(2,128)}), f32[16,2,768]{2,1,0:T(2,128)S(1)}, u32[]{:S(2)}, u32[]{:S(2)}) async-start(f32[16,2,768]{2,1,0:T(2,128)} %share.1), calls=%async_computation | async-start | bytes 196608 | tf_op jit(solution)/shard_map/all_to_all | solution.py:358
  18.1 7.4 %all-to-all-done = f32[16,2,768]{2,1,0:T(2,128)S(1)} async-done(((f32[16,2,768]{2,1,0:T(2,128)}), f32[16,2,768]{2,1,0:T(2,128)S(1)}, u32[]{:S(2)}, u32[]{:S(2)}) %all-to-all-start) | async-done | bytes 98336 | tf_op jit(solution)/shard_map/all_to_all | solution.py:358
  26.3 5.1 %all-to-all-start.1 = ((f32[16,2,2,768]{3,2,1,0:T(2,128)}), f32[16,2,2,768]{3,2,1,0:T(2,128)S(1)}, u32[]{:S(2)}, u32[]{:S(2)}) async-start(f32[16,2,2,768]{3,2,1,0:T(2,128)} %broadcast_in_dim.20), calls=%async_computation.1 | async-start | bytes 393216 | tf_op jit(solution)/shard_map/all_to_all | solution.py:361
  31.4 7.1 %all-to-all-done.1 = f32[16,2,2,768]{3,2,1,0:T(2,128)S(1)} async-done(((f32[16,2,2,768]{3,2,1,0:T(2,128)}), f32[16,2,2,768]{3,2,1,0:T(2,128)S(1)}, u32[]{:S(2)}, u32[]{:S(2)}) %all-to-all-start.1) | async-done | bytes 196640 | tf_op jit(solution)/shard_map/all_to_all | solution.py:361
  38.5 4.0 %project.1 = (bf16[2,512,128]{2,1,0:T(8,128)(2,1)S(1)}, bf16[528,256]{1,0:T(8,128)(2,1)S(1)}) custom-call(bf16[64,2048]{1,0:T(8,128)(2,1)S(1)} %collective-permute-done.refs_0_, bf16[64,2048]{1,0:T(8,128)(2,1)S(1)} %collective-permute-done.1.refs_1_, bf16[64,2048]{1,0:T(8,128)(2,1)S(1)} %collective-permute-done.2.refs_2_, ...), custom_call_target="tpu_custom_call" | custom-call | flops 1107296256 | bytes 4194304 | tf_op jit(solution)/shard_map/project/pallas_call | solution.py:368
  42.9 2.4 %collective-permute-start.18 = (bf16[2,512,128]{2,1,0:T(8,128)(2,1)S(1)}, bf16[2,512,128]{2,1,0:T(8,128)(2,1)S(1)}, u32[]{:S(2)}, u32[]{:S(2)}) collective-permute-start(bf16[2,512,128]{2,1,0:T(8,128)(2,1)S(1)} %get-tuple-element.22.q.q0), channel_id=1, source_target_pairs={{0,24},{8,0},{16,8},{24,16},{1,25},{9,1},{17,9},{25,17},{2,26},{10... | collective-permute-start | bytes 786440 | tf_op jit(solution)/shard_map/ppermute | solution.py:338
  46.8 1.5 collective-permute-start.23
  48.3 1.8 %collective-permute-done.17.q1 = bf16[2,512,128]{2,1,0:T(8,128)(2,1)S(1)} collective-permute-done((bf16[2,512,128]{2,1,0:T(8,128)(2,1)S(1)}, bf16[2,512,128]{2,1,0:T(8,128)(2,1)S(1)}, u32[]{:S(2)}, u32[]{:S(2)}) %collective-permute-start.17) | collective-permute-done | bytes 262176 | tf_op jit(solution)/shard_map/ppermute | solution.py:337
  50.1 2.7 %collective-permute-start.9 = (bf16[528,256]{1,0:T(8,128)(2,1)S(1)}, bf16[528,256]{1,0:T(8,128)(2,1)S(1)}, u32[]{:S(2)}, u32[]{:S(2)}) collective-permute-start(bf16[528,256]{1,0:T(8,128)(2,1)S(1)} %get-tuple-element.23.refs_0_.refs_8_.kv), channel_id=1, source_target_pairs={{0,224},{32,0},{64,32},{96,64},{128,96},{160,128},{192,160},{224,1... | collective-permute-start | bytes 811016 | tf_op jit(solution)/shard_map/ppermute | solution.py:387
  52.8 4.1 %collective-permute-done.8.refs_1_.refs_9_.up = bf16[528,256]{1,0:T(8,128)(2,1)S(1)} collective-permute-done((bf16[528,256]{1,0:T(8,128)(2,1)S(1)}, bf16[528,256]{1,0:T(8,128)(2,1)S(1)}, u32[]{:S(2)}, u32[]{:S(2)}) %collective-permute-start.8) | collective-permute-done | bytes 270368 | tf_op jit(solution)/shard_map/ppermute | solution.py:386
  56.9 2.7 %collective-permute-start.11 = (bf16[528,256]{1,0:T(8,128)(2,1)S(1)}, bf16[528,256]{1,0:T(8,128)(2,1)S(1)}, u32[]{:S(2)}, u32[]{:S(2)}) collective-permute-start(bf16[528,256]{1,0:T(8,128)(2,1)S(1)} %collective-permute-done.9.refs_2_.refs_12_.down), channel_id=1, source_target_pairs={{0,224},{32,0},{64,32},{96,64},{128,96},{160,128},{192,160},{224,1... | collective-permute-start | bytes 811016 | tf_op jit(solution)/shard_map/ppermute | solution.py:391
  59.6 4.1 %collective-permute-done.10.refs_3_.refs_10_.up = bf16[528,256]{1,0:T(8,128)(2,1)S(1)} collective-permute-done((bf16[528,256]{1,0:T(8,128)(2,1)S(1)}, bf16[528,256]{1,0:T(8,128)(2,1)S(1)}, u32[]{:S(2)}, u32[]{:S(2)}) %collective-permute-start.10) | collective-permute-done | bytes 270368 | tf_op jit(solution)/shard_map/ppermute | solution.py:390
  63.7 2.7 %collective-permute-start.13 = (bf16[528,256]{1,0:T(8,128)(2,1)S(1)}, bf16[528,256]{1,0:T(8,128)(2,1)S(1)}, u32[]{:S(2)}, u32[]{:S(2)}) collective-permute-start(bf16[528,256]{1,0:T(8,128)(2,1)S(1)} %collective-permute-done.11.refs_4_.refs_13_.down), channel_id=1, source_target_pairs={{0,224},{32,0},{64,32},{96,64},{128,96},{160,128},{192,160},{224,1... | collective-permute-start | bytes 811016 | tf_op jit(solution)/shard_map/ppermute | solution.py:391
  66.4 3.6 %shard_map.138 = (f32[1024,128]{1,0:T(8,128)S(1)}, f32[1024,128]{1,0:T(8,128)S(1)}, f32[1024,128]{1,0:T(8,128)S(1)}) custom-call(bf16[2,512,128]{2,1,0:T(8,128)(2,1)S(1)} %get-tuple-element.22.q.q0, bf16[528,256]{1,0:T(8,128)(2,1)S(1)} %get-tuple-element.23.refs_0_.refs_8_.kv, bf16[528,256]{1,0:T(8,128)(2,1)S(1)} %collective-permute-done.8.refs_1_.refs_9_.up, ...), custom_call_target="tpu_custom_call" | custom-call | flops 805306368 | bytes 1048576 | tf_op jit(solution)/shard_map/pallas_call | solution.py:301
  70.0 5.7 %shard_map.139 = (bf16[3072,128]{1,0:T(8,128)(2,1)S(1)}, f32[3072,128]{1,0:T(8,128)S(1)}, f32[3072,128]{1,0:T(8,128)S(1)}, f32[3072,128]{1,0:T(8,128)S(1)}) custom-call(bf16[2,512,128]{2,1,0:T(8,128)(2,1)S(1)} %get-tuple-element.22.q.q0, bf16[2,512,128]{2,1,0:T(8,128)(2,1)S(1)} %collective-permute-done.17.q1, ...), custom_call_target="tpu_custom_call" | custom-call | flops 1610612736 | bytes 1048576 | tf_op jit(solution)/shard_map/pallas_call | solution.py:301
  76.5 2.7 %collective-permute-start.15 = (bf16[528,128]{1,0:T(8,128)(2,1)S(1)}, bf16[528,128]{1,0:T(8,128)(2,1)S(1)}, u32[]{:S(2)}, u32[]{:S(2)}) collective-permute-start(bf16[528,128]{1,0:T(8,128)(2,1)S(1)} %slice.9), channel_id=1, source_target_pairs={{0,224},{32,0},{64,32},{96,64},{128,96},{160,128},{192,160},{224,1... | collective-permute-start | bytes 405512 | tf_op jit(solution)/shard_map/ppermute | solution.py:393
  79.2 5.9 %shard_map.140 = (f32[3072,128]{1,0:T(8,128)S(1)}, f32[3072,128]{1,0:T(8,128)S(1)}, f32[3072,128]{1,0:T(8,128)S(1)}) custom-call(bf16[3072,128]{1,0:T(8,128)(2,1)S(1)} %get-tuple-element.30.q_all.refs_0_, f32[3072,128]{1,0:T(8,128)S(1)} %get-tuple-element.31.m_in, ...), custom_call_target="tpu_custom_call", output_to_operand_aliasing={{0}: (1, {}), {1}: (2, {}), {2}: (3, {})} | custom-call | flops 1610612736 | bytes 1048576 | tf_op jit(solution)/shard_map/pallas_call | solution.py:301
  85.2 16.5 %collective-permute-start.24 = (bf16[256,2048]{1,0:T(8,128)(2,1)S(1)}, bf16[256,2048]{1,0:T(8,128)(2,1)}, u32[]{:S(2)}, u32[]{:S(2)}) collective-permute-start(bf16[256,2048]{1,0:T(8,128)(2,1)S(1)} %copy-done), channel_id=1, source_target_pairs={{0,1},{1,0},{2,3},{3,2},{4,5},{5,4},{6,7},{7,6},{8,9},{9,8},{10,11... | collective-permute-start | bytes 3145736 | tf_op jit(solution)/shard_map/ppermute | solution.py:343
  102.6 7.5 %shard_map.141 = (bf16[2,528,128]{2,1,0:T(8,128)(2,1)S(1)}, bf16[2,528,128]{2,1,0:T(8,128)(2,1)S(1)}) custom-call(bf16[3072,128]{1,0:T(8,128)(2,1)S(1)} %get-tuple-element.30.q_all.refs_0_, f32[3072,128]{1,0:T(8,128)S(1)} %get-tuple-element.34.refs_1_, f32[3072,128]{1,0:T(8,128)S(1)} %get-tuple-element.35.refs_2_, ...), custom_call_target="tpu_custom_call" | custom-call | flops 1879048192 | bytes 1048576 | tf_op jit(solution)/shard_map/pallas_call | solution.py:301
  110.2 7.8 %collective-permute-done.19.p1 = bf16[2,528,128]{2,1,0:T(8,128)(2,1)S(1)} collective-permute-done((bf16[2,528,128]{2,1,0:T(8,128)(2,1)S(1)}, bf16[2,528,128]{2,1,0:T(8,128)(2,1)S(1)}, u32[]{:S(2)}, u32[]{:S(2)}) %collective-permute-start.19) | collective-permute-done | bytes 270368 | tf_op jit(solution)/shard_map/ppermute | solution.py:422
  118.0 4.9 %shard_map.136 = (f32[1024,128]{1,0:T(8,128)S(1)}, f32[1024,128]{1,0:T(8,128)S(1)}, f32[1024,128]{1,0:T(8,128)S(1)}) custom-call(bf16[2,512,128]{2,1,0:T(8,128)(2,1)S(1)} %collective-permute-done.7.q, bf16[528,256]{1,0:T(8,128)(2,1)S(1)} %get-tuple-element.23.refs_0_.refs_8_.kv, bf16[528,256]{1,0:T(8,128)(2,1)S(1)} %collective-permute-done.8.refs_1_.refs_9_.up, ...), custom_call_target="tpu_custom_call" | custom-call | flops 1342177280 | bytes 1048576 | tf_op jit(solution)/shard_map/pallas_call | solution.py:301
  122.9 3.8 %shard_map.137 = bf16[2,528,128]{2,1,0:T(8,128)(2,1)S(1)} custom-call(bf16[1024,128]{1,0:T(8,128)(2,1)S(1)} %bitcast.9, f32[1024,128]{1,0:T(8,128)S(1)} %get-tuple-element.24.refs_1_, f32[1024,128]{1,0:T(8,128)S(1)} %get-tuple-element.25.refs_2_, f32[1024,128]{1,0:T(8,128)S(1)} %get-tuple-element.26.refs_3_, ...), custom_call_target="tpu_custom_call" | custom-call | flops 939524096 | bytes 1048576 | tf_op jit(solution)/shard_map/pallas_call | solution.py:301
  126.7 2.5 %collective-permute-start.16 = (bf16[2,528,128]{2,1,0:T(8,128)(2,1)S(1)}, bf16[2,528,128]{2,1,0:T(8,128)(2,1)S(1)}, u32[]{:S(2)}, u32[]{:S(2)}) collective-permute-start(bf16[2,528,128]{2,1,0:T(8,128)(2,1)S(1)} %shard_map.137), channel_id=1, source_target_pairs={{0,16},{8,24},{16,0},{24,8},{1,17},{9,25},{17,1},{25,9},{2,18},{10... | collective-permute-start | bytes 811016 | tf_op jit(solution)/shard_map/ppermute | solution.py:420
  129.2 4.6 %shard_map.142.p3 = bf16[2,528,128]{2,1,0:T(8,128)(2,1)S(1)} custom-call(bf16[3072,128]{1,0:T(8,128)(2,1)S(1)} %get-tuple-element.30.q_all.refs_0_, f32[3072,128]{1,0:T(8,128)S(1)} %get-tuple-element.34.refs_1_, f32[3072,128]{1,0:T(8,128)S(1)} %get-tuple-element.35.refs_2_, f32[3072,128]{1,0:T(8,128)S(1)} %get-tuple-element.36.refs_3_, ...), custom_call_target="tpu_custom_call" | custom-call | flops 939524096 | bytes 1048576 | tf_op jit(solution)/shard_map/pallas_call | solution.py:301
  133.8 1.3 collective-permute-done.16.p0
  136.4 6.1 %all-to-all-start.2 = ((bf16[8,64,256]{2,1,0:T(8,128)(2,1)}), bf16[8,64,256]{2,1,0:T(8,128)(2,1)}, u32[]{:S(2)}, u32[]{:S(2)}) async-start(bf16[8,64,256]{2,1,0:T(8,128)(2,1)} %copy-done.2), calls=%async_computation.2 | async-start | bytes 524288 | tf_op jit(solution)/shard_map/all_to_all | solution.py:426
  142.5 6.6 %all-to-all-done.2.got = bf16[8,64,256]{2,1,0:T(8,128)(2,1)} async-done(((bf16[8,64,256]{2,1,0:T(8,128)(2,1)}), bf16[8,64,256]{2,1,0:T(8,128)(2,1)}, u32[]{:S(2)}, u32[]{:S(2)}) %all-to-all-start.2) | async-done | bytes 262176 | tf_op jit(solution)/shard_map/all_to_all | solution.py:426
  150.1 5.0 %finish.1 = bf16[64,2048]{1,0:T(8,128)(2,1)} custom-call(bf16[8,64,256]{2,1,0:T(8,128)(2,1)} %all-to-all-done.2.got, bf16[256,2048]{1,0:T(8,128)(2,1)S(1)} %copy-done, bf16[256,2048]{1,0:T(8,128)(2,1)S(1)} %collective-permute-done.21.w1, bf16[256,2048]{1,0:T(8,128)(2,1)S(1)} %collective-permute-done.22.w2, bf16[256,2048]{1,0:T(8,128)(2,1)} %collective-permute-done.23.w3, ...), custom_call_target="tpu_custom_call" | custom-call | flops 536870912 | bytes 10485760 | tf_op jit(solution)/shard_map/finish/pallas_call | solution.py:428
  (51 shorter events, 7.6 us)
Async XLA Ops:
  0.0 17.2 %collective-permute-start = (bf16[64,2048]{1,0:T(8,128)(2,1)}, bf16[64,2048]{1,0:T(8,128)(2,1)S(1)}, u32[]{:S(2)}, u32[]{:S(2)}) collective-permute-start(bf16[64,2048]{1,0:T(8,128)(2,1)} %lat.1), channel_id=1, source_target_pairs={{0,2},{2,4},{4,6},{6,0},{1,3},{3,5},{5,7},{7,1},{8,10},{10,12},{12... | collective-permute-start | bytes 786440 | tf_op jit(solution)/shard_map/ppermute | solution.py:337
  2.1 15.4 %collective-permute-start.1 = (bf16[64,2048]{1,0:T(8,128)(2,1)}, bf16[64,2048]{1,0:T(8,128)(2,1)S(1)}, u32[]{:S(2)}, u32[]{:S(2)}) collective-permute-start(bf16[64,2048]{1,0:T(8,128)(2,1)} %lat.1), channel_id=1, source_target_pairs={{0,6},{2,0},{4,2},{6,4},{1,7},{3,1},{5,3},{7,5},{8,14},{10,8},{12,... | collective-permute-start | bytes 786440 | tf_op jit(solution)/shard_map/ppermute | solution.py:338
  3.6 14.2 %collective-permute-start.2 = (bf16[64,2048]{1,0:T(8,128)(2,1)}, bf16[64,2048]{1,0:T(8,128)(2,1)S(1)}, u32[]{:S(2)}, u32[]{:S(2)}) collective-permute-start(bf16[64,2048]{1,0:T(8,128)(2,1)} %lat.1), channel_id=1, source_target_pairs={{0,4},{2,6},{4,0},{6,2},{1,5},{3,7},{5,1},{7,3},{8,12},{10,14},{12... | collective-permute-start | bytes 786440 | tf_op jit(solution)/shard_map/ppermute | solution.py:339
  7.0 18.5 %all-to-all-start = ((f32[16,2,768]{2,1,0:T(2,128)}), f32[16,2,768]{2,1,0:T(2,128)S(1)}, u32[]{:S(2)}, u32[]{:S(2)}) async-start(f32[16,2,768]{2,1,0:T(2,128)} %share.1), calls=%async_computation | async-start | bytes 196608 | tf_op jit(solution)/shard_map/all_to_all | solution.py:358
  17.0 14.3 %collective-permute-start.3 = (bf16[64,2048]{1,0:T(8,128)(2,1)}, bf16[64,2048]{1,0:T(8,128)(2,1)S(1)}, u32[]{:S(2)}, u32[]{:S(2)}) collective-permute-start(bf16[64,2048]{1,0:T(8,128)(2,1)} %lat.1), channel_id=1, source_target_pairs={{0,1},{1,0},{2,3},{3,2},{4,5},{5,4},{6,7},{7,6},{8,9},{9,8},{10,11... | collective-permute-start | bytes 786440 | tf_op jit(solution)/shard_map/ppermute | solution.py:343
  17.2 21.3 %collective-permute-start.4 = (bf16[64,2048]{1,0:T(8,128)(2,1)S(1)}, bf16[64,2048]{1,0:T(8,128)(2,1)S(1)}, u32[]{:S(2)}, u32[]{:S(2)}) collective-permute-start(bf16[64,2048]{1,0:T(8,128)(2,1)S(1)} %collective-permute-done.refs_0_), channel_id=1, source_target_pairs={{0,1},{1,0},{2,3},{3,2},{4,5},{5,4},{6,7},{7,6},{8,9},{9,8},{10,11... | collective-permute-start | bytes 786440 | tf_op jit(solution)/shard_map/ppermute | solution.py:343
  17.6 21.0 %collective-permute-start.5 = (bf16[64,2048]{1,0:T(8,128)(2,1)S(1)}, bf16[64,2048]{1,0:T(8,128)(2,1)S(1)}, u32[]{:S(2)}, u32[]{:S(2)}) collective-permute-start(bf16[64,2048]{1,0:T(8,128)(2,1)S(1)} %collective-permute-done.1.refs_1_), channel_id=1, source_target_pairs={{0,1},{1,0},{2,3},{3,2},{4,5},{5,4},{6,7},{7,6},{8,9},{9,8},{10,11... | collective-permute-start | bytes 786440 | tf_op jit(solution)/shard_map/ppermute | solution.py:343
  17.8 20.8 %collective-permute-start.6 = (bf16[64,2048]{1,0:T(8,128)(2,1)S(1)}, bf16[64,2048]{1,0:T(8,128)(2,1)S(1)}, u32[]{:S(2)}, u32[]{:S(2)}) collective-permute-start(bf16[64,2048]{1,0:T(8,128)(2,1)S(1)} %collective-permute-done.2.refs_2_), channel_id=1, source_target_pairs={{0,1},{1,0},{2,3},{3,2},{4,5},{5,4},{6,7},{7,6},{8,9},{9,8},{10,11... | collective-permute-start | bytes 786440 | tf_op jit(solution)/shard_map/ppermute | solution.py:343
  26.3 12.2 %all-to-all-start.1 = ((f32[16,2,2,768]{3,2,1,0:T(2,128)}), f32[16,2,2,768]{3,2,1,0:T(2,128)S(1)}, u32[]{:S(2)}, u32[]{:S(2)}) async-start(f32[16,2,2,768]{3,2,1,0:T(2,128)} %broadcast_in_dim.20), calls=%async_computation.1 | async-start | bytes 393216 | tf_op jit(solution)/shard_map/all_to_all | solution.py:361
  38.5 6.8 %copy-start = (bf16[256,2048]{1,0:T(8,128)(2,1)S(1)}, bf16[256,2048]{1,0:T(8,128)(2,1)}, u32[]{:S(2)}) copy-start(bf16[256,2048]{1,0:T(8,128)(2,1)} %w0.1) | copy-start | bytes 3145732
  42.6 7.5 %collective-permute-start.17 = (bf16[2,512,128]{2,1,0:T(8,128)(2,1)S(1)}, bf16[2,512,128]{2,1,0:T(8,128)(2,1)S(1)}, u32[]{:S(2)}, u32[]{:S(2)}) collective-permute-start(bf16[2,512,128]{2,1,0:T(8,128)(2,1)S(1)} %get-tuple-element.22.q.q0), channel_id=1, source_target_pairs={{0,8},{8,16},{16,24},{24,0},{1,9},{9,17},{17,25},{25,1},{2,10},{10... | collective-permute-start | bytes 786440 | tf_op jit(solution)/shard_map/ppermute | solution.py:337
  42.9 7.2 %collective-permute-start.18 = (bf16[2,512,128]{2,1,0:T(8,128)(2,1)S(1)}, bf16[2,512,128]{2,1,0:T(8,128)(2,1)S(1)}, u32[]{:S(2)}, u32[]{:S(2)}) collective-permute-start(bf16[2,512,128]{2,1,0:T(8,128)(2,1)S(1)} %get-tuple-element.22.q.q0), channel_id=1, source_target_pairs={{0,24},{8,0},{16,8},{24,16},{1,25},{9,1},{17,9},{25,17},{2,26},{10... | collective-permute-start | bytes 786440 | tf_op jit(solution)/shard_map/ppermute | solution.py:338
  45.3 31.2 %collective-permute-start.21 = (bf16[256,2048]{1,0:T(8,128)(2,1)S(1)}, bf16[256,2048]{1,0:T(8,128)(2,1)S(1)}, u32[]{:S(2)}, u32[]{:S(2)}) collective-permute-start(bf16[256,2048]{1,0:T(8,128)(2,1)S(1)} %copy-done), channel_id=1, source_target_pairs={{0,2},{1,7},{2,4},{3,1},{4,6},{5,3},{6,0},{7,5},{8,10},{9,15},{10,... | collective-permute-start | bytes 3145736 | tf_op jit(solution)/shard_map/ppermute | solution.py:394
  46.4 38.8 %collective-permute-start.22 = (bf16[256,2048]{1,0:T(8,128)(2,1)S(1)}, bf16[256,2048]{1,0:T(8,128)(2,1)S(1)}, u32[]{:S(2)}, u32[]{:S(2)}) collective-permute-start(bf16[256,2048]{1,0:T(8,128)(2,1)S(1)} %copy-done), channel_id=1, source_target_pairs={{2,0},{7,1},{4,2},{1,3},{6,4},{3,5},{0,6},{5,7},{10,8},{15,9},{12,... | collective-permute-start | bytes 3145736 | tf_op jit(solution)/shard_map/ppermute | solution.py:395
  46.8 54.9 %collective-permute-start.23 = (bf16[256,2048]{1,0:T(8,128)(2,1)S(1)}, bf16[256,2048]{1,0:T(8,128)(2,1)}, u32[]{:S(2)}, u32[]{:S(2)}) collective-permute-start(bf16[256,2048]{1,0:T(8,128)(2,1)S(1)} %copy-done), channel_id=1, source_target_pairs={{0,4},{2,6},{4,0},{6,2},{1,5},{3,7},{5,1},{7,3},{8,12},{10,14},{12... | collective-permute-start | bytes 3145736 | tf_op jit(solution)/shard_map/ppermute | solution.py:396
  50.1 6.8 %collective-permute-start.8 = (bf16[528,256]{1,0:T(8,128)(2,1)S(1)}, bf16[528,256]{1,0:T(8,128)(2,1)S(1)}, u32[]{:S(2)}, u32[]{:S(2)}) collective-permute-start(bf16[528,256]{1,0:T(8,128)(2,1)S(1)} %get-tuple-element.23.refs_0_.refs_8_.kv), channel_id=1, source_target_pairs={{0,32},{32,64},{64,96},{96,128},{128,160},{160,192},{192,224},{224... | collective-permute-start | bytes 811016 | tf_op jit(solution)/shard_map/ppermute | solution.py:386
  50.1 6.8 %collective-permute-start.9 = (bf16[528,256]{1,0:T(8,128)(2,1)S(1)}, bf16[528,256]{1,0:T(8,128)(2,1)S(1)}, u32[]{:S(2)}, u32[]{:S(2)}) collective-permute-start(bf16[528,256]{1,0:T(8,128)(2,1)S(1)} %get-tuple-element.23.refs_0_.refs_8_.kv), channel_id=1, source_target_pairs={{0,224},{32,0},{64,32},{96,64},{128,96},{160,128},{192,160},{224,1... | collective-permute-start | bytes 811016 | tf_op jit(solution)/shard_map/ppermute | solution.py:387
  56.9 6.8 %collective-permute-start.10 = (bf16[528,256]{1,0:T(8,128)(2,1)S(1)}, bf16[528,256]{1,0:T(8,128)(2,1)S(1)}, u32[]{:S(2)}, u32[]{:S(2)}) collective-permute-start(bf16[528,256]{1,0:T(8,128)(2,1)S(1)} %collective-permute-done.8.refs_1_.refs_9_.up), channel_id=1, source_target_pairs={{0,32},{32,64},{64,96},{96,128},{128,160},{160,192},{192,224},{224... | collective-permute-start | bytes 811016 | tf_op jit(solution)/shard_map/ppermute | solution.py:390
  56.9 6.8 %collective-permute-start.11 = (bf16[528,256]{1,0:T(8,128)(2,1)S(1)}, bf16[528,256]{1,0:T(8,128)(2,1)S(1)}, u32[]{:S(2)}, u32[]{:S(2)}) collective-permute-start(bf16[528,256]{1,0:T(8,128)(2,1)S(1)} %collective-permute-done.9.refs_2_.refs_12_.down), channel_id=1, source_target_pairs={{0,224},{32,0},{64,32},{96,64},{128,96},{160,128},{192,160},{224,1... | collective-permute-start | bytes 811016 | tf_op jit(solution)/shard_map/ppermute | solution.py:391
  63.7 11.9 %collective-permute-start.12 = (bf16[528,256]{1,0:T(8,128)(2,1)S(1)}, bf16[528,256]{1,0:T(8,128)(2,1)S(1)}, u32[]{:S(2)}, u32[]{:S(2)}) collective-permute-start(bf16[528,256]{1,0:T(8,128)(2,1)S(1)} %collective-permute-done.10.refs_3_.refs_10_.up), channel_id=1, source_target_pairs={{0,32},{32,64},{64,96},{96,128},{128,160},{160,192},{192,224},{224... | collective-permute-start | bytes 811016 | tf_op jit(solution)/shard_map/ppermute | solution.py:390
  63.7 12.6 %collective-permute-start.13 = (bf16[528,256]{1,0:T(8,128)(2,1)S(1)}, bf16[528,256]{1,0:T(8,128)(2,1)S(1)}, u32[]{:S(2)}, u32[]{:S(2)}) collective-permute-start(bf16[528,256]{1,0:T(8,128)(2,1)S(1)} %collective-permute-done.11.refs_4_.refs_13_.down), channel_id=1, source_target_pairs={{0,224},{32,0},{64,32},{96,64},{128,96},{160,128},{192,160},{224,1... | collective-permute-start | bytes 811016 | tf_op jit(solution)/shard_map/ppermute | solution.py:391
  75.7 34.4 %collective-permute-start.7 = (bf16[2,512,128]{2,1,0:T(8,128)(2,1)S(1)}, bf16[2,512,128]{2,1,0:T(8,128)(2,1)S(1)}, u32[]{:S(2)}, u32[]{:S(2)}) collective-permute-start(bf16[2,512,128]{2,1,0:T(8,128)(2,1)S(1)} %get-tuple-element.22.q.q0), channel_id=1, source_target_pairs={{0,16},{8,24},{16,0},{24,8},{1,17},{9,25},{17,1},{25,9},{2,18},{10... | collective-permute-start | bytes 786440 | tf_op jit(solution)/shard_map/ppermute | solution.py:339
  76.4 25.5 %collective-permute-start.14 = (bf16[528,128]{1,0:T(8,128)(2,1)S(1)}, bf16[528,128]{1,0:T(8,128)(2,1)S(1)}, u32[]{:S(2)}, u32[]{:S(2)}) collective-permute-start(bf16[528,128]{1,0:T(8,128)(2,1)S(1)} %slice.8), channel_id=1, source_target_pairs={{0,32},{32,64},{64,96},{96,128},{128,160},{160,192},{192,224},{224... | collective-permute-start | bytes 405512 | tf_op jit(solution)/shard_map/ppermute | solution.py:392
  76.5 25.7 %collective-permute-start.15 = (bf16[528,128]{1,0:T(8,128)(2,1)S(1)}, bf16[528,128]{1,0:T(8,128)(2,1)S(1)}, u32[]{:S(2)}, u32[]{:S(2)}) collective-permute-start(bf16[528,128]{1,0:T(8,128)(2,1)S(1)} %slice.9), channel_id=1, source_target_pairs={{0,224},{32,0},{64,32},{96,64},{128,96},{160,128},{192,160},{224,1... | collective-permute-start | bytes 405512 | tf_op jit(solution)/shard_map/ppermute | solution.py:393
  85.2 57.3 %collective-permute-start.24 = (bf16[256,2048]{1,0:T(8,128)(2,1)S(1)}, bf16[256,2048]{1,0:T(8,128)(2,1)}, u32[]{:S(2)}, u32[]{:S(2)}) collective-permute-start(bf16[256,2048]{1,0:T(8,128)(2,1)S(1)} %copy-done), channel_id=1, source_target_pairs={{0,1},{1,0},{2,3},{3,2},{4,5},{5,4},{6,7},{7,6},{8,9},{9,8},{10,11... | collective-permute-start | bytes 3145736 | tf_op jit(solution)/shard_map/ppermute | solution.py:343
  101.7 47.4 %collective-permute-start.25 = (bf16[256,2048]{1,0:T(8,128)(2,1)S(1)}, bf16[256,2048]{1,0:T(8,128)(2,1)}, u32[]{:S(2)}, u32[]{:S(2)}) collective-permute-start(bf16[256,2048]{1,0:T(8,128)(2,1)S(1)} %collective-permute-done.21.w1), channel_id=1, source_target_pairs={{0,1},{1,0},{2,3},{3,2},{4,5},{5,4},{6,7},{7,6},{8,9},{9,8},{10,11... | collective-permute-start | bytes 3145736 | tf_op jit(solution)/shard_map/ppermute | solution.py:343
  101.9 47.2 %collective-permute-start.26 = (bf16[256,2048]{1,0:T(8,128)(2,1)S(1)}, bf16[256,2048]{1,0:T(8,128)(2,1)}, u32[]{:S(2)}, u32[]{:S(2)}) collective-permute-start(bf16[256,2048]{1,0:T(8,128)(2,1)S(1)} %collective-permute-done.22.w2), channel_id=1, source_target_pairs={{0,1},{1,0},{2,3},{3,2},{4,5},{5,4},{6,7},{7,6},{8,9},{9,8},{10,11... | collective-permute-start | bytes 3145736 | tf_op jit(solution)/shard_map/ppermute | solution.py:343
  102.3 46.8 %collective-permute-start.27 = (bf16[256,2048]{1,0:T(8,128)(2,1)}, bf16[256,2048]{1,0:T(8,128)(2,1)}, u32[]{:S(2)}, u32[]{:S(2)}) collective-permute-start(bf16[256,2048]{1,0:T(8,128)(2,1)} %collective-permute-done.23.w3), channel_id=1, source_target_pairs={{0,1},{1,0},{2,3},{3,2},{4,5},{5,4},{6,7},{7,6},{8,9},{9,8},{10,11... | collective-permute-start | bytes 3145736 | tf_op jit(solution)/shard_map/ppermute | solution.py:343
  110.1 7.9 %collective-permute-start.19 = (bf16[2,528,128]{2,1,0:T(8,128)(2,1)S(1)}, bf16[2,528,128]{2,1,0:T(8,128)(2,1)S(1)}, u32[]{:S(2)}, u32[]{:S(2)}) collective-permute-start(bf16[2,528,128]{2,1,0:T(8,128)(2,1)S(1)} %get-tuple-element.37), channel_id=1, source_target_pairs={{0,24},{8,0},{16,8},{24,16},{1,25},{9,1},{17,9},{25,17},{2,26},{10... | collective-permute-start | bytes 811016 | tf_op jit(solution)/shard_map/ppermute | solution.py:422
  118.0 8.7 %collective-permute-start.20 = (bf16[2,528,128]{2,1,0:T(8,128)(2,1)S(1)}, bf16[2,528,128]{2,1,0:T(8,128)(2,1)S(1)}, u32[]{:S(2)}, u32[]{:S(2)}) collective-permute-start(bf16[2,528,128]{2,1,0:T(8,128)(2,1)S(1)} %get-tuple-element.38), channel_id=1, source_target_pairs={{0,8},{8,16},{16,24},{24,0},{1,9},{9,17},{17,25},{25,1},{2,10},{10... | collective-permute-start | bytes 811016 | tf_op jit(solution)/shard_map/ppermute | solution.py:423
  126.7 8.3 %collective-permute-start.16 = (bf16[2,528,128]{2,1,0:T(8,128)(2,1)S(1)}, bf16[2,528,128]{2,1,0:T(8,128)(2,1)S(1)}, u32[]{:S(2)}, u32[]{:S(2)}) collective-permute-start(bf16[2,528,128]{2,1,0:T(8,128)(2,1)S(1)} %shard_map.137), channel_id=1, source_target_pairs={{0,16},{8,24},{16,0},{24,8},{1,17},{9,25},{17,1},{25,9},{2,18},{10... | collective-permute-start | bytes 811016 | tf_op jit(solution)/shard_map/ppermute | solution.py:420
  136.4 12.7 %all-to-all-start.2 = ((bf16[8,64,256]{2,1,0:T(8,128)(2,1)}), bf16[8,64,256]{2,1,0:T(8,128)(2,1)}, u32[]{:S(2)}, u32[]{:S(2)}) async-start(bf16[8,64,256]{2,1,0:T(8,128)(2,1)} %copy-done.2), calls=%async_computation.2 | async-start | bytes 524288 | tf_op jit(solution)/shard_map/all_to_all | solution.py:426
  (2 other events, 1.7 us)

commit v5 on v4

--- a/solution.py
+++ b/solution.py
@@ -205,17 +205,12 @@
 
 
 def final_kernel(*refs, parts, lift, size):
-    q_all, m_in, l_in, acc_in, up, down, k_far, v_far = refs[:8]
-    tails = refs[8:15]
-    outs, (k_buf, v_buf) = refs[15:-2], refs[-2:]
-    fill(k_buf, v_buf, (up, down))
-    at = 2 * CHUNK
-    k_buf[at : at + CHUNK] = k_far[:CHUNK]
-    v_buf[at : at + CHUNK] = v_far[:CHUNK]
-    at += CHUNK
-    k_buf[at : at + 16] = k_far[CHUNK:]
-    v_buf[at : at + 16] = v_far[CHUNK:]
-    for t in tails:
+    q_all, m_in, l_in, acc_in, up, down, opposite = refs[:7]
+    tails = refs[7:14]
+    outs, (k_buf, v_buf) = refs[14:-2], refs[-2:]
+    fill(k_buf, v_buf, (up, down, opposite))
+    at = 3 * CHUNK - 16
+    for t in (opposite, *tails):
         at += 16
         k_buf[at : at + 16] = t[CHUNK:, :HD]
         v_buf[at : at + 16] = t[CHUNK:, HD:]
@@ -389,8 +384,7 @@
     for _ in range(2):
         up.append(lax.ppermute(up[-1], "z", shift(8, 1)))
         down.append(lax.ppermute(down[-1], "z", shift(8, -1)))
-    k_far = lax.ppermute(up[3][:, :HD], "z", shift(8, 1))
-    v_far = lax.ppermute(down[3][:, HD:], "z", shift(8, -1))
+    opposite = lax.ppermute(up[3], "z", shift(8, 1))
     first = lax.ppermute(out_weight, TP, ahead)
     second = lax.ppermute(out_weight, TP, behind)
     weights = [out_weight, first, second, lax.ppermute(out_weight, "y", shift(4, 2))]
@@ -412,7 +406,7 @@
     def final(whose, size, *parts):
         return call(
             functools.partial(final_kernel, parts=parts, lift=lift, size=size),
-            [*whose, up[3], down[3], k_far, v_far, kv, *up[1:], *down[1:]],
+            [*whose, up[3], down[3], opposite, kv, *up[1:], *down[1:]],
             [pltpu.VMEM((2, CHUNK + 16, HD), BF)] * len(parts), 3 * CHUNK + 2 * HD, 2 * CHUNK * len(parts),
         )
 

time: 155 us -> 156 us (level)
  waiting for transfers between devices: 40.4 us -> 48.7 us
  starting transfers between devices: 64.6 us -> 57.2 us
    ppermute x1, waiting for transfers between devices: 0.01 us -> 12.8 us  [body(): second = lax.ppermute(out_weight, TP, behind)]
    ppermute x8, starting transfers between devices: 18.4 us -> 10.1 us  [swap(): return lax.ppermute(v, 'c', [(0, 1), (1, 0)])]
    ppermute x1, waiting for transfers between devices: 0.01 us -> 4.13 us  [body(): down.append(lax.ppermute(kv, 'z', shift(8, -1)))]
    ppermute x1, waiting for transfers between devices: 4.13 us -> 0.01 us  [body(): up.append(lax.ppermute(kv, 'z', shift(8, 1)))]
    ppermute x2, waiting for transfers between devices: 4.14 us -> 0.01 us  [body(): up.append(lax.ppermute(up[-1], 'z', shift(8, 1)))]
    ppermute x2 -> x1, starting transfers between devices: 2.82 us -> 0.01 us  [body(): opposite = lax.ppermute(up[3], 'z', shift(8, 1))]
    ppermute x2, starting transfers between devices: 2.34 us -> 4.15 us  [over_four(): lax.ppermute(v, axis, shift(4, 2))]
  transfers between devices with their start and end apart: 31 -> 30, of which waited for: 8 -> 8; matrix products, arithmetic and copies ran while one was open for 1% -> 0% of each run, Pallas kernels for 25% -> 25%
where the time goes in v5:
time: 156 us
  starting transfers between devices  57.2 us (37%)
  waiting for transfers between devices  48.7 us (31%)
  Pallas kernels  47.5 us (30%)
  local copies, waits for them, and re-layouts  2.38 us (2%)
    pallas_call x8, Pallas kernels, call(): pl.pallas_call(kernel, out_shape=shape, in_specs=[VMEM] * len(operands),...  36.6 us
    ppermute x1, waiting for transfers between devices, body(): second = lax.ppermute(out_weight, TP, behind)  12.8 us
    ppermute x8, starting transfers between devices, swap(): return lax.ppermute(v, 'c', [(0, 1), (1, 0)])  10.1 us
    all_to_all x1, starting transfers between devices, body(): shares = lax.all_to_all(shares, ('z', 'c'), 0, 0)  10 us
    all_to_all x1, waiting for transfers between devices, body(): shares = lax.all_to_all(shares, ('z', 'c'), 0, 0)  7.42 us
    all_to_all x1, waiting for transfers between devices, body(): lax.all_to_all(jnp.broadcast_to(summed[None], (16,) + summed.shape), ('x'...  7.12 us
    all_to_all x1, waiting for transfers between devices, body(): got = lax.all_to_all(sent, TP, 0, 0)  6.57 us
    ppermute x1, waiting for transfers between devices, body(): partials.append(lax.ppermute(to_down, 'x', shift(4, -1)))  6.49 us
  transfers between devices with their start and end apart: 30, of which 8 were waited for; matrix products, arithmetic and copies ran while one was open for 0% of the time, Pallas kernels for 25%

profile of v5, /device:TPU:1, one launch (start us, length us, event | category | flops | bytes accessed | tf_op | source)
XLA Modules:
  0.0 156.0 jit_solution(18368330210382738518)
XLA Ops:
  0.0 2.1 %collective-permute-start = (bf16[64,2048]{1,0:T(8,128)(2,1)}, bf16[64,2048]{1,0:T(8,128)(2,1)S(1)}, u32[]{:S(2)}, u32[]{:S(2)}) collective-permute-start(bf16[64,2048]{1,0:T(8,128)(2,1)} %lat.1), channel_id=1, source_target_pairs={{0,2},{2,4},{4,6},{6,0},{1,3},{3,5},{5,7},{7,1},{8,10},{10,12},{12... | collective-permute-start | bytes 786440 | tf_op jit(solution)/shard_map/ppermute | solution.py:332
  2.1 1.4 collective-permute-start.1
  3.6 1.6 %collective-permute-start.2 = (bf16[64,2048]{1,0:T(8,128)(2,1)}, bf16[64,2048]{1,0:T(8,128)(2,1)S(1)}, u32[]{:S(2)}, u32[]{:S(2)}) collective-permute-start(bf16[64,2048]{1,0:T(8,128)(2,1)} %lat.1), channel_id=1, source_target_pairs={{0,4},{2,6},{4,0},{6,2},{1,5},{3,7},{5,1},{7,3},{8,12},{10,14},{12... | collective-permute-start | bytes 786440 | tf_op jit(solution)/shard_map/ppermute | solution.py:334
  5.2 1.8 %share.1 = f32[16,2,768]{2,1,0:T(2,128)} custom-call(f32[1,64]{1,0:T(1,128)} %bitcast.11, f32[1,64]{1,0:T(1,128)} %bitcast.12, f32[64,768]{1,0:T(8,128)} %refs_2_.1), custom_call_target="tpu_custom_call" | custom-call | tf_op jit(solution)/shard_map/share/pallas_call | solution.py:345
  7.0 10.0 %all-to-all-start = ((f32[16,2,768]{2,1,0:T(2,128)}), f32[16,2,768]{2,1,0:T(2,128)S(1)}, u32[]{:S(2)}, u32[]{:S(2)}) async-start(f32[16,2,768]{2,1,0:T(2,128)} %share.1), calls=%async_computation | async-start | bytes 196608 | tf_op jit(solution)/shard_map/all_to_all | solution.py:353
  18.1 7.4 %all-to-all-done = f32[16,2,768]{2,1,0:T(2,128)S(1)} async-done(((f32[16,2,768]{2,1,0:T(2,128)}), f32[16,2,768]{2,1,0:T(2,128)S(1)}, u32[]{:S(2)}, u32[]{:S(2)}) %all-to-all-start) | async-done | bytes 98336 | tf_op jit(solution)/shard_map/all_to_all | solution.py:353
  26.3 5.1 %all-to-all-start.1 = ((f32[16,2,2,768]{3,2,1,0:T(2,128)}), f32[16,2,2,768]{3,2,1,0:T(2,128)S(1)}, u32[]{:S(2)}, u32[]{:S(2)}) async-start(f32[16,2,2,768]{3,2,1,0:T(2,128)} %broadcast_in_dim.20), calls=%async_computation.1 | async-start | bytes 393216 | tf_op jit(solution)/shard_map/all_to_all | solution.py:356
  31.4 7.1 %all-to-all-done.1 = f32[16,2,2,768]{3,2,1,0:T(2,128)S(1)} async-done(((f32[16,2,2,768]{3,2,1,0:T(2,128)}), f32[16,2,2,768]{3,2,1,0:T(2,128)S(1)}, u32[]{:S(2)}, u32[]{:S(2)}) %all-to-all-start.1) | async-done | bytes 196640 | tf_op jit(solution)/shard_map/all_to_all | solution.py:356
  38.5 4.0 %project.1 = (bf16[2,512,128]{2,1,0:T(8,128)(2,1)S(1)}, bf16[528,256]{1,0:T(8,128)(2,1)S(1)}) custom-call(bf16[64,2048]{1,0:T(8,128)(2,1)S(1)} %collective-permute-done.refs_0_, bf16[64,2048]{1,0:T(8,128)(2,1)S(1)} %collective-permute-done.1.refs_1_, bf16[64,2048]{1,0:T(8,128)(2,1)S(1)} %collective-permute-done.2.refs_2_, ...), custom_call_target="tpu_custom_call" | custom-call | flops 1107296256 | bytes 4194304 | tf_op jit(solution)/shard_map/project/pallas_call | solution.py:363
  43.8 2.6 %collective-permute-start.17 = (bf16[2,512,128]{2,1,0:T(8,128)(2,1)S(1)}, bf16[2,512,128]{2,1,0:T(8,128)(2,1)S(1)}, u32[]{:S(2)}, u32[]{:S(2)}) collective-permute-start(bf16[2,512,128]{2,1,0:T(8,128)(2,1)S(1)} %get-tuple-element.22.q.q0), channel_id=1, source_target_pairs={{0,24},{8,0},{16,8},{24,16},{1,25},{9,1},{17,9},{25,17},{2,26},{10... | collective-permute-start | bytes 786440 | tf_op jit(solution)/shard_map/ppermute | solution.py:333
  46.8 3.3 %collective-permute-done.16.q1 = bf16[2,512,128]{2,1,0:T(8,128)(2,1)S(1)} collective-permute-done((bf16[2,512,128]{2,1,0:T(8,128)(2,1)S(1)}, bf16[2,512,128]{2,1,0:T(8,128)(2,1)S(1)}, u32[]{:S(2)}, u32[]{:S(2)}) %collective-permute-start.16) | collective-permute-done | bytes 262176 | tf_op jit(solution)/shard_map/ppermute | solution.py:332
  50.1 1.7 %collective-permute-start.22 = (bf16[256,2048]{1,0:T(8,128)(2,1)S(1)}, bf16[256,2048]{1,0:T(8,128)(2,1)}, u32[]{:S(2)}, u32[]{:S(2)}) collective-permute-start(bf16[256,2048]{1,0:T(8,128)(2,1)S(1)} %copy-done), channel_id=1, source_target_pairs={{0,4},{2,6},{4,0},{6,2},{1,5},{3,7},{5,1},{7,3},{8,12},{10,14},{12... | collective-permute-start | bytes 3145736 | tf_op jit(solution)/shard_map/ppermute | solution.py:390
  51.8 1.3 collective-permute-start.9
  53.3 4.1 %collective-permute-done.9.refs_2_.refs_11_.down = bf16[528,256]{1,0:T(8,128)(2,1)S(1)} collective-permute-done((bf16[528,256]{1,0:T(8,128)(2,1)S(1)}, bf16[528,256]{1,0:T(8,128)(2,1)S(1)}, u32[]{:S(2)}, u32[]{:S(2)}) %collective-permute-start.9) | collective-permute-done | bytes 270368 | tf_op jit(solution)/shard_map/ppermute | solution.py:382
  57.4 2.5 %collective-permute-start.11 = (bf16[528,256]{1,0:T(8,128)(2,1)S(1)}, bf16[528,256]{1,0:T(8,128)(2,1)S(1)}, u32[]{:S(2)}, u32[]{:S(2)}) collective-permute-start(bf16[528,256]{1,0:T(8,128)(2,1)S(1)} %collective-permute-done.9.refs_2_.refs_11_.down), channel_id=1, source_target_pairs={{0,224},{32,0},{64,32},{96,64},{128,96},{160,128},{192,160},{224,1... | collective-permute-start | bytes 811016 | tf_op jit(solution)/shard_map/ppermute | solution.py:386
  59.9 3.6 %shard_map.138 = (f32[1024,128]{1,0:T(8,128)S(1)}, f32[1024,128]{1,0:T(8,128)S(1)}, f32[1024,128]{1,0:T(8,128)S(1)}) custom-call(bf16[2,512,128]{2,1,0:T(8,128)(2,1)S(1)} %get-tuple-element.22.q.q0, bf16[528,256]{1,0:T(8,128)(2,1)S(1)} %get-tuple-element.23.refs_0_.refs_7_.kv, bf16[528,256]{1,0:T(8,128)(2,1)S(1)} %collective-permute-done.8.refs_1_.refs_8_.up, ...), custom_call_target="tpu_custom_call" | custom-call | flops 805306368 | bytes 1048576 | tf_op jit(solution)/shard_map/pallas_call | solution.py:296
  63.5 3.2 %collective-permute-start.13 = (bf16[528,256]{1,0:T(8,128)(2,1)S(1)}, bf16[528,256]{1,0:T(8,128)(2,1)S(1)}, u32[]{:S(2)}, u32[]{:S(2)}) collective-permute-start(bf16[528,256]{1,0:T(8,128)(2,1)S(1)} %collective-permute-done.11.refs_4_.refs_12_.down), channel_id=1, source_target_pairs={{0,224},{32,0},{64,32},{96,64},{128,96},{160,128},{192,160},{224,1... | collective-permute-start | bytes 811016 | tf_op jit(solution)/shard_map/ppermute | solution.py:386
  66.7 5.7 %shard_map.139 = (bf16[3072,128]{1,0:T(8,128)(2,1)S(1)}, f32[3072,128]{1,0:T(8,128)S(1)}, f32[3072,128]{1,0:T(8,128)S(1)}, f32[3072,128]{1,0:T(8,128)S(1)}) custom-call(bf16[2,512,128]{2,1,0:T(8,128)(2,1)S(1)} %get-tuple-element.22.q.q0, bf16[2,512,128]{2,1,0:T(8,128)(2,1)S(1)} %collective-permute-done.16.q1, ...), custom_call_target="tpu_custom_call" | custom-call | flops 1610612736 | bytes 1048576 | tf_op jit(solution)/shard_map/pallas_call | solution.py:296
  72.4 2.5 %collective-permute-start.7 = (bf16[2,512,128]{2,1,0:T(8,128)(2,1)S(1)}, bf16[2,512,128]{2,1,0:T(8,128)(2,1)S(1)}, u32[]{:S(2)}, u32[]{:S(2)}) collective-permute-start(bf16[2,512,128]{2,1,0:T(8,128)(2,1)S(1)} %get-tuple-element.22.q.q0), channel_id=1, source_target_pairs={{0,16},{8,24},{16,0},{24,8},{1,17},{9,25},{17,1},{25,9},{2,18},{10... | collective-permute-start | bytes 786440 | tf_op jit(solution)/shard_map/ppermute | solution.py:334
  74.9 5.9 %shard_map.140 = (f32[3072,128]{1,0:T(8,128)S(1)}, f32[3072,128]{1,0:T(8,128)S(1)}, f32[3072,128]{1,0:T(8,128)S(1)}) custom-call(bf16[3072,128]{1,0:T(8,128)(2,1)S(1)} %get-tuple-element.30.q_all.refs_0_, f32[3072,128]{1,0:T(8,128)S(1)} %get-tuple-element.31.m_in, ...), custom_call_target="tpu_custom_call", output_to_operand_aliasing={{0}: (1, {}), {1}: (2, {}), {2}: (3, {})} | custom-call | flops 1610612736 | bytes 1048576 | tf_op jit(solution)/shard_map/pallas_call | solution.py:296
  80.9 12.8 %collective-permute-done.21.w2 = bf16[256,2048]{1,0:T(8,128)(2,1)S(1)} collective-permute-done((bf16[256,2048]{1,0:T(8,128)(2,1)S(1)}, bf16[256,2048]{1,0:T(8,128)(2,1)S(1)}, u32[]{:S(2)}, u32[]{:S(2)}) %collective-permute-start.21) | collective-permute-done | bytes 1048608 | tf_op jit(solution)/shard_map/ppermute | solution.py:389
  93.7 8.2 %collective-permute-start.23 = (bf16[256,2048]{1,0:T(8,128)(2,1)S(1)}, bf16[256,2048]{1,0:T(8,128)(2,1)}, u32[]{:S(2)}, u32[]{:S(2)}) collective-permute-start(bf16[256,2048]{1,0:T(8,128)(2,1)S(1)} %copy-done), channel_id=1, source_target_pairs={{0,1},{1,0},{2,3},{3,2},{4,5},{5,4},{6,7},{7,6},{8,9},{9,8},{10,11... | collective-permute-start | bytes 3145736 | tf_op jit(solution)/shard_map/ppermute | solution.py:338
  102.7 7.5 %shard_map.141 = (bf16[2,528,128]{2,1,0:T(8,128)(2,1)S(1)}, bf16[2,528,128]{2,1,0:T(8,128)(2,1)S(1)}) custom-call(bf16[3072,128]{1,0:T(8,128)(2,1)S(1)} %get-tuple-element.30.q_all.refs_0_, f32[3072,128]{1,0:T(8,128)S(1)} %get-tuple-element.34.refs_1_, f32[3072,128]{1,0:T(8,128)S(1)} %get-tuple-element.35.refs_2_, ...), custom_call_target="tpu_custom_call" | custom-call | flops 1879048192 | bytes 1048576 | tf_op jit(solution)/shard_map/pallas_call | solution.py:296
  110.3 1.4 collective-permute-start.18
  111.7 6.5 %collective-permute-done.18.p1 = bf16[2,528,128]{2,1,0:T(8,128)(2,1)S(1)} collective-permute-done((bf16[2,528,128]{2,1,0:T(8,128)(2,1)S(1)}, bf16[2,528,128]{2,1,0:T(8,128)(2,1)S(1)}, u32[]{:S(2)}, u32[]{:S(2)}) %collective-permute-start.18) | collective-permute-done | bytes 270368 | tf_op jit(solution)/shard_map/ppermute | solution.py:416
  118.8 4.9 %shard_map.136 = (f32[1024,128]{1,0:T(8,128)S(1)}, f32[1024,128]{1,0:T(8,128)S(1)}, f32[1024,128]{1,0:T(8,128)S(1)}) custom-call(bf16[2,512,128]{2,1,0:T(8,128)(2,1)S(1)} %collective-permute-done.7.q, bf16[528,256]{1,0:T(8,128)(2,1)S(1)} %get-tuple-element.23.refs_0_.refs_7_.kv, bf16[528,256]{1,0:T(8,128)(2,1)S(1)} %collective-permute-done.8.refs_1_.refs_8_.up, ...), custom_call_target="tpu_custom_call" | custom-call | flops 1342177280 | bytes 1048576 | tf_op jit(solution)/shard_map/pallas_call | solution.py:296
  123.7 3.8 %shard_map.137 = bf16[2,528,128]{2,1,0:T(8,128)(2,1)S(1)} custom-call(bf16[1024,128]{1,0:T(8,128)(2,1)S(1)} %bitcast.9, f32[1024,128]{1,0:T(8,128)S(1)} %get-tuple-element.24.refs_1_, f32[1024,128]{1,0:T(8,128)S(1)} %get-tuple-element.25.refs_2_, f32[1024,128]{1,0:T(8,128)S(1)} %get-tuple-element.26.refs_3_, ...), custom_call_target="tpu_custom_call" | custom-call | flops 939524096 | bytes 1048576 | tf_op jit(solution)/shard_map/pallas_call | solution.py:296
  127.6 3.2 %collective-permute-start.15 = (bf16[2,528,128]{2,1,0:T(8,128)(2,1)S(1)}, bf16[2,528,128]{2,1,0:T(8,128)(2,1)S(1)}, u32[]{:S(2)}, u32[]{:S(2)}) collective-permute-start(bf16[2,528,128]{2,1,0:T(8,128)(2,1)S(1)} %shard_map.137), channel_id=1, source_target_pairs={{0,16},{8,24},{16,0},{24,8},{1,17},{9,25},{17,1},{25,9},{2,18},{10... | collective-permute-start | bytes 811016 | tf_op jit(solution)/shard_map/ppermute | solution.py:414
  130.7 4.6 %shard_map.142.p3 = bf16[2,528,128]{2,1,0:T(8,128)(2,1)S(1)} custom-call(bf16[3072,128]{1,0:T(8,128)(2,1)S(1)} %get-tuple-element.30.q_all.refs_0_, f32[3072,128]{1,0:T(8,128)S(1)} %get-tuple-element.34.refs_1_, f32[3072,128]{1,0:T(8,128)S(1)} %get-tuple-element.35.refs_2_, f32[3072,128]{1,0:T(8,128)S(1)} %get-tuple-element.36.refs_3_, ...), custom_call_target="tpu_custom_call" | custom-call | flops 939524096 | bytes 1048576 | tf_op jit(solution)/shard_map/pallas_call | solution.py:296
  137.5 6.0 %all-to-all-start.2 = ((bf16[8,64,256]{2,1,0:T(8,128)(2,1)}), bf16[8,64,256]{2,1,0:T(8,128)(2,1)}, u32[]{:S(2)}, u32[]{:S(2)}) async-start(bf16[8,64,256]{2,1,0:T(8,128)(2,1)} %copy-done.2), calls=%async_computation.2 | async-start | bytes 524288 | tf_op jit(solution)/shard_map/all_to_all | solution.py:420
  143.5 6.6 %all-to-all-done.2.got = bf16[8,64,256]{2,1,0:T(8,128)(2,1)} async-done(((bf16[8,64,256]{2,1,0:T(8,128)(2,1)}), bf16[8,64,256]{2,1,0:T(8,128)(2,1)}, u32[]{:S(2)}, u32[]{:S(2)}) %all-to-all-start.2) | async-done | bytes 262176 | tf_op jit(solution)/shard_map/all_to_all | solution.py:420
  151.0 5.0 %finish.1 = bf16[64,2048]{1,0:T(8,128)(2,1)} custom-call(bf16[8,64,256]{2,1,0:T(8,128)(2,1)} %all-to-all-done.2.got, bf16[256,2048]{1,0:T(8,128)(2,1)S(1)} %copy-done, bf16[256,2048]{1,0:T(8,128)(2,1)S(1)} %collective-permute-done.20.w1, bf16[256,2048]{1,0:T(8,128)(2,1)S(1)} %collective-permute-done.21.w2, bf16[256,2048]{1,0:T(8,128)(2,1)} %collective-permute-done.22.w3, ...), custom_call_target="tpu_custom_call" | custom-call | flops 536870912 | bytes 10485760 | tf_op jit(solution)/shard_map/finish/pallas_call | solution.py:422
  (47 shorter events, 8.2 us)
Async XLA Ops:
  0.0 17.2 %collective-permute-start = (bf16[64,2048]{1,0:T(8,128)(2,1)}, bf16[64,2048]{1,0:T(8,128)(2,1)S(1)}, u32[]{:S(2)}, u32[]{:S(2)}) collective-permute-start(bf16[64,2048]{1,0:T(8,128)(2,1)} %lat.1), channel_id=1, source_target_pairs={{0,2},{2,4},{4,6},{6,0},{1,3},{3,5},{5,7},{7,1},{8,10},{10,12},{12... | collective-permute-start | bytes 786440 | tf_op jit(solution)/shard_map/ppermute | solution.py:332
  2.1 15.4 %collective-permute-start.1 = (bf16[64,2048]{1,0:T(8,128)(2,1)}, bf16[64,2048]{1,0:T(8,128)(2,1)S(1)}, u32[]{:S(2)}, u32[]{:S(2)}) collective-permute-start(bf16[64,2048]{1,0:T(8,128)(2,1)} %lat.1), channel_id=1, source_target_pairs={{0,6},{2,0},{4,2},{6,4},{1,7},{3,1},{5,3},{7,5},{8,14},{10,8},{12,... | collective-permute-start | bytes 786440 | tf_op jit(solution)/shard_map/ppermute | solution.py:333
  3.6 14.2 %collective-permute-start.2 = (bf16[64,2048]{1,0:T(8,128)(2,1)}, bf16[64,2048]{1,0:T(8,128)(2,1)S(1)}, u32[]{:S(2)}, u32[]{:S(2)}) collective-permute-start(bf16[64,2048]{1,0:T(8,128)(2,1)} %lat.1), channel_id=1, source_target_pairs={{0,4},{2,6},{4,0},{6,2},{1,5},{3,7},{5,1},{7,3},{8,12},{10,14},{12... | collective-permute-start | bytes 786440 | tf_op jit(solution)/shard_map/ppermute | solution.py:334
  7.0 18.5 %all-to-all-start = ((f32[16,2,768]{2,1,0:T(2,128)}), f32[16,2,768]{2,1,0:T(2,128)S(1)}, u32[]{:S(2)}, u32[]{:S(2)}) async-start(f32[16,2,768]{2,1,0:T(2,128)} %share.1), calls=%async_computation | async-start | bytes 196608 | tf_op jit(solution)/shard_map/all_to_all | solution.py:353
  17.0 14.3 %collective-permute-start.3 = (bf16[64,2048]{1,0:T(8,128)(2,1)}, bf16[64,2048]{1,0:T(8,128)(2,1)S(1)}, u32[]{:S(2)}, u32[]{:S(2)}) collective-permute-start(bf16[64,2048]{1,0:T(8,128)(2,1)} %lat.1), channel_id=1, source_target_pairs={{0,1},{1,0},{2,3},{3,2},{4,5},{5,4},{6,7},{7,6},{8,9},{9,8},{10,11... | collective-permute-start | bytes 786440 | tf_op jit(solution)/shard_map/ppermute | solution.py:338
  17.2 21.3 %collective-permute-start.4 = (bf16[64,2048]{1,0:T(8,128)(2,1)S(1)}, bf16[64,2048]{1,0:T(8,128)(2,1)S(1)}, u32[]{:S(2)}, u32[]{:S(2)}) collective-permute-start(bf16[64,2048]{1,0:T(8,128)(2,1)S(1)} %collective-permute-done.refs_0_), channel_id=1, source_target_pairs={{0,1},{1,0},{2,3},{3,2},{4,5},{5,4},{6,7},{7,6},{8,9},{9,8},{10,11... | collective-permute-start | bytes 786440 | tf_op jit(solution)/shard_map/ppermute | solution.py:338
  17.6 21.0 %collective-permute-start.5 = (bf16[64,2048]{1,0:T(8,128)(2,1)S(1)}, bf16[64,2048]{1,0:T(8,128)(2,1)S(1)}, u32[]{:S(2)}, u32[]{:S(2)}) collective-permute-start(bf16[64,2048]{1,0:T(8,128)(2,1)S(1)} %collective-permute-done.1.refs_1_), channel_id=1, source_target_pairs={{0,1},{1,0},{2,3},{3,2},{4,5},{5,4},{6,7},{7,6},{8,9},{9,8},{10,11... | collective-permute-start | bytes 786440 | tf_op jit(solution)/shard_map/ppermute | solution.py:338
  17.8 20.8 %collective-permute-start.6 = (bf16[64,2048]{1,0:T(8,128)(2,1)S(1)}, bf16[64,2048]{1,0:T(8,128)(2,1)S(1)}, u32[]{:S(2)}, u32[]{:S(2)}) collective-permute-start(bf16[64,2048]{1,0:T(8,128)(2,1)S(1)} %collective-permute-done.2.refs_2_), channel_id=1, source_target_pairs={{0,1},{1,0},{2,3},{3,2},{4,5},{5,4},{6,7},{7,6},{8,9},{9,8},{10,11... | collective-permute-start | bytes 786440 | tf_op jit(solution)/shard_map/ppermute | solution.py:338
  26.3 12.2 %all-to-all-start.1 = ((f32[16,2,2,768]{3,2,1,0:T(2,128)}), f32[16,2,2,768]{3,2,1,0:T(2,128)S(1)}, u32[]{:S(2)}, u32[]{:S(2)}) async-start(f32[16,2,2,768]{3,2,1,0:T(2,128)} %broadcast_in_dim.20), calls=%async_computation.1 | async-start | bytes 393216 | tf_op jit(solution)/shard_map/all_to_all | solution.py:356
  38.5 4.4 %copy-start = (bf16[256,2048]{1,0:T(8,128)(2,1)S(1)}, bf16[256,2048]{1,0:T(8,128)(2,1)}, u32[]{:S(2)}) copy-start(bf16[256,2048]{1,0:T(8,128)(2,1)} %w0.1) | copy-start | bytes 3145732
  42.6 7.5 %collective-permute-start.16 = (bf16[2,512,128]{2,1,0:T(8,128)(2,1)S(1)}, bf16[2,512,128]{2,1,0:T(8,128)(2,1)S(1)}, u32[]{:S(2)}, u32[]{:S(2)}) collective-permute-start(bf16[2,512,128]{2,1,0:T(8,128)(2,1)S(1)} %get-tuple-element.22.q.q0), channel_id=1, source_target_pairs={{0,8},{8,16},{16,24},{24,0},{1,9},{9,17},{17,25},{25,1},{2,10},{10... | collective-permute-start | bytes 786440 | tf_op jit(solution)/shard_map/ppermute | solution.py:332
  42.9 29.5 %collective-permute-start.20 = (bf16[256,2048]{1,0:T(8,128)(2,1)S(1)}, bf16[256,2048]{1,0:T(8,128)(2,1)S(1)}, u32[]{:S(2)}, u32[]{:S(2)}) collective-permute-start(bf16[256,2048]{1,0:T(8,128)(2,1)S(1)} %copy-done), channel_id=1, source_target_pairs={{0,2},{1,7},{2,4},{3,1},{4,6},{5,3},{6,0},{7,5},{8,10},{9,15},{10,... | collective-permute-start | bytes 3145736 | tf_op jit(solution)/shard_map/ppermute | solution.py:388
  43.8 9.3 %collective-permute-start.8 = (bf16[528,256]{1,0:T(8,128)(2,1)S(1)}, bf16[528,256]{1,0:T(8,128)(2,1)S(1)}, u32[]{:S(2)}, u32[]{:S(2)}) collective-permute-start(bf16[528,256]{1,0:T(8,128)(2,1)S(1)} %get-tuple-element.23.refs_0_.refs_7_.kv), channel_id=1, source_target_pairs={{0,32},{32,64},{64,96},{96,128},{128,160},{160,192},{192,224},{224... | collective-permute-start | bytes 811016 | tf_op jit(solution)/shard_map/ppermute | solution.py:381
  43.8 8.0 %collective-permute-start.17 = (bf16[2,512,128]{2,1,0:T(8,128)(2,1)S(1)}, bf16[2,512,128]{2,1,0:T(8,128)(2,1)S(1)}, u32[]{:S(2)}, u32[]{:S(2)}) collective-permute-start(bf16[2,512,128]{2,1,0:T(8,128)(2,1)S(1)} %get-tuple-element.22.q.q0), channel_id=1, source_target_pairs={{0,24},{8,0},{16,8},{24,16},{1,25},{9,1},{17,9},{25,17},{2,26},{10... | collective-permute-start | bytes 786440 | tf_op jit(solution)/shard_map/ppermute | solution.py:333
  46.4 47.3 %collective-permute-start.21 = (bf16[256,2048]{1,0:T(8,128)(2,1)S(1)}, bf16[256,2048]{1,0:T(8,128)(2,1)S(1)}, u32[]{:S(2)}, u32[]{:S(2)}) collective-permute-start(bf16[256,2048]{1,0:T(8,128)(2,1)S(1)} %copy-done), channel_id=1, source_target_pairs={{2,0},{7,1},{4,2},{1,3},{6,4},{3,5},{0,6},{5,7},{10,8},{15,9},{12,... | collective-permute-start | bytes 3145736 | tf_op jit(solution)/shard_map/ppermute | solution.py:389
  50.1 51.8 %collective-permute-start.22 = (bf16[256,2048]{1,0:T(8,128)(2,1)S(1)}, bf16[256,2048]{1,0:T(8,128)(2,1)}, u32[]{:S(2)}, u32[]{:S(2)}) collective-permute-start(bf16[256,2048]{1,0:T(8,128)(2,1)S(1)} %copy-done), channel_id=1, source_target_pairs={{0,4},{2,6},{4,0},{6,2},{1,5},{3,7},{5,1},{7,3},{8,12},{10,14},{12... | collective-permute-start | bytes 3145736 | tf_op jit(solution)/shard_map/ppermute | solution.py:390
  51.8 5.6 %collective-permute-start.9 = (bf16[528,256]{1,0:T(8,128)(2,1)S(1)}, bf16[528,256]{1,0:T(8,128)(2,1)S(1)}, u32[]{:S(2)}, u32[]{:S(2)}) collective-permute-start(bf16[528,256]{1,0:T(8,128)(2,1)S(1)} %get-tuple-element.23.refs_0_.refs_7_.kv), channel_id=1, source_target_pairs={{0,224},{32,0},{64,32},{96,64},{128,96},{160,128},{192,160},{224,1... | collective-permute-start | bytes 811016 | tf_op jit(solution)/shard_map/ppermute | solution.py:382
  53.1 6.8 %collective-permute-start.10 = (bf16[528,256]{1,0:T(8,128)(2,1)S(1)}, bf16[528,256]{1,0:T(8,128)(2,1)S(1)}, u32[]{:S(2)}, u32[]{:S(2)}) collective-permute-start(bf16[528,256]{1,0:T(8,128)(2,1)S(1)} %collective-permute-done.8.refs_1_.refs_8_.up), channel_id=1, source_target_pairs={{0,32},{32,64},{64,96},{96,128},{128,160},{160,192},{192,224},{224... | collective-permute-start | bytes 811016 | tf_op jit(solution)/shard_map/ppermute | solution.py:385
  57.4 6.0 %collective-permute-start.11 = (bf16[528,256]{1,0:T(8,128)(2,1)S(1)}, bf16[528,256]{1,0:T(8,128)(2,1)S(1)}, u32[]{:S(2)}, u32[]{:S(2)}) collective-permute-start(bf16[528,256]{1,0:T(8,128)(2,1)S(1)} %collective-permute-done.9.refs_2_.refs_11_.down), channel_id=1, source_target_pairs={{0,224},{32,0},{64,32},{96,64},{128,96},{160,128},{192,160},{224,1... | collective-permute-start | bytes 811016 | tf_op jit(solution)/shard_map/ppermute | solution.py:386
  59.9 6.8 %collective-permute-start.12 = (bf16[528,256]{1,0:T(8,128)(2,1)S(1)}, bf16[528,256]{1,0:T(8,128)(2,1)S(1)}, u32[]{:S(2)}, u32[]{:S(2)}) collective-permute-start(bf16[528,256]{1,0:T(8,128)(2,1)S(1)} %collective-permute-done.10.refs_3_.refs_9_.up), channel_id=1, source_target_pairs={{0,32},{32,64},{64,96},{96,128},{128,160},{160,192},{192,224},{224... | collective-permute-start | bytes 811016 | tf_op jit(solution)/shard_map/ppermute | solution.py:385
  63.5 38.6 %collective-permute-start.13 = (bf16[528,256]{1,0:T(8,128)(2,1)S(1)}, bf16[528,256]{1,0:T(8,128)(2,1)S(1)}, u32[]{:S(2)}, u32[]{:S(2)}) collective-permute-start(bf16[528,256]{1,0:T(8,128)(2,1)S(1)} %collective-permute-done.11.refs_4_.refs_12_.down), channel_id=1, source_target_pairs={{0,224},{32,0},{64,32},{96,64},{128,96},{160,128},{192,160},{224,1... | collective-permute-start | bytes 811016 | tf_op jit(solution)/shard_map/ppermute | solution.py:386
  66.7 35.7 %collective-permute-start.14 = (bf16[528,256]{1,0:T(8,128)(2,1)S(1)}, bf16[528,256]{1,0:T(8,128)(2,1)S(1)}, u32[]{:S(2)}, u32[]{:S(2)}) collective-permute-start(bf16[528,256]{1,0:T(8,128)(2,1)S(1)} %collective-permute-done.12.refs_4_.refs_10_), channel_id=1, source_target_pairs={{0,32},{32,64},{64,96},{96,128},{128,160},{160,192},{192,224},{224... | collective-permute-start | bytes 811016 | tf_op jit(solution)/shard_map/ppermute | solution.py:387
  72.4 37.9 %collective-permute-start.7 = (bf16[2,512,128]{2,1,0:T(8,128)(2,1)S(1)}, bf16[2,512,128]{2,1,0:T(8,128)(2,1)S(1)}, u32[]{:S(2)}, u32[]{:S(2)}) collective-permute-start(bf16[2,512,128]{2,1,0:T(8,128)(2,1)S(1)} %get-tuple-element.22.q.q0), channel_id=1, source_target_pairs={{0,16},{8,24},{16,0},{24,8},{1,17},{9,25},{17,1},{25,9},{2,18},{10... | collective-permute-start | bytes 786440 | tf_op jit(solution)/shard_map/ppermute | solution.py:334
  93.7 49.8 %collective-permute-start.23 = (bf16[256,2048]{1,0:T(8,128)(2,1)S(1)}, bf16[256,2048]{1,0:T(8,128)(2,1)}, u32[]{:S(2)}, u32[]{:S(2)}) collective-permute-start(bf16[256,2048]{1,0:T(8,128)(2,1)S(1)} %copy-done), channel_id=1, source_target_pairs={{0,1},{1,0},{2,3},{3,2},{4,5},{5,4},{6,7},{7,6},{8,9},{9,8},{10,11... | collective-permute-start | bytes 3145736 | tf_op jit(solution)/shard_map/ppermute | solution.py:338
  101.9 41.5 %collective-permute-start.24 = (bf16[256,2048]{1,0:T(8,128)(2,1)S(1)}, bf16[256,2048]{1,0:T(8,128)(2,1)}, u32[]{:S(2)}, u32[]{:S(2)}) collective-permute-start(bf16[256,2048]{1,0:T(8,128)(2,1)S(1)} %collective-permute-done.20.w1), channel_id=1, source_target_pairs={{0,1},{1,0},{2,3},{3,2},{4,5},{5,4},{6,7},{7,6},{8,9},{9,8},{10,11... | collective-permute-start | bytes 3145736 | tf_op jit(solution)/shard_map/ppermute | solution.py:338
  102.0 41.4 %collective-permute-start.25 = (bf16[256,2048]{1,0:T(8,128)(2,1)S(1)}, bf16[256,2048]{1,0:T(8,128)(2,1)}, u32[]{:S(2)}, u32[]{:S(2)}) collective-permute-start(bf16[256,2048]{1,0:T(8,128)(2,1)S(1)} %collective-permute-done.21.w2), channel_id=1, source_target_pairs={{0,1},{1,0},{2,3},{3,2},{4,5},{5,4},{6,7},{7,6},{8,9},{9,8},{10,11... | collective-permute-start | bytes 3145736 | tf_op jit(solution)/shard_map/ppermute | solution.py:338
  102.4 41.0 %collective-permute-start.26 = (bf16[256,2048]{1,0:T(8,128)(2,1)}, bf16[256,2048]{1,0:T(8,128)(2,1)}, u32[]{:S(2)}, u32[]{:S(2)}) collective-permute-start(bf16[256,2048]{1,0:T(8,128)(2,1)} %collective-permute-done.22.w3), channel_id=1, source_target_pairs={{0,1},{1,0},{2,3},{3,2},{4,5},{5,4},{6,7},{7,6},{8,9},{9,8},{10,11... | collective-permute-start | bytes 3145736 | tf_op jit(solution)/shard_map/ppermute | solution.py:338
  110.3 7.9 %collective-permute-start.18 = (bf16[2,528,128]{2,1,0:T(8,128)(2,1)S(1)}, bf16[2,528,128]{2,1,0:T(8,128)(2,1)S(1)}, u32[]{:S(2)}, u32[]{:S(2)}) collective-permute-start(bf16[2,528,128]{2,1,0:T(8,128)(2,1)S(1)} %get-tuple-element.37), channel_id=1, source_target_pairs={{0,24},{8,0},{16,8},{24,16},{1,25},{9,1},{17,9},{25,17},{2,26},{10... | collective-permute-start | bytes 811016 | tf_op jit(solution)/shard_map/ppermute | solution.py:416
  118.2 9.4 %collective-permute-start.19 = (bf16[2,528,128]{2,1,0:T(8,128)(2,1)S(1)}, bf16[2,528,128]{2,1,0:T(8,128)(2,1)S(1)}, u32[]{:S(2)}, u32[]{:S(2)}) collective-permute-start(bf16[2,528,128]{2,1,0:T(8,128)(2,1)S(1)} %get-tuple-element.38), channel_id=1, source_target_pairs={{0,8},{8,16},{16,24},{24,0},{1,9},{9,17},{17,25},{25,1},{2,10},{10... | collective-permute-start | bytes 811016 | tf_op jit(solution)/shard_map/ppermute | solution.py:417
  127.6 8.5 %collective-permute-start.15 = (bf16[2,528,128]{2,1,0:T(8,128)(2,1)S(1)}, bf16[2,528,128]{2,1,0:T(8,128)(2,1)S(1)}, u32[]{:S(2)}, u32[]{:S(2)}) collective-permute-start(bf16[2,528,128]{2,1,0:T(8,128)(2,1)S(1)} %shard_map.137), channel_id=1, source_target_pairs={{0,16},{8,24},{16,0},{24,8},{1,17},{9,25},{17,1},{25,9},{2,18},{10... | collective-permute-start | bytes 811016 | tf_op jit(solution)/shard_map/ppermute | solution.py:414
  137.5 12.6 %all-to-all-start.2 = ((bf16[8,64,256]{2,1,0:T(8,128)(2,1)}), bf16[8,64,256]{2,1,0:T(8,128)(2,1)}, u32[]{:S(2)}, u32[]{:S(2)}) async-start(bf16[8,64,256]{2,1,0:T(8,128)(2,1)} %copy-done.2), calls=%async_computation.2 | async-start | bytes 524288 | tf_op jit(solution)/shard_map/all_to_all | solution.py:420
  150.0 1.0 copy-start.1
  (1 other events, 0.7 us)
